TPU v7x, 256 devices: a whole 4x4x8 slice. The times are simulated.
256 devices in a mesh: sp: 64 (over z, y, core), tp: 4 (over x).
Axes of the slice: x: 4, y: 4, z: 8, core: 2. Of those that a mesh axis runs over, the one named last changes fastest.
Arguments:
- residual: bfloat16 [12288, 2048], P(('sp', 'tp')), may hold values from -6 to 6
- mixer_input: bfloat16 [12288, 512], P('sp', 'tp'), may hold values from -6 to 6
- log_gate: float32 [12288, 32], P('sp', 'tp'), may hold values from -2 to 0
- decay_rate: float32 [2, 32, 64], P(None, 'tp'), may hold values from 0 to 1
- turn_rate: float32 [2, 32, 64], P(None, 'tp'), may hold values from -1 to 1
- drive_real: float32 [2, 32, 16, 64], P(None, 'tp'), may hold values from -1 to 1
- drive_imaginary: float32 [2, 32, 16, 64], P(None, 'tp'), may hold values from -1 to 1
- read_real: float32 [2, 32, 16, 64], P(None, 'tp'), may hold values from -0.75 to 0.75
- read_imaginary: float32 [2, 32, 16, 64], P(None, 'tp'), may hold values from -0.75 to 0.75
- skip_gain: float32 [512], P('tp'), may hold values from -4 to 4
- project_weight: bfloat16 [512, 2048], replicated, may hold values from -0.25 to 0.25
- norm_gain: float32 [2048], replicated, may hold values from 0.1 to 1.9
- final_gain: float32 [2048], replicated, may hold values from 0.1 to 1.9
- routes: int32 [12288, 2], P('sp'), may hold values from 0 to 63, all different within a row; in each aligned block of 48 rows (0 to 47, 48 to 95, ...) at most 2 rows name the same one
- group_weight: float32 [12288], P('sp'), may hold values from 0.2 to 1
- expert_weight: float32 [12288, 2], P('sp'), may hold values from 0.1 to 1
- gate_weight: bfloat16 [64, 2048, 1024], P('sp', None, 'tp'), may hold values from -0.125 to 0.125
- linear_weight: bfloat16 [64, 2048, 1024], P('sp', None, 'tp'), may hold values from -0.125 to 0.125
- down_weight: bfloat16 [64, 1024, 2048], P('sp', 'tp'), may hold values from -0.1875 to 0.1875
Outputs:
- finished: bfloat16 [12288, 2048], P(('sp', 'tp'))
Inputs may be any that keep to these rules, and one draw needn't show every extreme that they name: `routes`: each row names 2 different experts. In each aligned block of 48 rows no expert is named by more than 2 rows; some expert is named by exactly 2 rows of some block.
All inputs are finite; a program needn't handle non-finite values.
Results may differ from a plain program's by a relative error of at most 0.006.
Values may be sent and summed in bfloat16 or wider, within the bound.
No kernel may reach another device: no remote copies, remote signals or barrier semaphores. Data moves between devices by JAX's collectives and lax.ppermute only.
A program may use at most 128 MiB of HBM per device.

v0:
```python
import jax
import jax.numpy as jnp
from jax import lax
from jax.experimental import pallas as pl
from jax.experimental.pallas import tpu as pltpu
from jax.sharding import PartitionSpec as P


deep_alpha = 2.0**0.25
norm_epsilon = 1e-05
f32 = jnp.float32
bf16 = jnp.bfloat16
VMEM = pltpu.MemorySpace.VMEM
lanes = 128
gate_row = 8
sent_rows = 9


def iota(shape, dim):
    return lax.broadcasted_iota(jnp.int32, shape, dim)


def mm(a, b):
    return lax.dot_general(a, b, (((1,), (0,)), ((), ())), preferred_element_type=f32)


def mm_nt(a, b):
    return lax.dot_general(a, b, (((1,), (1,)), ((), ())), preferred_element_type=f32)


def mm_tn(a, b):
    return lax.dot_general(a, b, (((0,), (0,)), ((), ())), preferred_element_type=f32)


def split(value, pieces):
    found = []
    for _ in range(pieces - 1):
        high = value.astype(bf16)
        found.append(high)
        value = value - high.astype(f32)
    return found + [value.astype(bf16)]


def exact_left(table, value):
    total = None
    for piece in split(value, 3):
        part = mm(table, piece)
        total = part if total is None else total + part
    return total


def exact_right(value, table):
    total = None
    for piece in split(value, 3):
        part = mm(piece, table)
        total = part if total is None else total + part
    return total


def reversal(size):
    return (iota((size, size), 0) + iota((size, size), 1) == size - 1).astype(f32).astype(bf16)


def as_row(table, groups, states):
    wide = jnp.concatenate([table] * groups, axis=1)
    keep = iota(wide.shape, 0) == iota(wide.shape, 1) // states
    return jnp.sum(jnp.where(keep, wide, 0.0), axis=0, keepdims=True)


def block_diagonal(table, groups, states):
    each = table.shape[0] // groups
    wide = jnp.concatenate([table] * groups, axis=1)
    keep = iota(wide.shape, 0) // each == iota(wide.shape, 1) // states
    return jnp.where(keep, wide, 0.0)


def steps_of(rate, turn, groups, states):
    retain = jnp.exp(-rate)
    return (
        as_row(retain * jnp.cos(turn), groups, states),
        as_row(retain * jnp.sin(turn), groups, states),
    )


def cmul(a, b):
    return (a[0] * b[0] - a[1] * b[1], a[0] * b[1] + a[1] * b[0])


def local_kernel(
    x_ref, gate_ref, rate_ref, turn_ref, drive_re_ref, drive_im_ref,
    send_ref, state_re_ref, state_im_ref, wide_ref, step_ref,
):
    length = x_ref.shape[0]
    groups, states = rate_ref.shape[1:]
    width = groups * states
    tiles = width // lanes
    turned = reversal(length)
    x = x_ref[...]
    log_gate = gate_ref[...]
    spread = (iota((groups, width), 0) == iota((groups, width), 1) // states).astype(f32).astype(bf16)
    factors = split(jnp.exp(log_gate), 3)
    for k in range(2):
        rate = rate_ref[k]
        step_re, step_im = steps_of(rate, turn_ref[k], groups, states)
        scale = as_row(jnp.sqrt(1.0 - jnp.exp(-2.0 * rate)), groups, states)
        x_k = x if k == 0 else mm(turned, x).astype(bf16)
        x_two = jnp.concatenate([x_k, x_k], axis=1)
        gates = None
        for piece in factors:
            piece_k = piece if k == 0 else mm(piece, turned).astype(bf16)
            part = mm_tn(piece_k, spread)
            gates = part if gates is None else gates + part
        pushes = []
        for drive_ref in (drive_re_ref, drive_im_ref):
            table = block_diagonal(drive_ref[k], groups, states) * scale
            pushes.append(mm(x_two, jnp.concatenate(split(table, 2), axis=0)))
        for j in range(tiles):
            cols = slice(j * lanes, (j + 1) * lanes)
            rows = pl.ds(k * tiles + j, length, stride=2 * tiles)
            wide_ref[rows, :] = gates[:, cols]
            state_re_ref[rows, :] = pushes[0][:, cols]
            state_im_ref[rows, :] = pushes[1][:, cols]
            at = k * tiles + j
            step_ref[at : at + 1, :] = step_re[:, cols]
            step_ref[2 * tiles + at : 2 * tiles + at + 1, :] = step_im[:, cols]
    high = 2 * tiles
    w_re = step_ref[0:high, :]
    w_im = step_ref[high : 2 * high, :]

    def advance(t, carried):
        re, im = carried
        at = pl.ds(pl.multiple_of(t * high, high), high)
        factor = wide_ref[at, :]
        a_re, a_im = factor * w_re, factor * w_im
        new_re = (state_re_ref[at, :] + a_re * re) - a_im * im
        new_im = (state_im_ref[at, :] + a_re * im) + a_im * re
        state_re_ref[at, :] = new_re
        state_im_ref[at, :] = new_im
        return new_re, new_im

    zero = jnp.zeros((high, lanes), f32)
    re, im = lax.fori_loop(0, length, advance, (zero, zero), unroll=8)
    step_ref[0:high, :] = re
    step_ref[high : 2 * high, :] = im
    blocks = send_ref.shape[0] // sent_rows
    later = iota((blocks, lanes), 0) > lax.axis_index("sp")
    for part in range(2):
        for j in range(tiles):
            forward = step_ref[part * high + j : part * high + j + 1, :]
            backward = step_ref[part * high + tiles + j : part * high + tiles + j + 1, :]
            send_ref[pl.ds(part * tiles + j, blocks, stride=sent_rows), :] = jnp.where(
                later, forward, backward
            )
    total = jnp.sum(log_gate, axis=1, keepdims=True)
    thin = iota((groups, lanes), 0) == iota((groups, lanes), 1) // (lanes // groups)
    total_row = jnp.sum(jnp.where(thin, total, 0.0), axis=0, keepdims=True)
    send_ref[pl.ds(gate_row, blocks, stride=sent_rows), :] = jnp.broadcast_to(
        total_row, (blocks, lanes)
    )


def powers(step, length, backward):
    width = step[0].shape[1]
    exponent = iota((8, width), 0)
    exponent = 8 - exponent if backward else exponent + 1
    current = step
    rows = (jnp.ones((8, width), f32), jnp.zeros((8, width), f32))
    for bit in range(4):
        taken = (exponent >> bit) % 2 == 1
        more = cmul(rows, current)
        rows = tuple(jnp.where(taken, m, r) for m, r in zip(more, rows))
        if bit < 3:
            current = cmul(current, current)
    grown = {8: (rows, current)}
    size = 8
    while size * 2 <= length:
        rows, current = grown[size]
        more = cmul(rows, current)
        pair = (more, rows) if backward else (rows, more)
        rows = tuple(jnp.concatenate([a, b], axis=0) for a, b in zip(*pair))
        grown[size * 2] = (rows, cmul(current, current))
        size *= 2
    rows, current = grown[size]
    rest = length - size
    if rest:
        tail_rows, tail_power = grown[rest]
        more = cmul(tail_rows, current)
        pair = (more, rows) if backward else (rows, more)
        rows = tuple(jnp.concatenate([a, b], axis=0) for a, b in zip(*pair))
        current = cmul(current, tail_power)
    return rows, current


def powers_at(step, exponents, most):
    rows = (jnp.ones(exponents.shape, f32), jnp.zeros(exponents.shape, f32))
    bit = 0
    while (1 << bit) <= most:
        taken = (exponents >> bit) % 2 == 1
        more = cmul(rows, step)
        rows = tuple(jnp.where(taken, m, r) for m, r in zip(more, rows))
        step = cmul(step, step)
        bit += 1
    return rows


def beside_kernel(
    x_ref, gate_ref, rate_ref, turn_ref, read_re_ref, read_im_ref, skip_ref,
    state_re_ref, state_im_ref, routes_ref, group_ref, weight_ref,
    local_ref, run_ref, chain_ref, pick_ref, mix_ref,
):
    length = x_ref.shape[0]
    groups, states = rate_ref.shape[1:]
    width = groups * states
    tiles = width // lanes
    each = lanes // groups
    blocks = chain_ref.shape[1]
    here = lax.axis_index("sp")
    thin = (iota((groups, lanes), 0) == iota((groups, lanes), 1) // each).astype(f32).astype(bf16)
    log_gate = gate_ref[...]
    rows, cols = iota((length, length), 0), iota((length, length), 1)
    outs = []
    for k in range(2):
        total = None
        for part, state_ref in enumerate((state_re_ref, state_im_ref)):
            read_ref = (read_re_ref, read_im_ref)[part]
            table_high, table_low = split(block_diagonal(read_ref[k], groups, states), 2)
            for j in range(tiles):
                state = state_ref[pl.ds(k * tiles + j, length, stride=2 * tiles), :]
                state_high, state_low = split(state, 2)
                lane = slice(j * lanes, (j + 1) * lanes)
                value = (
                    mm_nt(state_high, table_high[:, lane])
                    + mm_nt(state_low, table_high[:, lane])
                    + mm_nt(state_high, table_low[:, lane])
                )
                if part:
                    value = -value
                total = value if total is None else total + value
        outs.append(total)
        seen = (rows <= cols) if k == 0 else (rows >= cols)
        run = jnp.exp(exact_right(log_gate, seen.astype(f32).astype(bf16)))
        spread = None
        for piece in split(run, 3):
            more = mm_tn(piece, thin)
            spread = more if spread is None else spread + more
        run_ref[k] = spread
        step = steps_of(rate_ref[k], turn_ref[k], groups, states)
        whole = powers_at(step, jnp.full((1, width), length, jnp.int32), length)
        source = iota((blocks, width), 0)
        gap = here - 1 - source if k == 0 else source - 1 - here
        chained = powers_at(whole, jnp.maximum(gap, 0), blocks - 1)
        for part in range(2):
            chain_ref[2 * k + part] = jnp.where(gap >= 0, chained[part], 0.0)
    local_ref[...] = (
        outs[0] + exact_left(reversal(length), outs[1]) + skip_ref[...] * x_ref[...].astype(f32)
    )
    slots, share = pick_ref.shape
    routes = routes_ref[...]
    weights = weight_ref[...]
    scaled = group_ref[...] * weights / (weights[0:1] + weights[1:2])
    place = iota((slots, length), 0)
    first = routes[0:1] == place // 2
    second = routes[1:2] == place // 2
    named = jnp.where(first | second, 1.0, 0.0)
    before = (rows < cols) & (rows // share == cols // share)
    prior = mm(named.astype(bf16), before.astype(f32).astype(bf16))
    picked = jnp.where(prior == (place % 2).astype(f32), named, 0.0)
    base = lax.axis_index("tp") * share
    own = (iota((length, share), 0) == base + iota((length, share), 1)).astype(f32).astype(bf16)
    pick_ref[...] = mm(picked.astype(bf16), own).astype(bf16)
    own = (iota((share, length), 1) == base + iota((share, length), 0)).astype(f32).astype(bf16)
    mixing = None
    for piece in split(picked * jnp.where(first, scaled[0:1], scaled[1:2]), 3):
        more = mm_nt(own, piece)
        mixing = more if mixing is None else mixing + more
    mix_ref[...] = mixing


def carry_kernel(
    come_ref, local_ref, run_ref, chain_ref, rate_ref, turn_ref, read_re_ref, read_im_ref,
    own_ref, next_ref, last_ref, far_ref, act_ref,
):
    here, member = lax.axis_index("sp"), lax.axis_index("tp")
    blocks, width = chain_ref.shape[1:]
    groups, states = rate_ref.shape[1:]
    tiles = width // lanes
    length = local_ref.shape[0]
    came = [
        jnp.concatenate(
            [come_ref[pl.ds(p * tiles + j, blocks, stride=sent_rows), :] for j in range(tiles)],
            axis=1,
        )
        for p in range(2)
    ]
    logs = come_ref[pl.ds(gate_row, blocks, stride=sent_rows), :]
    each = lanes // groups
    fan = (iota((lanes, width), 0) == each * (iota((lanes, width), 1) // states)).astype(f32)
    fan = fan.astype(bf16)
    source, mid = iota((blocks, blocks), 0), iota((blocks, blocks), 1)
    total = local_ref[...]
    for k in range(2):
        if k == 0:
            between = (mid > source) & (mid < here)
        else:
            between = (mid < source) & (mid > here)
        fade = jnp.exp(exact_left(between.astype(f32).astype(bf16), logs))
        fade = exact_right(fade, fan)
        chain = (chain_ref[2 * k] * fade, chain_ref[2 * k + 1] * fade)
        carry = [jnp.sum(v, axis=0, keepdims=True) for v in cmul(chain, came)]
        real = block_diagonal(read_re_ref[k], groups, states)
        imaginary = block_diagonal(read_im_ref[k], groups, states)
        step = steps_of(rate_ref[k], turn_ref[k], groups, states)
        grown, _ = powers(step, length, k == 1)
        first = carry[0] * real - carry[1] * imaginary
        second = -(carry[0] * imaginary + carry[1] * real)
        value = None
        for part, side in enumerate((first, second)):
            side_high, side_low = split(side, 2)
            high, low = split(grown[part], 2)
            more = mm_nt(high, side_high) + mm_nt(low, side_high) + mm_nt(high, side_low)
            value = more if value is None else value + more
        total = total + run_ref[k] * value
    act_ref[...] = jax.nn.gelu(total).astype(bf16)
    share = own_ref.shape[0]
    members = act_ref.shape[0] // share
    for shift, out_ref in enumerate((own_ref, next_ref, far_ref, last_ref)):
        at = lax.rem(member + shift, members) * share
        out_ref[...] = act_ref[pl.ds(pl.multiple_of(at, share), share), :]


def normed(values, gain):
    center = values - jnp.mean(values, axis=-1, keepdims=True)
    spread = jnp.mean(center * center, axis=-1, keepdims=True)
    return center * lax.rsqrt(spread + norm_epsilon) * gain


def to_lines(rows, rows_ref, out_ref):
    count, width = rows.shape
    each = width // lanes
    for q in range(each):
        rows_ref[pl.ds(q, count, stride=each), :] = rows[:, q * lanes : (q + 1) * lanes]
    out_ref[...] = rows_ref[...].astype(bf16)


def from_lines(lines_ref, rows_ref, each):
    count = lines_ref.shape[0] // each
    rows_ref[...] = lines_ref[...].astype(f32)
    return [rows_ref[pl.ds(q, count, stride=each), :].astype(bf16) for q in range(each)]


def branch_kernel(
    weight_hbm, residual_hbm, own_ref, from_last_ref, from_far_ref, from_next_ref, gain_ref,
    pick_ref, middle_ref, out_ref, rows_ref, weight_ref, residual_ref, sems,
):
    member = lax.axis_index("tp")
    channels = own_ref.shape[1]
    members = weight_ref.shape[0] // channels
    copies = []
    for shift in range(members):
        at = lax.rem(member + shift, members) * channels
        rows = pl.ds(pl.multiple_of(at, channels), channels)
        here = pl.ds(shift * channels, channels)
        copies.append(
            pltpu.make_async_copy(weight_hbm.at[rows, :], weight_ref.at[here, :], sems.at[shift])
        )
    copies.append(pltpu.make_async_copy(residual_hbm, residual_ref, sems.at[members]))
    for copy in copies:
        copy.start()
    branch = None
    for shift, part_ref in enumerate((own_ref, from_next_ref, from_far_ref, from_last_ref)):
        copies[shift].wait()
        more = mm(part_ref[...], weight_ref[shift * channels : (shift + 1) * channels, :])
        branch = more if branch is None else branch + more
    copies[members].wait()
    middle = normed(deep_alpha * residual_ref[...].astype(f32) + branch, gain_ref[...])
    middle_ref[...] = middle
    to_lines(mm(pick_ref[...], middle.astype(bf16)), rows_ref, out_ref)


def hidden_kernel(top_ref, low_ref, gate_ref, linear_ref, out_ref, rows_ref):
    each = gate_ref.shape[0] // lanes
    half = top_ref.shape[0] // each
    for at, ref in ((0, top_ref), (half, low_ref)):
        rows = jnp.concatenate(from_lines(ref, rows_ref, each), axis=1)
        gate = mm(rows, gate_ref[...])
        linear = mm(rows, linear_ref[...])
        out_ref[at : at + half, :] = (jax.nn.silu(gate) * linear).astype(bf16)


def down_kernel(own_ref, last_ref, next_ref, w_own_ref, w_last_ref, w_next_ref, out_ref):
    total = mm(own_ref[...], w_own_ref[...]).astype(bf16).astype(f32)
    total = total + mm(last_ref[...], w_last_ref[...]).astype(bf16).astype(f32)
    out_ref[...] = total + mm(next_ref[...], w_next_ref[...]).astype(bf16).astype(f32)


def answer_kernel(sum_ref, far_ref, w_far_top_ref, w_far_low_ref, out_ref, rows_ref):
    half = w_far_top_ref.shape[0]
    far = mm(far_ref[:, :half], w_far_top_ref[...]) + mm(far_ref[:, half:], w_far_low_ref[...])
    to_lines(sum_ref[...] + far.astype(bf16).astype(f32), rows_ref, out_ref)


def final_kernel(answers_ref, mix_ref, middle_ref, gain_ref, out_ref, rows_ref):
    each = middle_ref.shape[1] // lanes
    mixing = split(mix_ref[...], 3)
    routed = []
    for answers in from_lines(answers_ref, rows_ref, each):
        routed.append(mm(mixing[0], answers) + mm(mixing[1], answers) + mm(mixing[2], answers))
    routed = jnp.concatenate(routed, axis=1)
    out_ref[...] = normed(deep_alpha * middle_ref[...] + routed, gain_ref[...]).astype(bf16)


def shape(dims, dtype):
    return jax.ShapeDtypeStruct(dims, dtype)


def call(kernel, outs, scratch, cost, *args, room=16, kept=0):
    many = isinstance(outs, (list, tuple))
    whole = pl.BlockSpec(memory_space=VMEM)
    return pl.pallas_call(
        kernel,
        out_shape=outs,
        in_specs=[pl.BlockSpec(memory_space=pl.ANY)] * kept + [whole] * (len(args) - kept),
        out_specs=[whole] * len(outs) if many else whole,
        scratch_shapes=scratch,
        compiler_params=pltpu.CompilerParams(vmem_limit_bytes=room << 20),
        cost_estimate=pl.CostEstimate(flops=cost, bytes_accessed=1 << 20, transcendentals=0),
    )(*args)


def on_device(
    residual, mixer_input, log_gate, decay_rate, turn_rate, drive_real, drive_imaginary,
    read_real, read_imaginary, skip_gain, project_weight, norm_gain, final_gain, routes,
    group_weight, expert_weight, gate_weight, linear_weight, down_weight,
):
    length, channels = mixer_input.shape
    groups, states = decay_rate.shape[1:]
    width = groups * states
    share, model = residual.shape
    blocks = lax.axis_size("sp")
    members = lax.axis_size("tp")
    slots = 2 * blocks
    right = [(i, (i + 1) % members) for i in range(members)]
    left = [(i, (i - 1) % members) for i in range(members)]
    across = [(i, (i + 2) % members) for i in range(members)]

    def moved(array, way):
        return lax.ppermute(array, "tp", way)

    down = down_weight[0]
    half_down = down.shape[0] // 2
    down_last = moved(down, right)
    down_next = moved(down, left)

    flat = lambda table: table.reshape(2, -1, states)
    send, state_re, state_im = call(
        local_kernel,
        [
            shape((blocks * sent_rows, lanes), f32),
            shape((length * 2 * width // lanes, lanes), f32),
            shape((length * 2 * width // lanes, lanes), f32),
        ],
        [
            pltpu.VMEM((length * 2 * width // lanes, lanes), f32),
            pltpu.VMEM((4 * width // lanes, lanes), f32),
        ],
        1 << 30,
        mixer_input, log_gate.T, decay_rate, turn_rate, flat(drive_real), flat(drive_imaginary),
        room=60,
    )
    come = lax.all_to_all(
        send.reshape(blocks, 1, sent_rows * lanes), "sp", split_axis=0, concat_axis=0,
        tiled=True,
    ).reshape(blocks * sent_rows, lanes)
    local, run, chain, pick, mix = call(
        beside_kernel,
        [
            shape((length, lanes), f32),
            shape((2, length, lanes), f32),
            shape((4, blocks, width), f32),
            shape((slots, share), bf16),
            shape((share, slots), f32),
        ],
        [],
        1 << 30,
        mixer_input, log_gate.T, decay_rate, turn_rate, flat(read_real), flat(read_imaginary),
        skip_gain[None], state_re, state_im, routes.T, group_weight[None], expert_weight.T,
        room=60,
    )
    own, to_next, to_last, to_far = call(
        carry_kernel,
        [shape((share, channels), bf16)] * 4,
        [pltpu.VMEM((length, channels), bf16)],
        1 << 29,
        come, local, run, chain, decay_rate, turn_rate, flat(read_real), flat(read_imaginary),
        room=60,
    )
    from_last = moved(to_next, right)
    from_far = moved(to_far, across)
    from_next = moved(to_last, left)
    down_far_top = moved(down_last[:half_down], right)
    down_far_low = moved(down_next[half_down:], left)
    lines = slots * model // lanes
    middle, outgoing = call(
        branch_kernel,
        [shape((share, model), f32), shape((lines, lanes), bf16)],
        [
            pltpu.VMEM((lines, lanes), f32),
            pltpu.VMEM(project_weight.shape, bf16),
            pltpu.VMEM(residual.shape, bf16),
            pltpu.SemaphoreType.DMA((members + 1,)),
        ],
        1 << 29,
        project_weight, residual, own, from_last, from_far, from_next, norm_gain[None], pick,
        room=60, kept=2,
    )

    def exchanged(array):
        return lax.all_to_all(
            array.reshape(blocks, lines // blocks, lanes), "sp", split_axis=0, concat_axis=0,
            tiled=True,
        ).reshape(lines, lanes)

    landed = exchanged(outgoing)
    top, low = landed[: lines // 2], landed[lines // 2 :]
    last_top = moved(top, right)
    next_low = moved(low, left)
    last_low = moved(low, right)
    next_top = moved(top, left)
    far_top = moved(last_top, right)
    far_low = moved(next_low, left)

    def hidden_of(upper, lower):
        return call(
            hidden_kernel, shape((slots, gate_weight.shape[2]), bf16),
            [pltpu.VMEM((lines // 2, lanes), f32)], 1 << 29,
            upper, lower, gate_weight[0], linear_weight[0],
        )

    hidden_own = hidden_of(top, low)
    hidden_last = moved(hidden_of(last_top, last_low), left)
    hidden_next = moved(hidden_of(next_top, next_low), right)
    hidden_far = moved(hidden_of(far_top, far_low), across)
    summed = call(
        down_kernel, shape((slots, model), f32), [], 1 << 29,
        hidden_own, hidden_next, hidden_last, down, down_last, down_next,
    )
    answers = call(
        answer_kernel, shape((lines, lanes), bf16), [pltpu.VMEM((lines, lanes), f32)], 1 << 28,
        summed, hidden_far, down_far_top, down_far_low,
    )
    returned = exchanged(answers)
    return call(
        final_kernel, shape((share, model), bf16), [pltpu.VMEM((lines, lanes), f32)], 1 << 28,
        returned, mix, middle, final_gain[None],
    )


def solution(mesh):
    placed = (
        P(("sp", "tp"), None), P("sp", "tp"), P("sp", "tp"),
        P(None, "tp", None), P(None, "tp", None),
        P(None, "tp", None, None), P(None, "tp", None, None),
        P(None, "tp", None, None), P(None, "tp", None, None),
        P("tp"), P(), P(), P(),
        P("sp", None), P("sp"), P("sp", None),
        P("sp", None, "tp"), P("sp", None, "tp"), P("sp", "tp", None),
    )

    return jax.shard_map(
        on_device, mesh=mesh, in_specs=placed, out_specs=P(("sp", "tp"), None), check_vma=False
    )
```

profile of v0, /device:TPU:1, one launch (start us, length us, event | category | flops | bytes accessed | tf_op | source)
XLA Modules:
  0.0 145.9 jit_solution(8526508207065043705)
XLA Ops:
  0.0 4.2 %shard_map.181 = (f32[576,128]{1,0:T(8,128)}, f32[1536,128]{1,0:T(8,128)}, f32[1536,128]{1,0:T(8,128)}) custom-call(bf16[192,128]{1,0:T(8,128)(2,1)} %x_ref.3, f32[8,192]{1,0:T(8,128)} %bitcast.51, f32[2,8,64]{2,1,0:T(8,128)} %rate_ref.5, f32[2,8,64]{2,1,0:T(8,128)} %turn_ref.5, f32[2,128,64]{2,1,0:T(8,128)} %bitcast.45, f32[2,128,64]{2,1,0:T(8,128)} %bitcast.46), custom_call_target="tpu_custom_call" | custom-call | flops 1073741824 | bytes 1048576 | tf_op jit(solution)/shard_map/pallas_call | solution.py:419
  4.2 13.2 %all-to-all-start = ((f32[64,1,1152]{2,1,0:T(1,128)}), f32[64,1,1152]{2,1,0:T(1,128)S(1)}, u32[]{:S(2)}, u32[]{:S(2)}) async-start(f32[64,1,1152]{2,1,0:T(1,128)} %bitcast.43), calls=%async_computation | async-start | bytes 589824 | tf_op jit(solution)/shard_map/all_to_all | solution.py:470
  17.4 4.9 %shard_map.182 = (f32[192,128]{1,0:T(8,128)}, f32[2,192,128]{2,1,0:T(8,128)}, f32[4,64,512]{2,1,0:T(8,128)}, bf16[128,48]{1,0:T(8,128)(2,1)}, f32[48,128]{1,0:T(8,128)}) custom-call(bf16[192,128]{1,0:T(8,128)(2,1)} %x_ref.3, f32[8,192]{1,0:T(8,128)} %bitcast.52, f32[2,8,64]{2,1,0:T(8,128)} %rate_ref.5, f32[2,8,64]{2,1,0:T(8,128)} %turn_ref.5, ...), custom_call_target="tpu_custom_call" | custom-call | flops 1073741824 | bytes 1048576 | tf_op jit(solution)/shard_map/pallas_call | solution.py:419
  22.2 8.8 %all-to-all-done = f32[64,1,1152]{2,1,0:T(1,128)S(1)} async-done(((f32[64,1,1152]{2,1,0:T(1,128)}), f32[64,1,1152]{2,1,0:T(1,128)S(1)}, u32[]{:S(2)}, u32[]{:S(2)}) %all-to-all-start) | async-done | bytes 294944 | tf_op jit(solution)/shard_map/all_to_all | solution.py:470
  31.0 0.7 copy-done.6
  31.7 3.4 %shard_map.183 = (bf16[48,128]{1,0:T(8,128)(2,1)}, bf16[48,128]{1,0:T(8,128)(2,1)}, bf16[48,128]{1,0:T(8,128)(2,1)}, bf16[48,128]{1,0:T(8,128)(2,1)}) custom-call(f32[576,128]{1,0:T(8,128)} %bitcast.42, f32[192,128]{1,0:T(8,128)} %get-tuple-element.22.local_ref, f32[2,192,128]{2,1,0:T(8,128)} %get-tuple-element.23.run_ref, ...), custom_call_target="tpu_custom_call" | custom-call | flops 536870912 | bytes 1048576 | tf_op jit(solution)/shard_map/pallas_call | solution.py:419
  35.1 1.2 collective-permute-start
  36.3 2.4 %collective-permute-start.1 = (bf16[48,128]{1,0:T(8,128)(2,1)}, bf16[48,128]{1,0:T(8,128)(2,1)S(1)}, u32[]{:S(2)}, u32[]{:S(2)}) collective-permute-start(bf16[48,128]{1,0:T(8,128)(2,1)} %get-tuple-element.27), channel_id=1, source_target_pairs={{0,2},{1,3},{2,0},{3,1},{4,6},{5,7},{6,4},{7,5},{8,10},{9,11},{10,... | collective-permute-start | bytes 36872 | tf_op jit(solution)/shard_map/ppermute | solution.py:447
  38.8 1.1 collective-permute-start.2
  39.9 0.0 collective-permute-done.from_last_ref
  39.9 0.7 collective-permute-done.1.from_far_ref
  40.6 1.2 collective-permute-done.2.from_next_ref
  41.8 0.6 copy-done.9
  42.4 4.1 %shard_map.184 = (f32[48,2048]{1,0:T(8,128)}, bf16[2048,128]{1,0:T(8,128)(2,1)}) custom-call(bf16[512,2048]{1,0:T(8,128)(2,1)} %weight_hbm.1, bf16[48,2048]{1,0:T(8,128)(2,1)} %residual_hbm.1, bf16[48,128]{1,0:T(8,128)(2,1)} %get-tuple-element.25.own_ref, bf16[48,128]{1,0:T(8,128)(2,1)} %copy-done.7, bf16[48,128]{1,0:T(8,128)(2,1)} %copy-done.8, ...), custom_call_target="tpu_custom_call" | custom-call | flops 536870912 | bytes 1048576 | tf_op jit(solution)/shard_map/pallas_call | solution.py:419
  46.6 0.0 copy-start
  46.6 0.0 copy-start.1
  46.6 6.6 %all-to-all-start.1 = ((bf16[64,32,128]{2,1,0:T(8,128)(2,1)}), bf16[64,32,128]{2,1,0:T(8,128)(2,1)}, u32[]{:S(2)}, u32[]{:S(2)}) async-start(bf16[64,32,128]{2,1,0:T(8,128)(2,1)} %bitcast.41), calls=%async_computation.1 | async-start | bytes 1048576 | tf_op jit(solution)/shard_map/all_to_all | solution.py:518
  53.2 0.1 collective-permute-start.9
  53.3 2.7 %collective-permute-start.10 = (bf16[256,2048]{1,0:T(8,128)(2,1)}, bf16[256,2048]{1,0:T(8,128)(2,1)}, u32[]{:S(2)}, u32[]{:S(2)}) collective-permute-start(bf16[256,2048]{1,0:T(8,128)(2,1)} %bitcast.32), channel_id=1, source_target_pairs={{0,3},{1,0},{2,1},{3,2},{4,7},{5,4},{6,5},{7,6},{8,11},{9,8},{10,9... | collective-permute-start | bytes 3145736 | tf_op jit(solution)/shard_map/ppermute | solution.py:447
  56.0 14.9 %all-to-all-done.1 = bf16[64,32,128]{2,1,0:T(8,128)(2,1)} async-done(((bf16[64,32,128]{2,1,0:T(8,128)(2,1)}), bf16[64,32,128]{2,1,0:T(8,128)(2,1)}, u32[]{:S(2)}, u32[]{:S(2)}) %all-to-all-start.1) | async-done | bytes 524320 | tf_op jit(solution)/shard_map/all_to_all | solution.py:518
  70.9 1.1 fusion
  72.0 0.1 collective-permute-start.6
  72.1 2.7 %collective-permute-start.4 = (bf16[1024,128]{1,0:T(8,128)(2,1)S(1)}, bf16[1024,128]{1,0:T(8,128)(2,1)S(1)}, u32[]{:S(2)}, u32[]{:S(2)}) collective-permute-start(bf16[1024,128]{1,0:T(8,128)(2,1)S(1)} %bitcast.34), channel_id=1, source_target_pairs={{0,3},{1,0},{2,1},{3,2},{4,7},{5,4},{6,5},{7,6},{8,11},{9,8},{10,9... | collective-permute-start | bytes 786440 | tf_op jit(solution)/shard_map/ppermute | solution.py:447
  74.7 0.0 collective-permute-start.7
  74.7 4.1 %collective-permute-done.9.w_last_ref = bf16[256,2048]{1,0:T(8,128)(2,1)S(1)} collective-permute-done((bf16[256,2048]{1,0:T(8,128)(2,1)}, bf16[256,2048]{1,0:T(8,128)(2,1)S(1)}, u32[]{:S(2)}, u32[]{:S(2)}) %collective-permute-start.9) | collective-permute-done | bytes 1048608 | tf_op jit(solution)/shard_map/ppermute | solution.py:447
  78.9 0.1 collective-permute-start.14
  79.0 1.1 slice.27
  80.0 2.7 %collective-permute-start.15 = (bf16[128,2048]{1,0:T(8,128)(2,1)S(1)}, bf16[128,2048]{1,0:T(8,128)(2,1)S(1)}, u32[]{:S(2)}, u32[]{:S(2)}) collective-permute-start(bf16[128,2048]{1,0:T(8,128)(2,1)S(1)} %slice.27), channel_id=1, source_target_pairs={{0,3},{1,0},{2,1},{3,2},{4,7},{5,4},{6,5},{7,6},{8,11},{9,8},{10,9... | collective-permute-start | bytes 1572872 | tf_op jit(solution)/shard_map/ppermute | solution.py:447
  82.8 1.7 %collective-permute-done.6.top_ref = bf16[1024,128]{1,0:T(8,128)(2,1)S(1)} collective-permute-done((bf16[1024,128]{1,0:T(8,128)(2,1)S(1)}, bf16[1024,128]{1,0:T(8,128)(2,1)S(1)}, u32[]{:S(2)}, u32[]{:S(2)}) %collective-permute-start.6) | collective-permute-done | bytes 262176 | tf_op jit(solution)/shard_map/ppermute | solution.py:447
  84.4 1.1 collective-permute-start.3
  85.6 0.3 collective-permute-start.11
  85.9 4.1 %collective-permute-done.7.low_ref = bf16[1024,128]{1,0:T(8,128)(2,1)S(1)} collective-permute-done((bf16[1024,128]{1,0:T(8,128)(2,1)S(1)}, bf16[1024,128]{1,0:T(8,128)(2,1)S(1)}, u32[]{:S(2)}, u32[]{:S(2)}) %collective-permute-start.7) | collective-permute-done | bytes 262176 | tf_op jit(solution)/shard_map/ppermute | solution.py:447
  90.1 1.1 collective-permute-start.12
  91.2 0.8 shard_map.187
  92.0 7.9 %collective-permute-done.3.top_ref = bf16[1024,128]{1,0:T(8,128)(2,1)S(1)} collective-permute-done((bf16[1024,128]{1,0:T(8,128)(2,1)S(1)}, bf16[1024,128]{1,0:T(8,128)(2,1)S(1)}, u32[]{:S(2)}, u32[]{:S(2)}) %collective-permute-start.3) | collective-permute-done | bytes 262176 | tf_op jit(solution)/shard_map/ppermute | solution.py:447
  99.8 3.4 %collective-permute-start.8 = (bf16[128,256]{1,0:T(8,128)(2,1)S(1)}, bf16[128,256]{1,0:T(8,128)(2,1)S(1)}, u32[]{:S(2)}, u32[]{:S(2)}) collective-permute-start(bf16[128,256]{1,0:T(8,128)(2,1)S(1)} %shard_map.187), channel_id=1, source_target_pairs={{0,3},{1,0},{2,1},{3,2},{4,7},{5,4},{6,5},{7,6},{8,11},{9,8},{10,9... | collective-permute-start | bytes 196616 | tf_op jit(solution)/shard_map/ppermute | solution.py:447
  103.2 0.8 shard_map.186
  104.0 0.0 copy-start.2
  104.0 2.9 %collective-permute-done.11.top_ref = bf16[1024,128]{1,0:T(8,128)(2,1)S(1)} collective-permute-done((bf16[1024,128]{1,0:T(8,128)(2,1)S(1)}, bf16[1024,128]{1,0:T(8,128)(2,1)S(1)}, u32[]{:S(2)}, u32[]{:S(2)}) %collective-permute-start.11) | collective-permute-done | bytes 262176 | tf_op jit(solution)/shard_map/ppermute | solution.py:447
  106.9 0.8 shard_map.189
  107.7 2.4 %collective-permute-start.13 = (bf16[128,256]{1,0:T(8,128)(2,1)S(1)}, bf16[128,256]{1,0:T(8,128)(2,1)S(1)}, u32[]{:S(2)}, u32[]{:S(2)}) collective-permute-start(bf16[128,256]{1,0:T(8,128)(2,1)S(1)} %shard_map.189), channel_id=1, source_target_pairs={{0,2},{1,3},{2,0},{3,1},{4,6},{5,7},{6,4},{7,5},{8,10},{9,11},{10,... | collective-permute-start | bytes 196616 | tf_op jit(solution)/shard_map/ppermute | solution.py:447
  110.1 0.8 shard_map.185.own_ref
  110.9 0.4 collective-permute-done.5.last_ref
  111.2 1.9 %shard_map.188.sum_ref = f32[128,2048]{1,0:T(8,128)S(1)} custom-call(bf16[128,256]{1,0:T(8,128)(2,1)S(1)} %shard_map.185.own_ref, bf16[128,256]{1,0:T(8,128)(2,1)S(1)} %collective-permute-done.5.last_ref, bf16[128,256]{1,0:T(8,128)(2,1)S(1)} %collective-permute-done.8.next_ref, bf16[256,2048]{1,0:T(8,128)(2,1)S(1)} %bitcast.33, ...), custom_call_target="tpu_custom_call" | custom-call | flops 536870912 | bytes 1048576 | tf_op jit(solution)/shard_map/pallas_call | solution.py:419
  113.1 0.0 copy-start.5
  113.2 0.7 shard_map.190
  113.9 30.4 %all_to_all.15 = bf16[64,32,128]{2,1,0:T(8,128)(2,1)S(1)} all-to-all(bf16[64,32,128]{2,1,0:T(8,128)(2,1)S(1)} %bitcast.30), channel_id=1, replica_groups=mesh['sp'=64,'tp'=4] {'sp'}, dimensions={0} | all-to-all | bytes 1048576 | tf_op jit(solution)/shard_map/all_to_all | solution.py:518
  144.3 1.6 %shard_map.191 = bf16[48,2048]{1,0:T(8,128)(2,1)} custom-call(bf16[2048,128]{1,0:T(8,128)(2,1)S(1)} %bitcast.29, f32[48,128]{1,0:T(8,128)S(1)} %copy-done.4, f32[48,2048]{1,0:T(8,128)S(1)} %copy-done.3, f32[1,2048]{1,0:T(1,128)S(1)} %bitcast.40), custom_call_target="tpu_custom_call" | custom-call | flops 268435456 | bytes 1048576 | tf_op jit(solution)/shard_map/pallas_call | solution.py:419
  (23 shorter events, 0.1 us)
Async XLA Ops:
  4.2 26.8 %all-to-all-start = ((f32[64,1,1152]{2,1,0:T(1,128)}), f32[64,1,1152]{2,1,0:T(1,128)S(1)}, u32[]{:S(2)}, u32[]{:S(2)}) async-start(f32[64,1,1152]{2,1,0:T(1,128)} %bitcast.43), calls=%async_computation | async-start | bytes 589824 | tf_op jit(solution)/shard_map/all_to_all | solution.py:470
  31.0 0.7 copy-start.6
  35.1 4.8 %collective-permute-start = (bf16[48,128]{1,0:T(8,128)(2,1)}, bf16[48,128]{1,0:T(8,128)(2,1)S(1)}, u32[]{:S(2)}, u32[]{:S(2)}) collective-permute-start(bf16[48,128]{1,0:T(8,128)(2,1)} %get-tuple-element.26), channel_id=1, source_target_pairs={{0,1},{1,2},{2,3},{3,0},{4,5},{5,6},{6,7},{7,4},{8,9},{9,10},{10,1... | collective-permute-start | bytes 36872 | tf_op jit(solution)/shard_map/ppermute | solution.py:447
  36.3 4.3 %collective-permute-start.1 = (bf16[48,128]{1,0:T(8,128)(2,1)}, bf16[48,128]{1,0:T(8,128)(2,1)S(1)}, u32[]{:S(2)}, u32[]{:S(2)}) collective-permute-start(bf16[48,128]{1,0:T(8,128)(2,1)} %get-tuple-element.27), channel_id=1, source_target_pairs={{0,2},{1,3},{2,0},{3,1},{4,6},{5,7},{6,4},{7,5},{8,10},{9,11},{10,... | collective-permute-start | bytes 36872 | tf_op jit(solution)/shard_map/ppermute | solution.py:447
  38.8 3.0 %collective-permute-start.2 = (bf16[48,128]{1,0:T(8,128)(2,1)}, bf16[48,128]{1,0:T(8,128)(2,1)S(1)}, u32[]{:S(2)}, u32[]{:S(2)}) collective-permute-start(bf16[48,128]{1,0:T(8,128)(2,1)} %get-tuple-element.28), channel_id=1, source_target_pairs={{0,3},{1,0},{2,1},{3,2},{4,7},{5,4},{6,5},{7,6},{8,11},{9,8},{10,9... | collective-permute-start | bytes 36872 | tf_op jit(solution)/shard_map/ppermute | solution.py:447
  39.9 1.9 %copy-start.7 = (bf16[48,128]{1,0:T(8,128)(2,1)}, bf16[48,128]{1,0:T(8,128)(2,1)S(1)}, u32[]{:S(2)}) copy-start(bf16[48,128]{1,0:T(8,128)(2,1)S(1)} %collective-permute-done.from_last_ref) | copy-start | bytes 36868
  40.6 1.2 copy-start.8
  41.8 0.6 copy-start.9
  46.6 44.6 %copy-start = (bf16[1,2048,256]{2,1,0:T(8,128)(2,1)S(1)}, bf16[1,2048,256]{2,1,0:T(8,128)(2,1)}, u32[]{:S(2)}) copy-start(bf16[1,2048,256]{2,1,0:T(8,128)(2,1)} %param.35) | copy-start | bytes 3145732
  46.6 44.6 %copy-start.1 = (bf16[1,2048,256]{2,1,0:T(8,128)(2,1)S(1)}, bf16[1,2048,256]{2,1,0:T(8,128)(2,1)}, u32[]{:S(2)}) copy-start(bf16[1,2048,256]{2,1,0:T(8,128)(2,1)} %param.36) | copy-start | bytes 3145732
  46.6 24.3 %all-to-all-start.1 = ((bf16[64,32,128]{2,1,0:T(8,128)(2,1)}), bf16[64,32,128]{2,1,0:T(8,128)(2,1)}, u32[]{:S(2)}, u32[]{:S(2)}) async-start(bf16[64,32,128]{2,1,0:T(8,128)(2,1)} %bitcast.41), calls=%async_computation.1 | async-start | bytes 1048576 | tf_op jit(solution)/shard_map/all_to_all | solution.py:518
  53.2 25.6 %collective-permute-start.9 = (bf16[256,2048]{1,0:T(8,128)(2,1)}, bf16[256,2048]{1,0:T(8,128)(2,1)S(1)}, u32[]{:S(2)}, u32[]{:S(2)}) collective-permute-start(bf16[256,2048]{1,0:T(8,128)(2,1)} %bitcast.31), channel_id=1, source_target_pairs={{0,1},{1,2},{2,3},{3,0},{4,5},{5,6},{6,7},{7,4},{8,9},{9,10},{10,1... | collective-permute-start | bytes 3145736 | tf_op jit(solution)/shard_map/ppermute | solution.py:447
  53.3 25.6 %collective-permute-start.10 = (bf16[256,2048]{1,0:T(8,128)(2,1)}, bf16[256,2048]{1,0:T(8,128)(2,1)}, u32[]{:S(2)}, u32[]{:S(2)}) collective-permute-start(bf16[256,2048]{1,0:T(8,128)(2,1)} %bitcast.32), channel_id=1, source_target_pairs={{0,3},{1,0},{2,1},{3,2},{4,7},{5,4},{6,5},{7,6},{8,11},{9,8},{10,9... | collective-permute-start | bytes 3145736 | tf_op jit(solution)/shard_map/ppermute | solution.py:447
  72.0 12.5 %collective-permute-start.6 = (bf16[1024,128]{1,0:T(8,128)(2,1)S(1)}, bf16[1024,128]{1,0:T(8,128)(2,1)S(1)}, u32[]{:S(2)}, u32[]{:S(2)}) collective-permute-start(bf16[1024,128]{1,0:T(8,128)(2,1)S(1)} %bitcast.37), channel_id=1, source_target_pairs={{0,1},{1,2},{2,3},{3,0},{4,5},{5,6},{6,7},{7,4},{8,9},{9,10},{10,1... | collective-permute-start | bytes 786440 | tf_op jit(solution)/shard_map/ppermute | solution.py:447
  72.1 13.5 %collective-permute-start.4 = (bf16[1024,128]{1,0:T(8,128)(2,1)S(1)}, bf16[1024,128]{1,0:T(8,128)(2,1)S(1)}, u32[]{:S(2)}, u32[]{:S(2)}) collective-permute-start(bf16[1024,128]{1,0:T(8,128)(2,1)S(1)} %bitcast.34), channel_id=1, source_target_pairs={{0,3},{1,0},{2,1},{3,2},{4,7},{5,4},{6,5},{7,6},{8,11},{9,8},{10,9... | collective-permute-start | bytes 786440 | tf_op jit(solution)/shard_map/ppermute | solution.py:447
  74.7 15.3 %collective-permute-start.7 = (bf16[1024,128]{1,0:T(8,128)(2,1)S(1)}, bf16[1024,128]{1,0:T(8,128)(2,1)S(1)}, u32[]{:S(2)}, u32[]{:S(2)}) collective-permute-start(bf16[1024,128]{1,0:T(8,128)(2,1)S(1)} %bitcast.35), channel_id=1, source_target_pairs={{0,1},{1,2},{2,3},{3,0},{4,5},{5,6},{6,7},{7,4},{8,9},{9,10},{10,1... | collective-permute-start | bytes 786440 | tf_op jit(solution)/shard_map/ppermute | solution.py:447
  78.9 34.3 %collective-permute-start.14 = (bf16[128,2048]{1,0:T(8,128)(2,1)S(1)}, bf16[128,2048]{1,0:T(8,128)(2,1)S(1)}, u32[]{:S(2)}, u32[]{:S(2)}) collective-permute-start(bf16[128,2048]{1,0:T(8,128)(2,1)S(1)} %slice.26), channel_id=1, source_target_pairs={{0,1},{1,2},{2,3},{3,0},{4,5},{5,6},{6,7},{7,4},{8,9},{9,10},{10,1... | collective-permute-start | bytes 1572872 | tf_op jit(solution)/shard_map/ppermute | solution.py:447
  80.0 33.1 %collective-permute-start.15 = (bf16[128,2048]{1,0:T(8,128)(2,1)S(1)}, bf16[128,2048]{1,0:T(8,128)(2,1)S(1)}, u32[]{:S(2)}, u32[]{:S(2)}) collective-permute-start(bf16[128,2048]{1,0:T(8,128)(2,1)S(1)} %slice.27), channel_id=1, source_target_pairs={{0,3},{1,0},{2,1},{3,2},{4,7},{5,4},{6,5},{7,6},{8,11},{9,8},{10,9... | collective-permute-start | bytes 1572872 | tf_op jit(solution)/shard_map/ppermute | solution.py:447
  84.4 15.4 %collective-permute-start.3 = (bf16[1024,128]{1,0:T(8,128)(2,1)S(1)}, bf16[1024,128]{1,0:T(8,128)(2,1)S(1)}, u32[]{:S(2)}, u32[]{:S(2)}) collective-permute-start(bf16[1024,128]{1,0:T(8,128)(2,1)S(1)} %bitcast.38), channel_id=1, source_target_pairs={{0,3},{1,0},{2,1},{3,2},{4,7},{5,4},{6,5},{7,6},{8,11},{9,8},{10,9... | collective-permute-start | bytes 786440 | tf_op jit(solution)/shard_map/ppermute | solution.py:447
  85.6 21.3 %collective-permute-start.11 = (bf16[1024,128]{1,0:T(8,128)(2,1)S(1)}, bf16[1024,128]{1,0:T(8,128)(2,1)S(1)}, u32[]{:S(2)}, u32[]{:S(2)}) collective-permute-start(bf16[1024,128]{1,0:T(8,128)(2,1)S(1)} %collective-permute-done.6.top_ref), channel_id=1, source_target_pairs={{0,1},{1,2},{2,3},{3,0},{4,5},{5,6},{6,7},{7,4},{8,9},{9,10},{10,1... | collective-permute-start | bytes 786440 | tf_op jit(solution)/shard_map/ppermute | solution.py:447
  90.1 16.9 %collective-permute-start.12 = (bf16[1024,128]{1,0:T(8,128)(2,1)S(1)}, bf16[1024,128]{1,0:T(8,128)(2,1)S(1)}, u32[]{:S(2)}, u32[]{:S(2)}) collective-permute-start(bf16[1024,128]{1,0:T(8,128)(2,1)S(1)} %collective-permute-done.4.low_ref), channel_id=1, source_target_pairs={{0,3},{1,0},{2,1},{3,2},{4,7},{5,4},{6,5},{7,6},{8,11},{9,8},{10,9... | collective-permute-start | bytes 786440 | tf_op jit(solution)/shard_map/ppermute | solution.py:447
  99.8 11.0 %collective-permute-start.8 = (bf16[128,256]{1,0:T(8,128)(2,1)S(1)}, bf16[128,256]{1,0:T(8,128)(2,1)S(1)}, u32[]{:S(2)}, u32[]{:S(2)}) collective-permute-start(bf16[128,256]{1,0:T(8,128)(2,1)S(1)} %shard_map.187), channel_id=1, source_target_pairs={{0,3},{1,0},{2,1},{3,2},{4,7},{5,4},{6,5},{7,6},{8,11},{9,8},{10,9... | collective-permute-start | bytes 196616 | tf_op jit(solution)/shard_map/ppermute | solution.py:447
  104.0 7.2 %copy-start.2 = (bf16[1,256,2048]{2,1,0:T(8,128)(2,1)S(1)}, bf16[1,256,2048]{2,1,0:T(8,128)(2,1)}, u32[]{:S(2)}) copy-start(bf16[1,256,2048]{2,1,0:T(8,128)(2,1)} %param.37) | copy-start | bytes 3145732
  106.9 4.3 %collective-permute-start.5 = (bf16[128,256]{1,0:T(8,128)(2,1)S(1)}, bf16[128,256]{1,0:T(8,128)(2,1)S(1)}, u32[]{:S(2)}, u32[]{:S(2)}) collective-permute-start(bf16[128,256]{1,0:T(8,128)(2,1)S(1)} %shard_map.186), channel_id=1, source_target_pairs={{0,1},{1,2},{2,3},{3,0},{4,5},{5,6},{6,7},{7,4},{8,9},{9,10},{10,1... | collective-permute-start | bytes 196616 | tf_op jit(solution)/shard_map/ppermute | solution.py:447
  107.7 5.5 %collective-permute-start.13 = (bf16[128,256]{1,0:T(8,128)(2,1)S(1)}, bf16[128,256]{1,0:T(8,128)(2,1)S(1)}, u32[]{:S(2)}, u32[]{:S(2)}) collective-permute-start(bf16[128,256]{1,0:T(8,128)(2,1)S(1)} %shard_map.189), channel_id=1, source_target_pairs={{0,2},{1,3},{2,0},{3,1},{4,6},{5,7},{6,4},{7,5},{8,10},{9,11},{10,... | collective-permute-start | bytes 196616 | tf_op jit(solution)/shard_map/ppermute | solution.py:447
  113.1 31.2 %copy-start.3 = (f32[48,2048]{1,0:T(8,128)S(1)}, f32[48,2048]{1,0:T(8,128)}, u32[]{:S(2)}) copy-start(f32[48,2048]{1,0:T(8,128)} %get-tuple-element.32.middle_ref) | copy-start | bytes 1179652
  113.1 31.2 %copy-start.4 = (f32[48,128]{1,0:T(8,128)S(1)}, f32[48,128]{1,0:T(8,128)}, u32[]{:S(2)}) copy-start(f32[48,128]{1,0:T(8,128)} %get-tuple-element.31.mix_ref) | copy-start | bytes 73732
  113.1 31.2 %copy-start.5 = (f32[2048]{0:T(1024)S(1)}, f32[2048]{0:T(1024)}, u32[]{:S(2)}) copy-start(f32[2048]{0:T(1024)} %param.31) | copy-start | bytes 24580
where the time goes:
time: 146 us
  waiting for transfers between devices  46.7 us (32%)
  starting transfers between devices  41.3 us (28%)
  blocking collectives  30.4 us (21%)
  Pallas kernels  23.7 us (16%)
  local copies, waits for them, and re-layouts  3.51 us (2%)
    all_to_all x1, blocking collectives, exchanged(): lax.all_to_all(array.reshape(blocks, lines // blocks, lanes), 'sp', split...  30.4 us
    pallas_call x11, Pallas kernels, call(): pl.pallas_call(kernel, out_shape=outs, in_specs=[pl.BlockSpec(memory_spac...  23.7 us
    ppermute x16, waiting for transfers between devices, moved(): return lax.ppermute(array, 'tp', way)  22.9 us
    ppermute x16, starting transfers between devices, moved(): return lax.ppermute(array, 'tp', way)  21.5 us
    all_to_all x1, waiting for transfers between devices, exchanged(): lax.all_to_all(array.reshape(blocks, lines // blocks, lanes), 'sp', split...  14.9 us
    all_to_all x1, starting transfers between devices, on_device(): lax.all_to_all(send.reshape(blocks, 1, sent_rows * lanes), 'sp', split_ax...  13.2 us
    all_to_all x1, waiting for transfers between devices, on_device(): lax.all_to_all(send.reshape(blocks, 1, sent_rows * lanes), 'sp', split_ax...  8.82 us
    all_to_all x1, starting transfers between devices, exchanged(): lax.all_to_all(array.reshape(blocks, lines // blocks, lanes), 'sp', split...  6.62 us
  transfers between devices with their start and end apart: 18, of which 10 were waited for; matrix products, arithmetic and copies ran while one was open for 1% of the time, Pallas kernels for 7%

commit v1 on v0

--- a/solution.py
+++ b/solution.py
@@ -204,21 +204,18 @@
 
 
 def beside_kernel(
-    x_ref, gate_ref, rate_ref, turn_ref, read_re_ref, read_im_ref, skip_ref,
+    x_ref, rate_ref, turn_ref, read_re_ref, read_im_ref, skip_ref,
     state_re_ref, state_im_ref, routes_ref, group_ref, weight_ref,
-    local_ref, run_ref, chain_ref, pick_ref, mix_ref,
+    local_ref, chain_ref, pick_ref, mix_ref,
 ):
     length = x_ref.shape[0]
     groups, states = rate_ref.shape[1:]
     width = groups * states
     tiles = width // lanes
-    each = lanes // groups
     blocks = chain_ref.shape[1]
     here = lax.axis_index("sp")
-    thin = (iota((groups, lanes), 0) == iota((groups, lanes), 1) // each).astype(f32).astype(bf16)
-    log_gate = gate_ref[...]
     rows, cols = iota((length, length), 0), iota((length, length), 1)
-    outs = []
+    outs, wholes = [], []
     for k in range(2):
         total = None
         for part, state_ref in enumerate((state_re_ref, state_im_ref)):
@@ -237,20 +234,16 @@
                     value = -value
                 total = value if total is None else total + value
         outs.append(total)
-        seen = (rows <= cols) if k == 0 else (rows >= cols)
-        run = jnp.exp(exact_right(log_gate, seen.astype(f32).astype(bf16)))
-        spread = None
-        for piece in split(run, 3):
-            more = mm_tn(piece, thin)
-            spread = more if spread is None else spread + more
-        run_ref[k] = spread
         step = steps_of(rate_ref[k], turn_ref[k], groups, states)
         whole = powers_at(step, jnp.full((1, width), length, jnp.int32), length)
-        source = iota((blocks, width), 0)
-        gap = here - 1 - source if k == 0 else source - 1 - here
-        chained = powers_at(whole, jnp.maximum(gap, 0), blocks - 1)
-        for part in range(2):
-            chain_ref[2 * k + part] = jnp.where(gap >= 0, chained[part], 0.0)
+        wholes.append(whole)
+    source = iota((blocks, width), 0)
+    earlier = source < here
+    gap = jnp.where(earlier, here - 1 - source, source - 1 - here)
+    whole = tuple(jnp.where(earlier, a, b) for a, b in zip(*wholes))
+    chained = powers_at(whole, jnp.maximum(gap, 0), blocks - 1)
+    for part in range(2):
+        chain_ref[part] = jnp.where(gap >= 0, chained[part], 0.0)
     local_ref[...] = (
         outs[0] + exact_left(reversal(length), outs[1]) + skip_ref[...] * x_ref[...].astype(f32)
     )
@@ -277,7 +270,7 @@
 
 
 def carry_kernel(
-    come_ref, local_ref, run_ref, chain_ref, rate_ref, turn_ref, read_re_ref, read_im_ref,
+    come_ref, local_ref, gate_ref, chain_ref, rate_ref, turn_ref, read_re_ref, read_im_ref,
     own_ref, next_ref, last_ref, far_ref, act_ref,
 ):
     here, member = lax.axis_index("sp"), lax.axis_index("tp")
@@ -296,17 +289,18 @@
     each = lanes // groups
     fan = (iota((lanes, width), 0) == each * (iota((lanes, width), 1) // states)).astype(f32)
     fan = fan.astype(bf16)
+    thin = (iota((groups, lanes), 0) == iota((groups, lanes), 1) // each).astype(f32).astype(bf16)
     source, mid = iota((blocks, blocks), 0), iota((blocks, blocks), 1)
+    rows, cols = iota((length, length), 0), iota((length, length), 1)
+    between = ((mid > source) & (mid < here)) | ((mid < source) & (mid > here))
+    between = jnp.where(between & (source != here), 1.0, 0.0).astype(bf16)
+    fade = exact_right(jnp.exp(exact_left(between, logs)), fan)
+    gathered = cmul((chain_ref[0] * fade, chain_ref[1] * fade), came)
+    earlier = iota((blocks, width), 0) < here
     total = local_ref[...]
     for k in range(2):
-        if k == 0:
-            between = (mid > source) & (mid < here)
-        else:
-            between = (mid < source) & (mid > here)
-        fade = jnp.exp(exact_left(between.astype(f32).astype(bf16), logs))
-        fade = exact_right(fade, fan)
-        chain = (chain_ref[2 * k] * fade, chain_ref[2 * k + 1] * fade)
-        carry = [jnp.sum(v, axis=0, keepdims=True) for v in cmul(chain, came)]
+        taken = earlier if k == 0 else ~earlier
+        carry = [jnp.sum(jnp.where(taken, v, 0.0), axis=0, keepdims=True) for v in gathered]
         real = block_diagonal(read_re_ref[k], groups, states)
         imaginary = block_diagonal(read_im_ref[k], groups, states)
         step = steps_of(rate_ref[k], turn_ref[k], groups, states)
@@ -319,7 +313,13 @@
             high, low = split(grown[part], 2)
             more = mm_nt(high, side_high) + mm_nt(low, side_high) + mm_nt(high, side_low)
             value = more if value is None else value + more
-        total = total + run_ref[k] * value
+        seen = (rows <= cols) if k == 0 else (rows >= cols)
+        fade = jnp.exp(exact_right(gate_ref[...], seen.astype(f32).astype(bf16)))
+        run = None
+        for piece in split(fade, 3):
+            more = mm_tn(piece, thin)
+            run = more if run is None else run + more
+        total = total + run * value
     act_ref[...] = jax.nn.gelu(total).astype(bf16)
     share = own_ref.shape[0]
     members = act_ref.shape[0] // share
@@ -349,29 +349,17 @@
 
 
 def branch_kernel(
-    weight_hbm, residual_hbm, own_ref, from_last_ref, from_far_ref, from_next_ref, gain_ref,
-    pick_ref, middle_ref, out_ref, rows_ref, weight_ref, residual_ref, sems,
+    own_ref, from_last_ref, from_far_ref, from_next_ref, weight_ref, residual_ref, gain_ref,
+    pick_ref, middle_ref, out_ref, rows_ref,
 ):
     member = lax.axis_index("tp")
     channels = own_ref.shape[1]
     members = weight_ref.shape[0] // channels
-    copies = []
-    for shift in range(members):
-        at = lax.rem(member + shift, members) * channels
-        rows = pl.ds(pl.multiple_of(at, channels), channels)
-        here = pl.ds(shift * channels, channels)
-        copies.append(
-            pltpu.make_async_copy(weight_hbm.at[rows, :], weight_ref.at[here, :], sems.at[shift])
-        )
-    copies.append(pltpu.make_async_copy(residual_hbm, residual_ref, sems.at[members]))
-    for copy in copies:
-        copy.start()
     branch = None
     for shift, part_ref in enumerate((own_ref, from_next_ref, from_far_ref, from_last_ref)):
-        copies[shift].wait()
-        more = mm(part_ref[...], weight_ref[shift * channels : (shift + 1) * channels, :])
+        at = lax.rem(member + shift, members) * channels
+        more = mm(part_ref[...], weight_ref[pl.ds(pl.multiple_of(at, channels), channels), :])
         branch = more if branch is None else branch + more
-    copies[members].wait()
     middle = normed(deep_alpha * residual_ref[...].astype(f32) + branch, gain_ref[...])
     middle_ref[...] = middle
     to_lines(mm(pick_ref[...], middle.astype(bf16)), rows_ref, out_ref)
@@ -471,31 +459,30 @@
         send.reshape(blocks, 1, sent_rows * lanes), "sp", split_axis=0, concat_axis=0,
         tiled=True,
     ).reshape(blocks * sent_rows, lanes)
-    local, run, chain, pick, mix = call(
+    local, chain, pick, mix = call(
         beside_kernel,
         [
             shape((length, lanes), f32),
-            shape((2, length, lanes), f32),
-            shape((4, blocks, width), f32),
+            shape((2, blocks, width), f32),
             shape((slots, share), bf16),
             shape((share, slots), f32),
         ],
         [],
         1 << 30,
-        mixer_input, log_gate.T, decay_rate, turn_rate, flat(read_real), flat(read_imaginary),
+        mixer_input, decay_rate, turn_rate, flat(read_real), flat(read_imaginary),
         skip_gain[None], state_re, state_im, routes.T, group_weight[None], expert_weight.T,
-        room=60,
+        room=40,
     )
     own, to_next, to_last, to_far = call(
         carry_kernel,
         [shape((share, channels), bf16)] * 4,
         [pltpu.VMEM((length, channels), bf16)],
         1 << 29,
-        come, local, run, chain, decay_rate, turn_rate, flat(read_real), flat(read_imaginary),
-        room=60,
-    )
+        come, local, log_gate.T, chain, decay_rate, turn_rate, flat(read_real), flat(read_imaginary),
+        room=40,
+    )
+    from_far = moved(to_far, across)
     from_last = moved(to_next, right)
-    from_far = moved(to_far, across)
     from_next = moved(to_last, left)
     down_far_top = moved(down_last[:half_down], right)
     down_far_low = moved(down_next[half_down:], left)
@@ -503,15 +490,9 @@
     middle, outgoing = call(
         branch_kernel,
         [shape((share, model), f32), shape((lines, lanes), bf16)],
-        [
-            pltpu.VMEM((lines, lanes), f32),
-            pltpu.VMEM(project_weight.shape, bf16),
-            pltpu.VMEM(residual.shape, bf16),
-            pltpu.SemaphoreType.DMA((members + 1,)),
-        ],
+        [pltpu.VMEM((lines, lanes), f32)],
         1 << 29,
-        project_weight, residual, own, from_last, from_far, from_next, norm_gain[None], pick,
-        room=60, kept=2,
+        own, from_last, from_far, from_next, project_weight, residual, norm_gain[None], pick,
     )
 
     def exchanged(array):

time: 146 us -> 141 us (0.966)
  Pallas kernels: 23.7 us -> 17.1 us
  local copies, waits for them, and re-layouts: 3.51 us -> 5.12 us
    pallas_call x11, Pallas kernels: 23.7 us -> 17.1 us  [call(): pl.pallas_call(kernel, out_shape=outs, in_specs=[pl.BlockSpec(memory_spac...]
    unnamed x20 -> x42, local copies, waits for them, and re-layouts: 1.33 us -> 2.94 us
  transfers between devices with their start and end apart: 18 -> 18, of which waited for: 10 -> 10; matrix products, arithmetic and copies ran while one was open for 1% -> 2% of each run, Pallas kernels for 7% -> 5%
where the time goes in v1:
time: 141 us
  waiting for transfers between devices  46.1 us (33%)
  starting transfers between devices  41.4 us (29%)
  blocking collectives  30.5 us (22%)
  Pallas kernels  17.1 us (12%)
  local copies, waits for them, and re-layouts  5.12 us (4%)
    all_to_all x1, blocking collectives, exchanged(): lax.all_to_all(array.reshape(blocks, lines // blocks, lanes), 'sp', split...  30.5 us
    ppermute x16, waiting for transfers between devices, moved(): return lax.ppermute(array, 'tp', way)  22.6 us
    ppermute x16, starting transfers between devices, moved(): return lax.ppermute(array, 'tp', way)  21.7 us
    pallas_call x11, Pallas kernels, call(): pl.pallas_call(kernel, out_shape=outs, in_specs=[pl.BlockSpec(memory_spac...  17.1 us
    all_to_all x1, waiting for transfers between devices, exchanged(): lax.all_to_all(array.reshape(blocks, lines // blocks, lanes), 'sp', split...  15 us
    all_to_all x1, starting transfers between devices, on_device(): lax.all_to_all(send.reshape(blocks, 1, sent_rows * lanes), 'sp', split_ax...  13.2 us
    all_to_all x1, waiting for transfers between devices, on_device(): lax.all_to_all(send.reshape(blocks, 1, sent_rows * lanes), 'sp', split_ax...  8.6 us
    all_to_all x1, starting transfers between devices, exchanged(): lax.all_to_all(array.reshape(blocks, lines // blocks, lanes), 'sp', split...  6.61 us
  transfers between devices with their start and end apart: 18, of which 10 were waited for; matrix products, arithmetic and copies ran while one was open for 2% of the time, Pallas kernels for 5%

profile of v1, /device:TPU:1, one launch (start us, length us, event | category | flops | bytes accessed | tf_op | source)
XLA Modules:
  0.0 140.7 jit_solution(3174672171263638306)
XLA Ops:
  0.1 4.3 %shard_map.181 = (f32[576,128]{1,0:T(8,128)}, f32[1536,128]{1,0:T(8,128)}, f32[1536,128]{1,0:T(8,128)}) custom-call(bf16[192,128]{1,0:T(8,128)(2,1)} %x_ref.3, f32[8,192]{1,0:T(8,128)} %bitcast.47, f32[2,8,64]{2,1,0:T(8,128)} %rate_ref.5, f32[2,8,64]{2,1,0:T(8,128)} %turn_ref.5, f32[2,128,64]{2,1,0:T(8,128)} %bitcast.54, f32[2,128,64]{2,1,0:T(8,128)} %bitcast.55), custom_call_target="tpu_custom_call" | custom-call | flops 1073741824 | bytes 1048576 | tf_op jit(solution)/shard_map/pallas_call | solution.py:407
  4.4 13.2 %all-to-all-start = ((f32[64,1,1152]{2,1,0:T(1,128)}), f32[64,1,1152]{2,1,0:T(1,128)S(1)}, u32[]{:S(2)}, u32[]{:S(2)}) async-start(f32[64,1,1152]{2,1,0:T(1,128)} %bitcast.53), calls=%async_computation | async-start | bytes 589824 | tf_op jit(solution)/shard_map/all_to_all | solution.py:458
  17.5 0.0 copy-start.12
  17.7 1.1 copy-done.19
  18.8 1.1 copy-done.20
  19.9 2.1 %shard_map.182 = (f32[192,128]{1,0:T(8,128)S(1)}, f32[2,64,512]{2,1,0:T(8,128)S(1)}, bf16[128,48]{1,0:T(8,128)(2,1)S(1)}, f32[48,128]{1,0:T(8,128)S(1)}) custom-call(bf16[192,128]{1,0:T(8,128)(2,1)S(1)} %copy-done.11, f32[2,8,64]{2,1,0:T(8,128)S(1)} %copy-done.13, f32[2,8,64]{2,1,0:T(8,128)S(1)} %copy-done.14, f32[2,128,64]{2,1,0:T(8,128)S(1)} %bitcast.43, ...), custom_call_target="tpu_custom_call" | custom-call | flops 1073741824 | bytes 1048576 | tf_op jit(solution)/shard_map/pallas_call | solution.py:407
  22.0 0.0 copy-start.5
  22.0 0.6 copy-done.5
  22.6 8.6 %all-to-all-done = f32[64,1,1152]{2,1,0:T(1,128)S(1)} async-done(((f32[64,1,1152]{2,1,0:T(1,128)}), f32[64,1,1152]{2,1,0:T(1,128)S(1)}, u32[]{:S(2)}, u32[]{:S(2)}) %all-to-all-start) | async-done | bytes 294944 | tf_op jit(solution)/shard_map/all_to_all | solution.py:458
  31.2 1.7 %shard_map.183 = (bf16[48,128]{1,0:T(8,128)(2,1)S(1)}, bf16[48,128]{1,0:T(8,128)(2,1)S(1)}, bf16[48,128]{1,0:T(8,128)(2,1)S(1)}, bf16[48,128]{1,0:T(8,128)(2,1)S(1)}) custom-call(f32[576,128]{1,0:T(8,128)S(1)} %bitcast.40, f32[192,128]{1,0:T(8,128)S(1)} %get-tuple-element.21.local_ref, f32[8,192]{1,0:T(8,128)S(1)} %bitcast.48, ...), custom_call_target="tpu_custom_call" | custom-call | flops 536870912 | bytes 1048576 | tf_op jit(solution)/shard_map/pallas_call | solution.py:407
  32.9 1.3 collective-permute-start
  34.2 2.4 %collective-permute-start.1 = (bf16[48,128]{1,0:T(8,128)(2,1)S(1)}, bf16[48,128]{1,0:T(8,128)(2,1)S(1)}, u32[]{:S(2)}, u32[]{:S(2)}) collective-permute-start(bf16[48,128]{1,0:T(8,128)(2,1)S(1)} %get-tuple-element.25), channel_id=1, source_target_pairs={{0,2},{1,3},{2,0},{3,1},{4,6},{5,7},{6,4},{7,5},{8,10},{9,11},{10,... | collective-permute-start | bytes 36872 | tf_op jit(solution)/shard_map/ppermute | solution.py:435
  36.6 1.2 collective-permute-start.2
  37.8 0.5 collective-permute-done.1.from_far_ref
  38.2 1.2 collective-permute-done.2.from_next_ref
  39.5 1.9 %shard_map.184 = (f32[48,2048]{1,0:T(8,128)S(1)}, bf16[2048,128]{1,0:T(8,128)(2,1)}) custom-call(bf16[48,128]{1,0:T(8,128)(2,1)S(1)} %get-tuple-element.23.own_ref, bf16[48,128]{1,0:T(8,128)(2,1)S(1)} %collective-permute-done.from_last_ref, bf16[48,128]{1,0:T(8,128)(2,1)S(1)} %collective-permute-done.1.from_far_ref, ...), custom_call_target="tpu_custom_call" | custom-call | flops 536870912 | bytes 1048576 | tf_op jit(solution)/shard_map/pallas_call | solution.py:407
  41.4 6.6 %all-to-all-start.1 = ((bf16[64,32,128]{2,1,0:T(8,128)(2,1)}), bf16[64,32,128]{2,1,0:T(8,128)(2,1)}, u32[]{:S(2)}, u32[]{:S(2)}) async-start(bf16[64,32,128]{2,1,0:T(8,128)(2,1)} %bitcast.12), calls=%async_computation.1 | async-start | bytes 1048576 | tf_op jit(solution)/shard_map/all_to_all | solution.py:499
  48.0 0.1 collective-permute-start.9
  48.1 2.7 %collective-permute-start.10 = (bf16[256,2048]{1,0:T(8,128)(2,1)}, bf16[256,2048]{1,0:T(8,128)(2,1)}, u32[]{:S(2)}, u32[]{:S(2)}) collective-permute-start(bf16[256,2048]{1,0:T(8,128)(2,1)} %bitcast.32), channel_id=1, source_target_pairs={{0,3},{1,0},{2,1},{3,2},{4,7},{5,4},{6,5},{7,6},{8,11},{9,8},{10,9... | collective-permute-start | bytes 3145736 | tf_op jit(solution)/shard_map/ppermute | solution.py:435
  50.8 15.0 %all-to-all-done.1 = bf16[64,32,128]{2,1,0:T(8,128)(2,1)} async-done(((bf16[64,32,128]{2,1,0:T(8,128)(2,1)}), bf16[64,32,128]{2,1,0:T(8,128)(2,1)}, u32[]{:S(2)}, u32[]{:S(2)}) %all-to-all-start.1) | async-done | bytes 524320 | tf_op jit(solution)/shard_map/all_to_all | solution.py:499
  65.7 1.1 fusion
  66.8 0.1 collective-permute-start.6
  66.9 2.7 %collective-permute-start.4 = (bf16[1024,128]{1,0:T(8,128)(2,1)S(1)}, bf16[1024,128]{1,0:T(8,128)(2,1)S(1)}, u32[]{:S(2)}, u32[]{:S(2)}) collective-permute-start(bf16[1024,128]{1,0:T(8,128)(2,1)S(1)} %bitcast.34), channel_id=1, source_target_pairs={{0,3},{1,0},{2,1},{3,2},{4,7},{5,4},{6,5},{7,6},{8,11},{9,8},{10,9... | collective-permute-start | bytes 786440 | tf_op jit(solution)/shard_map/ppermute | solution.py:435
  69.5 4.0 %collective-permute-done.9.w_last_ref = bf16[256,2048]{1,0:T(8,128)(2,1)S(1)} collective-permute-done((bf16[256,2048]{1,0:T(8,128)(2,1)}, bf16[256,2048]{1,0:T(8,128)(2,1)S(1)}, u32[]{:S(2)}, u32[]{:S(2)}) %collective-permute-start.9) | collective-permute-done | bytes 1048608 | tf_op jit(solution)/shard_map/ppermute | solution.py:435
  73.6 0.1 collective-permute-start.14
  73.7 1.1 slice.27
  74.8 2.7 %collective-permute-start.15 = (bf16[128,2048]{1,0:T(8,128)(2,1)S(1)}, bf16[128,2048]{1,0:T(8,128)(2,1)S(1)}, u32[]{:S(2)}, u32[]{:S(2)}) collective-permute-start(bf16[128,2048]{1,0:T(8,128)(2,1)S(1)} %slice.27), channel_id=1, source_target_pairs={{0,3},{1,0},{2,1},{3,2},{4,7},{5,4},{6,5},{7,6},{8,11},{9,8},{10,9... | collective-permute-start | bytes 1572872 | tf_op jit(solution)/shard_map/ppermute | solution.py:435
  77.5 1.7 %collective-permute-done.6.top_ref = bf16[1024,128]{1,0:T(8,128)(2,1)S(1)} collective-permute-done((bf16[1024,128]{1,0:T(8,128)(2,1)S(1)}, bf16[1024,128]{1,0:T(8,128)(2,1)S(1)}, u32[]{:S(2)}, u32[]{:S(2)}) %collective-permute-start.6) | collective-permute-done | bytes 262176 | tf_op jit(solution)/shard_map/ppermute | solution.py:435
  79.2 1.2 collective-permute-start.3
  80.4 0.3 collective-permute-start.11
  80.7 4.1 %collective-permute-done.7.low_ref = bf16[1024,128]{1,0:T(8,128)(2,1)S(1)} collective-permute-done((bf16[1024,128]{1,0:T(8,128)(2,1)S(1)}, bf16[1024,128]{1,0:T(8,128)(2,1)S(1)}, u32[]{:S(2)}, u32[]{:S(2)}) %collective-permute-start.7) | collective-permute-done | bytes 262176 | tf_op jit(solution)/shard_map/ppermute | solution.py:435
  84.8 1.2 collective-permute-start.12
  86.0 0.8 shard_map.187
  86.8 7.8 %collective-permute-done.3.top_ref = bf16[1024,128]{1,0:T(8,128)(2,1)S(1)} collective-permute-done((bf16[1024,128]{1,0:T(8,128)(2,1)S(1)}, bf16[1024,128]{1,0:T(8,128)(2,1)S(1)}, u32[]{:S(2)}, u32[]{:S(2)}) %collective-permute-start.3) | collective-permute-done | bytes 262176 | tf_op jit(solution)/shard_map/ppermute | solution.py:435
  94.6 3.4 %collective-permute-start.8 = (bf16[128,256]{1,0:T(8,128)(2,1)S(1)}, bf16[128,256]{1,0:T(8,128)(2,1)S(1)}, u32[]{:S(2)}, u32[]{:S(2)}) collective-permute-start(bf16[128,256]{1,0:T(8,128)(2,1)S(1)} %shard_map.187), channel_id=1, source_target_pairs={{0,3},{1,0},{2,1},{3,2},{4,7},{5,4},{6,5},{7,6},{8,11},{9,8},{10,9... | collective-permute-start | bytes 196616 | tf_op jit(solution)/shard_map/ppermute | solution.py:435
  98.0 0.8 shard_map.186
  98.8 0.0 copy-start.3
  98.8 2.9 %collective-permute-done.11.top_ref = bf16[1024,128]{1,0:T(8,128)(2,1)S(1)} collective-permute-done((bf16[1024,128]{1,0:T(8,128)(2,1)S(1)}, bf16[1024,128]{1,0:T(8,128)(2,1)S(1)}, u32[]{:S(2)}, u32[]{:S(2)}) %collective-permute-start.11) | collective-permute-done | bytes 262176 | tf_op jit(solution)/shard_map/ppermute | solution.py:435
  101.7 0.8 shard_map.189
  102.4 2.4 %collective-permute-start.13 = (bf16[128,256]{1,0:T(8,128)(2,1)S(1)}, bf16[128,256]{1,0:T(8,128)(2,1)S(1)}, u32[]{:S(2)}, u32[]{:S(2)}) collective-permute-start(bf16[128,256]{1,0:T(8,128)(2,1)S(1)} %shard_map.189), channel_id=1, source_target_pairs={{0,2},{1,3},{2,0},{3,1},{4,6},{5,7},{6,4},{7,5},{8,10},{9,11},{10,... | collective-permute-start | bytes 196616 | tf_op jit(solution)/shard_map/ppermute | solution.py:435
  104.9 0.8 shard_map.185.own_ref
  105.7 0.3 collective-permute-done.5.last_ref
  106.0 1.9 %shard_map.188.sum_ref = f32[128,2048]{1,0:T(8,128)S(1)} custom-call(bf16[128,256]{1,0:T(8,128)(2,1)S(1)} %shard_map.185.own_ref, bf16[128,256]{1,0:T(8,128)(2,1)S(1)} %collective-permute-done.5.last_ref, bf16[128,256]{1,0:T(8,128)(2,1)S(1)} %collective-permute-done.8.next_ref, bf16[256,2048]{1,0:T(8,128)(2,1)S(1)} %bitcast.33, ...), custom_call_target="tpu_custom_call" | custom-call | flops 536870912 | bytes 1048576 | tf_op jit(solution)/shard_map/pallas_call | solution.py:407
  107.9 0.0 copy-start.6
  107.9 0.0 copy-start.8
  107.9 0.7 shard_map.190
  108.6 30.5 %all_to_all.15 = bf16[64,32,128]{2,1,0:T(8,128)(2,1)S(1)} all-to-all(bf16[64,32,128]{2,1,0:T(8,128)(2,1)S(1)} %bitcast.30), channel_id=1, replica_groups=mesh['sp'=64,'tp'=4] {'sp'}, dimensions={0} | all-to-all | bytes 1048576 | tf_op jit(solution)/shard_map/all_to_all | solution.py:499
  139.1 1.6 %shard_map.191 = bf16[48,2048]{1,0:T(8,128)(2,1)} custom-call(bf16[2048,128]{1,0:T(8,128)(2,1)S(1)} %bitcast.29, f32[48,128]{1,0:T(8,128)S(1)} %copy-done.6, f32[48,2048]{1,0:T(8,128)S(1)} %get-tuple-element.30.middle_ref, f32[1,2048]{1,0:T(1,128)S(1)} %bitcast.42), custom_call_target="tpu_custom_call" | custom-call | flops 268435456 | bytes 1048576 | tf_op jit(solution)/shard_map/pallas_call | solution.py:407
  (45 shorter events, 0.1 us)
Async XLA Ops:
  0.0 17.6 %copy-start.9 = (f32[2,8,16,64]{3,2,1,0:T(8,128)S(1)}, f32[2,8,16,64]{3,2,1,0:T(8,128)}, u32[]{:S(2)}) copy-start(f32[2,8,16,64]{3,2,1,0:T(8,128)} %param.26) | copy-start | bytes 196612
  0.0 17.6 %copy-start.10 = (f32[2,8,16,64]{3,2,1,0:T(8,128)S(1)}, f32[2,8,16,64]{3,2,1,0:T(8,128)}, u32[]{:S(2)}) copy-start(f32[2,8,16,64]{3,2,1,0:T(8,128)} %param.27) | copy-start | bytes 196612
  0.0 17.6 %copy-start.11 = (bf16[192,128]{1,0:T(8,128)(2,1)S(1)}, bf16[192,128]{1,0:T(8,128)(2,1)}, u32[]{:S(2)}) copy-start(bf16[192,128]{1,0:T(8,128)(2,1)} %x_ref.3) | copy-start | bytes 147460
  0.0 17.6 %copy-start.13 = (f32[2,8,64]{2,1,0:T(8,128)S(1)}, f32[2,8,64]{2,1,0:T(8,128)}, u32[]{:S(2)}) copy-start(f32[2,8,64]{2,1,0:T(8,128)} %rate_ref.5) | copy-start | bytes 12292
  0.0 17.6 %copy-start.14 = (f32[2,8,64]{2,1,0:T(8,128)S(1)}, f32[2,8,64]{2,1,0:T(8,128)}, u32[]{:S(2)}) copy-start(f32[2,8,64]{2,1,0:T(8,128)} %turn_ref.5) | copy-start | bytes 12292
  0.0 17.6 %copy-start.15 = (s32[192,2]{0,1:T(2,128)S(1)}, s32[192,2]{0,1:T(2,128)}, u32[]{:S(2)}) copy-start(s32[192,2]{0,1:T(2,128)} %param.32) | copy-start | bytes 4612
  0.0 17.6 %copy-start.16 = (f32[192,2]{0,1:T(2,128)S(1)}, f32[192,2]{0,1:T(2,128)}, u32[]{:S(2)}) copy-start(f32[192,2]{0,1:T(2,128)} %param.34) | copy-start | bytes 4612
  0.0 17.6 %copy-start.17 = (f32[192]{0:T(256)S(1)}, f32[192]{0:T(256)}, u32[]{:S(2)}) copy-start(f32[192]{0:T(256)} %param.33) | copy-start | bytes 2308
  0.1 17.6 %copy-start.18 = (f32[128]{0:T(128)S(1)}, f32[128]{0:T(128)}, u32[]{:S(2)}) copy-start(f32[128]{0:T(128)} %param.28) | copy-start | bytes 1540
  4.4 26.8 %all-to-all-start = ((f32[64,1,1152]{2,1,0:T(1,128)}), f32[64,1,1152]{2,1,0:T(1,128)S(1)}, u32[]{:S(2)}, u32[]{:S(2)}) async-start(f32[64,1,1152]{2,1,0:T(1,128)} %bitcast.53), calls=%async_computation | async-start | bytes 589824 | tf_op jit(solution)/shard_map/all_to_all | solution.py:458
  17.5 13.7 %copy-start.12 = (f32[192,8]{0,1:T(8,128)S(1)}, f32[192,8]{0,1:T(8,128)}, u32[]{:S(2)}) copy-start(f32[192,8]{0,1:T(8,128)} %param.21) | copy-start | bytes 18436
  17.6 1.1 copy-start.19
  18.8 1.1 copy-start.20
  19.9 19.5 %copy-start.2 = (bf16[512,2048]{1,0:T(8,128)(2,1)S(1)}, bf16[512,2048]{1,0:T(8,128)(2,1)}, u32[]{:S(2)}) copy-start(bf16[512,2048]{1,0:T(8,128)(2,1)} %weight_ref.1) | copy-start | bytes 6291460
  19.9 19.5 %copy-start.4 = (bf16[48,2048]{1,0:T(8,128)(2,1)S(1)}, bf16[48,2048]{1,0:T(8,128)(2,1)}, u32[]{:S(2)}) copy-start(bf16[48,2048]{1,0:T(8,128)(2,1)} %residual_ref.1) | copy-start | bytes 589828
  19.9 19.5 %copy-start.7 = (f32[2048]{0:T(1024)S(1)}, f32[2048]{0:T(1024)}, u32[]{:S(2)}) copy-start(f32[2048]{0:T(1024)} %param.30) | copy-start | bytes 24580
  22.0 0.6 copy-start.5
  32.9 4.9 %collective-permute-start = (bf16[48,128]{1,0:T(8,128)(2,1)S(1)}, bf16[48,128]{1,0:T(8,128)(2,1)S(1)}, u32[]{:S(2)}, u32[]{:S(2)}) collective-permute-start(bf16[48,128]{1,0:T(8,128)(2,1)S(1)} %get-tuple-element.24), channel_id=1, source_target_pairs={{0,1},{1,2},{2,3},{3,0},{4,5},{5,6},{6,7},{7,4},{8,9},{9,10},{10,1... | collective-permute-start | bytes 36872 | tf_op jit(solution)/shard_map/ppermute | solution.py:435
  34.2 4.1 %collective-permute-start.1 = (bf16[48,128]{1,0:T(8,128)(2,1)S(1)}, bf16[48,128]{1,0:T(8,128)(2,1)S(1)}, u32[]{:S(2)}, u32[]{:S(2)}) collective-permute-start(bf16[48,128]{1,0:T(8,128)(2,1)S(1)} %get-tuple-element.25), channel_id=1, source_target_pairs={{0,2},{1,3},{2,0},{3,1},{4,6},{5,7},{6,4},{7,5},{8,10},{9,11},{10,... | collective-permute-start | bytes 36872 | tf_op jit(solution)/shard_map/ppermute | solution.py:435
  36.6 2.8 %collective-permute-start.2 = (bf16[48,128]{1,0:T(8,128)(2,1)S(1)}, bf16[48,128]{1,0:T(8,128)(2,1)S(1)}, u32[]{:S(2)}, u32[]{:S(2)}) collective-permute-start(bf16[48,128]{1,0:T(8,128)(2,1)S(1)} %get-tuple-element.26), channel_id=1, source_target_pairs={{0,3},{1,0},{2,1},{3,2},{4,7},{5,4},{6,5},{7,6},{8,11},{9,8},{10,9... | collective-permute-start | bytes 36872 | tf_op jit(solution)/shard_map/ppermute | solution.py:435
  41.4 44.6 %copy-start = (bf16[1,2048,256]{2,1,0:T(8,128)(2,1)S(1)}, bf16[1,2048,256]{2,1,0:T(8,128)(2,1)}, u32[]{:S(2)}) copy-start(bf16[1,2048,256]{2,1,0:T(8,128)(2,1)} %param.35) | copy-start | bytes 3145732
  41.4 44.6 %copy-start.1 = (bf16[1,2048,256]{2,1,0:T(8,128)(2,1)S(1)}, bf16[1,2048,256]{2,1,0:T(8,128)(2,1)}, u32[]{:S(2)}) copy-start(bf16[1,2048,256]{2,1,0:T(8,128)(2,1)} %param.36) | copy-start | bytes 3145732
  41.4 24.3 %all-to-all-start.1 = ((bf16[64,32,128]{2,1,0:T(8,128)(2,1)}), bf16[64,32,128]{2,1,0:T(8,128)(2,1)}, u32[]{:S(2)}, u32[]{:S(2)}) async-start(bf16[64,32,128]{2,1,0:T(8,128)(2,1)} %bitcast.12), calls=%async_computation.1 | async-start | bytes 1048576 | tf_op jit(solution)/shard_map/all_to_all | solution.py:499
  48.0 25.6 %collective-permute-start.9 = (bf16[256,2048]{1,0:T(8,128)(2,1)}, bf16[256,2048]{1,0:T(8,128)(2,1)S(1)}, u32[]{:S(2)}, u32[]{:S(2)}) collective-permute-start(bf16[256,2048]{1,0:T(8,128)(2,1)} %bitcast.31), channel_id=1, source_target_pairs={{0,1},{1,2},{2,3},{3,0},{4,5},{5,6},{6,7},{7,4},{8,9},{9,10},{10,1... | collective-permute-start | bytes 3145736 | tf_op jit(solution)/shard_map/ppermute | solution.py:435
  48.1 25.6 %collective-permute-start.10 = (bf16[256,2048]{1,0:T(8,128)(2,1)}, bf16[256,2048]{1,0:T(8,128)(2,1)}, u32[]{:S(2)}, u32[]{:S(2)}) collective-permute-start(bf16[256,2048]{1,0:T(8,128)(2,1)} %bitcast.32), channel_id=1, source_target_pairs={{0,3},{1,0},{2,1},{3,2},{4,7},{5,4},{6,5},{7,6},{8,11},{9,8},{10,9... | collective-permute-start | bytes 3145736 | tf_op jit(solution)/shard_map/ppermute | solution.py:435
  66.8 12.4 %collective-permute-start.6 = (bf16[1024,128]{1,0:T(8,128)(2,1)S(1)}, bf16[1024,128]{1,0:T(8,128)(2,1)S(1)}, u32[]{:S(2)}, u32[]{:S(2)}) collective-permute-start(bf16[1024,128]{1,0:T(8,128)(2,1)S(1)} %bitcast.37), channel_id=1, source_target_pairs={{0,1},{1,2},{2,3},{3,0},{4,5},{5,6},{6,7},{7,4},{8,9},{9,10},{10,1... | collective-permute-start | bytes 786440 | tf_op jit(solution)/shard_map/ppermute | solution.py:435
  66.9 13.5 %collective-permute-start.4 = (bf16[1024,128]{1,0:T(8,128)(2,1)S(1)}, bf16[1024,128]{1,0:T(8,128)(2,1)S(1)}, u32[]{:S(2)}, u32[]{:S(2)}) collective-permute-start(bf16[1024,128]{1,0:T(8,128)(2,1)S(1)} %bitcast.34), channel_id=1, source_target_pairs={{0,3},{1,0},{2,1},{3,2},{4,7},{5,4},{6,5},{7,6},{8,11},{9,8},{10,9... | collective-permute-start | bytes 786440 | tf_op jit(solution)/shard_map/ppermute | solution.py:435
  69.5 15.3 %collective-permute-start.7 = (bf16[1024,128]{1,0:T(8,128)(2,1)S(1)}, bf16[1024,128]{1,0:T(8,128)(2,1)S(1)}, u32[]{:S(2)}, u32[]{:S(2)}) collective-permute-start(bf16[1024,128]{1,0:T(8,128)(2,1)S(1)} %bitcast.35), channel_id=1, source_target_pairs={{0,1},{1,2},{2,3},{3,0},{4,5},{5,6},{6,7},{7,4},{8,9},{9,10},{10,1... | collective-permute-start | bytes 786440 | tf_op jit(solution)/shard_map/ppermute | solution.py:435
  73.6 34.3 %collective-permute-start.14 = (bf16[128,2048]{1,0:T(8,128)(2,1)S(1)}, bf16[128,2048]{1,0:T(8,128)(2,1)S(1)}, u32[]{:S(2)}, u32[]{:S(2)}) collective-permute-start(bf16[128,2048]{1,0:T(8,128)(2,1)S(1)} %slice.26), channel_id=1, source_target_pairs={{0,1},{1,2},{2,3},{3,0},{4,5},{5,6},{6,7},{7,4},{8,9},{9,10},{10,1... | collective-permute-start | bytes 1572872 | tf_op jit(solution)/shard_map/ppermute | solution.py:435
  74.8 33.1 %collective-permute-start.15 = (bf16[128,2048]{1,0:T(8,128)(2,1)S(1)}, bf16[128,2048]{1,0:T(8,128)(2,1)S(1)}, u32[]{:S(2)}, u32[]{:S(2)}) collective-permute-start(bf16[128,2048]{1,0:T(8,128)(2,1)S(1)} %slice.27), channel_id=1, source_target_pairs={{0,3},{1,0},{2,1},{3,2},{4,7},{5,4},{6,5},{7,6},{8,11},{9,8},{10,9... | collective-permute-start | bytes 1572872 | tf_op jit(solution)/shard_map/ppermute | solution.py:435
  79.2 15.4 %collective-permute-start.3 = (bf16[1024,128]{1,0:T(8,128)(2,1)S(1)}, bf16[1024,128]{1,0:T(8,128)(2,1)S(1)}, u32[]{:S(2)}, u32[]{:S(2)}) collective-permute-start(bf16[1024,128]{1,0:T(8,128)(2,1)S(1)} %bitcast.38), channel_id=1, source_target_pairs={{0,3},{1,0},{2,1},{3,2},{4,7},{5,4},{6,5},{7,6},{8,11},{9,8},{10,9... | collective-permute-start | bytes 786440 | tf_op jit(solution)/shard_map/ppermute | solution.py:435
  80.4 21.3 %collective-permute-start.11 = (bf16[1024,128]{1,0:T(8,128)(2,1)S(1)}, bf16[1024,128]{1,0:T(8,128)(2,1)S(1)}, u32[]{:S(2)}, u32[]{:S(2)}) collective-permute-start(bf16[1024,128]{1,0:T(8,128)(2,1)S(1)} %collective-permute-done.6.top_ref), channel_id=1, source_target_pairs={{0,1},{1,2},{2,3},{3,0},{4,5},{5,6},{6,7},{7,4},{8,9},{9,10},{10,1... | collective-permute-start | bytes 786440 | tf_op jit(solution)/shard_map/ppermute | solution.py:435
  84.8 16.9 %collective-permute-start.12 = (bf16[1024,128]{1,0:T(8,128)(2,1)S(1)}, bf16[1024,128]{1,0:T(8,128)(2,1)S(1)}, u32[]{:S(2)}, u32[]{:S(2)}) collective-permute-start(bf16[1024,128]{1,0:T(8,128)(2,1)S(1)} %collective-permute-done.4.low_ref), channel_id=1, source_target_pairs={{0,3},{1,0},{2,1},{3,2},{4,7},{5,4},{6,5},{7,6},{8,11},{9,8},{10,9... | collective-permute-start | bytes 786440 | tf_op jit(solution)/shard_map/ppermute | solution.py:435
  94.6 11.0 %collective-permute-start.8 = (bf16[128,256]{1,0:T(8,128)(2,1)S(1)}, bf16[128,256]{1,0:T(8,128)(2,1)S(1)}, u32[]{:S(2)}, u32[]{:S(2)}) collective-permute-start(bf16[128,256]{1,0:T(8,128)(2,1)S(1)} %shard_map.187), channel_id=1, source_target_pairs={{0,3},{1,0},{2,1},{3,2},{4,7},{5,4},{6,5},{7,6},{8,11},{9,8},{10,9... | collective-permute-start | bytes 196616 | tf_op jit(solution)/shard_map/ppermute | solution.py:435
  98.8 7.2 %copy-start.3 = (bf16[1,256,2048]{2,1,0:T(8,128)(2,1)S(1)}, bf16[1,256,2048]{2,1,0:T(8,128)(2,1)}, u32[]{:S(2)}) copy-start(bf16[1,256,2048]{2,1,0:T(8,128)(2,1)} %param.37) | copy-start | bytes 3145732
  101.7 4.3 %collective-permute-start.5 = (bf16[128,256]{1,0:T(8,128)(2,1)S(1)}, bf16[128,256]{1,0:T(8,128)(2,1)S(1)}, u32[]{:S(2)}, u32[]{:S(2)}) collective-permute-start(bf16[128,256]{1,0:T(8,128)(2,1)S(1)} %shard_map.186), channel_id=1, source_target_pairs={{0,1},{1,2},{2,3},{3,0},{4,5},{5,6},{6,7},{7,4},{8,9},{9,10},{10,1... | collective-permute-start | bytes 196616 | tf_op jit(solution)/shard_map/ppermute | solution.py:435
  102.4 5.5 %collective-permute-start.13 = (bf16[128,256]{1,0:T(8,128)(2,1)S(1)}, bf16[128,256]{1,0:T(8,128)(2,1)S(1)}, u32[]{:S(2)}, u32[]{:S(2)}) collective-permute-start(bf16[128,256]{1,0:T(8,128)(2,1)S(1)} %shard_map.189), channel_id=1, source_target_pairs={{0,2},{1,3},{2,0},{3,1},{4,6},{5,7},{6,4},{7,5},{8,10},{9,11},{10,... | collective-permute-start | bytes 196616 | tf_op jit(solution)/shard_map/ppermute | solution.py:435
  107.9 31.2 %copy-start.6 = (f32[48,128]{1,0:T(8,128)S(1)}, f32[48,128]{1,0:T(8,128)}, u32[]{:S(2)}) copy-start(f32[48,128]{1,0:T(8,128)} %copy-done.5) | copy-start | bytes 73732
  107.9 31.2 %copy-start.8 = (f32[2048]{0:T(1024)S(1)}, f32[2048]{0:T(1024)}, u32[]{:S(2)}) copy-start(f32[2048]{0:T(1024)} %param.31) | copy-start | bytes 24580

commit v2 on v1

--- a/solution.py
+++ b/solution.py
@@ -12,8 +12,6 @@
 bf16 = jnp.bfloat16
 VMEM = pltpu.MemorySpace.VMEM
 lanes = 128
-gate_row = 8
-sent_rows = 9
 
 
 def iota(shape, dim):
@@ -86,9 +84,9 @@
     return (a[0] * b[0] - a[1] * b[1], a[0] * b[1] + a[1] * b[0])
 
 
-def local_kernel(
+def pushed(
     x_ref, gate_ref, rate_ref, turn_ref, drive_re_ref, drive_im_ref,
-    send_ref, state_re_ref, state_im_ref, wide_ref, step_ref,
+    push_re_ref, push_im_ref, wide_ref, step_ref,
 ):
     length = x_ref.shape[0]
     groups, states = rate_ref.shape[1:]
@@ -96,9 +94,8 @@
     tiles = width // lanes
     turned = reversal(length)
     x = x_ref[...]
-    log_gate = gate_ref[...]
     spread = (iota((groups, width), 0) == iota((groups, width), 1) // states).astype(f32).astype(bf16)
-    factors = split(jnp.exp(log_gate), 3)
+    factors = split(jnp.exp(gate_ref[...]), 3)
     for k in range(2):
         rate = rate_ref[k]
         step_re, step_im = steps_of(rate, turn_ref[k], groups, states)
@@ -118,45 +115,63 @@
             cols = slice(j * lanes, (j + 1) * lanes)
             rows = pl.ds(k * tiles + j, length, stride=2 * tiles)
             wide_ref[rows, :] = gates[:, cols]
-            state_re_ref[rows, :] = pushes[0][:, cols]
-            state_im_ref[rows, :] = pushes[1][:, cols]
+            push_re_ref[rows, :] = pushes[0][:, cols]
+            push_im_ref[rows, :] = pushes[1][:, cols]
             at = k * tiles + j
             step_ref[at : at + 1, :] = step_re[:, cols]
             step_ref[2 * tiles + at : 2 * tiles + at + 1, :] = step_im[:, cols]
-    high = 2 * tiles
-    w_re = step_ref[0:high, :]
-    w_im = step_ref[high : 2 * high, :]
+
+
+def local_kernel(
+    x_ref, gate_ref, rate_ref, turn_ref, drive_re_ref, drive_im_ref,
+    send_ref, push_re_ref, push_im_ref, wide_ref, step_ref, pair_ref,
+):
+    pushed(
+        x_ref, gate_ref, rate_ref, turn_ref, drive_re_ref, drive_im_ref,
+        push_re_ref, push_im_ref, wide_ref, step_ref,
+    )
+    groups = rate_ref.shape[1]
+    high = step_ref.shape[0] // 2
+    tiles = high // 2
+    half = x_ref.shape[0] // 2
+    w = (step_ref[0:high, :], step_ref[high : 2 * high, :])
 
     def advance(t, carried):
-        re, im = carried
-        at = pl.ds(pl.multiple_of(t * high, high), high)
-        factor = wide_ref[at, :]
-        a_re, a_im = factor * w_re, factor * w_im
-        new_re = (state_re_ref[at, :] + a_re * re) - a_im * im
-        new_im = (state_im_ref[at, :] + a_re * im) + a_im * re
-        state_re_ref[at, :] = new_re
-        state_im_ref[at, :] = new_im
-        return new_re, new_im
-
-    zero = jnp.zeros((high, lanes), f32)
-    re, im = lax.fori_loop(0, length, advance, (zero, zero), unroll=8)
-    step_ref[0:high, :] = re
-    step_ref[high : 2 * high, :] = im
-    blocks = send_ref.shape[0] // sent_rows
-    later = iota((blocks, lanes), 0) > lax.axis_index("sp")
-    for part in range(2):
-        for j in range(tiles):
-            forward = step_ref[part * high + j : part * high + j + 1, :]
-            backward = step_ref[part * high + tiles + j : part * high + tiles + j + 1, :]
-            send_ref[pl.ds(part * tiles + j, blocks, stride=sent_rows), :] = jnp.where(
-                later, forward, backward
+        states = []
+        for side, (re, im) in enumerate(carried[:2]):
+            at = pl.ds(pl.multiple_of((t + side * half) * high, high), high)
+            factor = wide_ref[at, :]
+            a_re, a_im = factor * w[0], factor * w[1]
+            states.append(
+                (
+                    (push_re_ref[at, :] + a_re * re) - a_im * im,
+                    (push_im_ref[at, :] + a_re * im) + a_im * re,
+                )
             )
-    total = jnp.sum(log_gate, axis=1, keepdims=True)
+        return (*states, cmul((a_re, a_im), carried[2]))
+
+    zero, one = jnp.zeros((high, lanes), f32), jnp.ones((high, lanes), f32)
+    early, late, faded = lax.fori_loop(
+        0, half, advance, ((zero, zero), (zero, zero), (one, zero)), unroll=8
+    )
+    whole = cmul(faded, early)
+    step_ref[0:high, :] = late[0] + whole[0]
+    step_ref[high : 2 * high, :] = late[1] + whole[1]
+    total = jnp.sum(gate_ref[...], axis=1, keepdims=True)
     thin = iota((groups, lanes), 0) == iota((groups, lanes), 1) // (lanes // groups)
-    total_row = jnp.sum(jnp.where(thin, total, 0.0), axis=0, keepdims=True)
-    send_ref[pl.ds(gate_row, blocks, stride=sent_rows), :] = jnp.broadcast_to(
-        total_row, (blocks, lanes)
-    )
+    total = jnp.sum(jnp.where(thin, total, 0.0), axis=0, keepdims=True)
+    total_high = total.astype(bf16).astype(f32)
+    for k in range(2):
+        for part, rest in enumerate((total_high, total - total_high)):
+            at = 2 * k + part
+            for j in range(tiles):
+                row = part * high + k * tiles + j
+                pair_ref[at : at + 1, j * lanes : (j + 1) * lanes] = step_ref[row : row + 1, :]
+            pair_ref[at : at + 1, tiles * lanes :] = rest
+    forward, backward = pair_ref[0:2, :], pair_ref[2:4, :]
+    here = lax.axis_index("sp")
+    for block in range(send_ref.shape[0]):
+        send_ref[block] = jnp.where(block > here, forward, backward).astype(bf16)
 
 
 def powers(step, length, backward):
@@ -204,9 +219,10 @@
 
 
 def beside_kernel(
-    x_ref, rate_ref, turn_ref, read_re_ref, read_im_ref, skip_ref,
-    state_re_ref, state_im_ref, routes_ref, group_ref, weight_ref,
+    x_ref, gate_ref, rate_ref, turn_ref, drive_re_ref, drive_im_ref, read_re_ref, read_im_ref,
+    skip_ref, routes_ref, group_ref, weight_ref,
     local_ref, chain_ref, pick_ref, mix_ref,
+    state_re_ref, state_im_ref, wide_ref, step_ref,
 ):
     length = x_ref.shape[0]
     groups, states = rate_ref.shape[1:]
@@ -214,6 +230,27 @@
     tiles = width // lanes
     blocks = chain_ref.shape[1]
     here = lax.axis_index("sp")
+    pushed(
+        x_ref, gate_ref, rate_ref, turn_ref, drive_re_ref, drive_im_ref,
+        state_re_ref, state_im_ref, wide_ref, step_ref,
+    )
+    high = 2 * tiles
+    w_re = step_ref[0:high, :]
+    w_im = step_ref[high : 2 * high, :]
+
+    def advance(t, carried):
+        re, im = carried
+        at = pl.ds(pl.multiple_of(t * high, high), high)
+        factor = wide_ref[at, :]
+        a_re, a_im = factor * w_re, factor * w_im
+        new_re = (state_re_ref[at, :] + a_re * re) - a_im * im
+        new_im = (state_im_ref[at, :] + a_re * im) + a_im * re
+        state_re_ref[at, :] = new_re
+        state_im_ref[at, :] = new_im
+        return new_re, new_im
+
+    zero = jnp.zeros((high, lanes), f32)
+    lax.fori_loop(0, length, advance, (zero, zero), unroll=8)
     rows, cols = iota((length, length), 0), iota((length, length), 1)
     outs, wholes = [], []
     for k in range(2):
@@ -271,21 +308,26 @@
 
 def carry_kernel(
     come_ref, local_ref, gate_ref, chain_ref, rate_ref, turn_ref, read_re_ref, read_im_ref,
-    own_ref, next_ref, last_ref, far_ref, act_ref,
+    own_ref, next_ref, last_ref, far_ref, act_ref, lines_ref,
 ):
     here, member = lax.axis_index("sp"), lax.axis_index("tp")
     blocks, width = chain_ref.shape[1:]
     groups, states = rate_ref.shape[1:]
     tiles = width // lanes
     length = local_ref.shape[0]
+    for block in range(blocks):
+        pair = come_ref[block].astype(f32)
+        for j in range(tiles + 1):
+            at = 2 * (j * blocks + block)
+            lines_ref[at : at + 2, :] = pair[:, j * lanes : (j + 1) * lanes]
+
+    def lines_of(part, j):
+        return lines_ref[pl.ds(2 * j * blocks + part, blocks, stride=2), :]
+
     came = [
-        jnp.concatenate(
-            [come_ref[pl.ds(p * tiles + j, blocks, stride=sent_rows), :] for j in range(tiles)],
-            axis=1,
-        )
-        for p in range(2)
+        jnp.concatenate([lines_of(part, j) for j in range(tiles)], axis=1) for part in range(2)
     ]
-    logs = come_ref[pl.ds(gate_row, blocks, stride=sent_rows), :]
+    logs = lines_of(0, tiles) + lines_of(1, tiles)
     each = lanes // groups
     fan = (iota((lanes, width), 0) == each * (iota((lanes, width), 1) // states)).astype(f32)
     fan = fan.astype(bf16)
@@ -381,9 +423,8 @@
     out_ref[...] = total + mm(next_ref[...], w_next_ref[...]).astype(bf16).astype(f32)
 
 
-def answer_kernel(sum_ref, far_ref, w_far_top_ref, w_far_low_ref, out_ref, rows_ref):
-    half = w_far_top_ref.shape[0]
-    far = mm(far_ref[:, :half], w_far_top_ref[...]) + mm(far_ref[:, half:], w_far_low_ref[...])
+def answer_kernel(sum_ref, far_ref, w_far_ref, out_ref, rows_ref):
+    far = mm(far_ref[...], w_far_ref[...])
     to_lines(sum_ref[...] + far.astype(bf16).astype(f32), rows_ref, out_ref)
 
 
@@ -435,30 +476,20 @@
         return lax.ppermute(array, "tp", way)
 
     down = down_weight[0]
-    half_down = down.shape[0] // 2
     down_last = moved(down, right)
     down_next = moved(down, left)
 
     flat = lambda table: table.reshape(2, -1, states)
-    send, state_re, state_im = call(
-        local_kernel,
-        [
-            shape((blocks * sent_rows, lanes), f32),
-            shape((length * 2 * width // lanes, lanes), f32),
-            shape((length * 2 * width // lanes, lanes), f32),
-        ],
-        [
-            pltpu.VMEM((length * 2 * width // lanes, lanes), f32),
-            pltpu.VMEM((4 * width // lanes, lanes), f32),
-        ],
-        1 << 30,
-        mixer_input, log_gate.T, decay_rate, turn_rate, flat(drive_real), flat(drive_imaginary),
+    rows = length * 2 * width // lanes
+    swept = [pltpu.VMEM((rows, lanes), f32)] * 3 + [pltpu.VMEM((4 * width // lanes, lanes), f32)]
+    send = call(
+        local_kernel, shape((blocks, 2, width + lanes), bf16),
+        swept + [pltpu.VMEM((8, width + lanes), f32)], 1 << 30,
+        mixer_input, log_gate.T, decay_rate, turn_rate, flat(drive_real),
+        flat(drive_imaginary),
         room=60,
     )
-    come = lax.all_to_all(
-        send.reshape(blocks, 1, sent_rows * lanes), "sp", split_axis=0, concat_axis=0,
-        tiled=True,
-    ).reshape(blocks * sent_rows, lanes)
+    come = lax.all_to_all(send, "sp", split_axis=0, concat_axis=0, tiled=True)
     local, chain, pick, mix = call(
         beside_kernel,
         [
@@ -467,16 +498,19 @@
             shape((slots, share), bf16),
             shape((share, slots), f32),
         ],
-        [],
+        swept,
         1 << 30,
-        mixer_input, decay_rate, turn_rate, flat(read_real), flat(read_imaginary),
-        skip_gain[None], state_re, state_im, routes.T, group_weight[None], expert_weight.T,
+        mixer_input, log_gate.T, decay_rate, turn_rate, flat(drive_real),
+        flat(drive_imaginary), flat(read_real), flat(read_imaginary), skip_gain[None], routes.T, group_weight[None], expert_weight.T,
         room=40,
     )
     own, to_next, to_last, to_far = call(
         carry_kernel,
         [shape((share, channels), bf16)] * 4,
-        [pltpu.VMEM((length, channels), bf16)],
+        [
+            pltpu.VMEM((length, channels), bf16),
+            pltpu.VMEM((2 * blocks * (width // lanes + 1), lanes), f32),
+        ],
         1 << 29,
         come, local, log_gate.T, chain, decay_rate, turn_rate, flat(read_real), flat(read_imaginary),
         room=40,
@@ -484,8 +518,7 @@
     from_far = moved(to_far, across)
     from_last = moved(to_next, right)
     from_next = moved(to_last, left)
-    down_far_top = moved(down_last[:half_down], right)
-    down_far_low = moved(down_next[half_down:], left)
+    down_far = moved(down_last, right)
     lines = slots * model // lanes
     middle, outgoing = call(
         branch_kernel,
@@ -527,7 +560,7 @@
     )
     answers = call(
         answer_kernel, shape((lines, lanes), bf16), [pltpu.VMEM((lines, lanes), f32)], 1 << 28,
-        summed, hidden_far, down_far_top, down_far_low,
+        summed, hidden_far, down_far,
     )
     returned = exchanged(answers)
     return call(

time: 141 us -> 147 us (1.043)
  waiting for transfers between devices: 46.1 us -> 49.5 us
  Pallas kernels: 17.1 us -> 19 us
  starting transfers between devices: 41.4 us -> 39.6 us
    ppermute x16 -> x15, starting transfers between devices: 21.7 us -> 14.8 us  [moved(): return lax.ppermute(array, 'tp', way)]
    ppermute x16 -> x15, waiting for transfers between devices: 22.6 us -> 28.5 us  [moved(): return lax.ppermute(array, 'tp', way)]
    all_to_all x1, starting transfers between devices: 6.61 us -> 11.7 us  [exchanged(): lax.all_to_all(array.reshape(blocks, lines // blocks, lanes), 'sp', split...]
    all_to_all x1, waiting for transfers between devices: 8.6 us -> 5.08 us  [on_device(): come = lax.all_to_all(send, 'sp', split_axis=0, concat_axis=0, tiled=True)]
    unnamed x42 -> x48, local copies, waits for them, and re-layouts: 2.94 us -> 5.37 us
    pallas_call x11, Pallas kernels: 17.1 us -> 19 us  [call(): pl.pallas_call(kernel, out_shape=outs, in_specs=[pl.BlockSpec(memory_spac...]
  transfers between devices with their start and end apart: 18 -> 17, of which waited for: 10 -> 8; matrix products, arithmetic and copies ran while one was open for 2% -> 1% of each run, Pallas kernels for 5% -> 8%
where the time goes in v2:
time: 147 us; the launch traced here: 146 us
  waiting for transfers between devices  49.5 us (34%)
  starting transfers between devices  39.6 us (27%)
  blocking collectives  31.2 us (21%)
  Pallas kernels  19 us (13%)
  local copies, waits for them, and re-layouts  6.43 us (4%)
    all_to_all x1, blocking collectives, exchanged(): lax.all_to_all(array.reshape(blocks, lines // blocks, lanes), 'sp', split...  31.2 us
    ppermute x15, waiting for transfers between devices, moved(): return lax.ppermute(array, 'tp', way)  28.5 us
    pallas_call x11, Pallas kernels, call(): pl.pallas_call(kernel, out_shape=outs, in_specs=[pl.BlockSpec(memory_spac...  19 us
    all_to_all x1, waiting for transfers between devices, exchanged(): lax.all_to_all(array.reshape(blocks, lines // blocks, lanes), 'sp', split...  15.9 us
    ppermute x15, starting transfers between devices, moved(): return lax.ppermute(array, 'tp', way)  14.8 us
    all_to_all x1, starting transfers between devices, on_device(): come = lax.all_to_all(send, 'sp', split_axis=0, concat_axis=0, tiled=True)  13.2 us
    all_to_all x1, starting transfers between devices, exchanged(): lax.all_to_all(array.reshape(blocks, lines // blocks, lanes), 'sp', split...  11.7 us
    unnamed x48, local copies, waits for them, and re-layouts  5.37 us
  transfers between devices with their start and end apart: 17, of which 8 were waited for; matrix products, arithmetic and copies ran while one was open for 1% of the time, Pallas kernels for 8%

profile of v2, /device:TPU:1, one launch (start us, length us, event | category | flops | bytes accessed | tf_op | source)
XLA Modules:
  0.0 146.1 jit_solution(2998214520309269856)
XLA Ops:
  0.1 3.5 %shard_map.181 = bf16[64,2,640]{2,1,0:T(2,128)(2,1)} custom-call(bf16[192,128]{1,0:T(8,128)(2,1)} %x_ref.3, f32[8,192]{1,0:T(8,128)} %bitcast.49, f32[2,8,64]{2,1,0:T(8,128)} %rate_ref.5, f32[2,8,64]{2,1,0:T(8,128)} %turn_ref.5, f32[2,128,64]{2,1,0:T(8,128)} %bitcast.41, f32[2,128,64]{2,1,0:T(8,128)} %bitcast.43), custom_call_target="tpu_custom_call" | custom-call | flops 1073741824 | bytes 1048576 | tf_op jit(solution)/shard_map/pallas_call | solution.py:448
  3.6 13.2 %all-to-all-start = ((bf16[64,2,640]{2,1,0:T(2,128)(2,1)}), bf16[64,2,640]{2,1,0:T(2,128)(2,1)S(1)}, u32[]{:S(2)}, u32[]{:S(2)}) async-start(bf16[64,2,640]{2,1,0:T(2,128)(2,1)} %shard_map.181), calls=%async_computation | async-start | bytes 327680 | tf_op jit(solution)/shard_map/all_to_all | solution.py:492
  16.8 1.3 collective-permute-start.9
  18.2 0.0 copy-start.10
  18.2 3.9 %shard_map.182 = (f32[192,128]{1,0:T(8,128)S(1)}, f32[2,64,512]{2,1,0:T(8,128)S(1)}, bf16[128,48]{1,0:T(8,128)(2,1)S(1)}, f32[48,128]{1,0:T(8,128)S(1)}) custom-call(bf16[192,128]{1,0:T(8,128)(2,1)S(1)} %copy-done.16, f32[8,192]{1,0:T(8,128)S(1)} %bitcast.50, f32[2,8,64]{2,1,0:T(8,128)S(1)} %copy-done.18, f32[2,8,64]{2,1,0:T(8,128)S(1)} %copy-done.19, ...), custom_call_target="tpu_custom_call" | custom-call | flops 1073741824 | bytes 1048576 | tf_op jit(solution)/shard_map/pallas_call | solution.py:448
  22.2 0.6 copy-done.6
  22.8 0.6 copy-done.8
  23.4 5.1 %all-to-all-done.come_ref = bf16[64,2,640]{2,1,0:T(2,128)(2,1)S(1)} async-done(((bf16[64,2,640]{2,1,0:T(2,128)(2,1)}), bf16[64,2,640]{2,1,0:T(2,128)(2,1)S(1)}, u32[]{:S(2)}, u32[]{:S(2)}) %all-to-all-start) | async-done | bytes 163872 | tf_op jit(solution)/shard_map/all_to_all | solution.py:492
  28.5 1.8 %shard_map.183 = (bf16[48,128]{1,0:T(8,128)(2,1)S(1)}, bf16[48,128]{1,0:T(8,128)(2,1)S(1)}, bf16[48,128]{1,0:T(8,128)(2,1)S(1)}, bf16[48,128]{1,0:T(8,128)(2,1)S(1)}) custom-call(bf16[64,2,640]{2,1,0:T(2,128)(2,1)S(1)} %all-to-all-done.come_ref, f32[192,128]{1,0:T(8,128)S(1)} %get-tuple-element.15.local_ref, f32[8,192]{1,0:T(8,128)S(1)} %bitcast.51, ...), custom_call_target="tpu_custom_call" | custom-call | flops 536870912 | bytes 1048576 | tf_op jit(solution)/shard_map/pallas_call | solution.py:448
  30.2 1.3 collective-permute-start
  31.5 2.4 %collective-permute-start.1 = (bf16[48,128]{1,0:T(8,128)(2,1)S(1)}, bf16[48,128]{1,0:T(8,128)(2,1)S(1)}, u32[]{:S(2)}, u32[]{:S(2)}) collective-permute-start(bf16[48,128]{1,0:T(8,128)(2,1)S(1)} %get-tuple-element.19), channel_id=1, source_target_pairs={{0,2},{1,3},{2,0},{3,1},{4,6},{5,7},{6,4},{7,5},{8,10},{9,11},{10,... | collective-permute-start | bytes 36872 | tf_op jit(solution)/shard_map/ppermute | solution.py:476
  34.0 1.2 collective-permute-start.2
  35.1 7.6 %collective-permute-done.from_last_ref = bf16[48,128]{1,0:T(8,128)(2,1)S(1)} collective-permute-done((bf16[48,128]{1,0:T(8,128)(2,1)S(1)}, bf16[48,128]{1,0:T(8,128)(2,1)S(1)}, u32[]{:S(2)}, u32[]{:S(2)}) %collective-permute-start) | collective-permute-done | bytes 12320 | tf_op jit(solution)/shard_map/ppermute | solution.py:476
  42.7 0.8 collective-permute-done.1.from_far_ref
  43.6 1.6 %copy-done.2 = bf16[512,2048]{1,0:T(8,128)(2,1)S(1)} copy-done((bf16[512,2048]{1,0:T(8,128)(2,1)S(1)}, bf16[512,2048]{1,0:T(8,128)(2,1)}, u32[]{:S(2)}) %copy-start.2) | copy-done | bytes 2097176
  45.2 0.9 copy-done.5
  46.1 0.8 copy-done.7
  46.9 1.1 shard_map.184
  48.0 0.8 copy-done.4
  48.8 11.7 %all-to-all-start.1 = ((bf16[64,32,128]{2,1,0:T(8,128)(2,1)}), bf16[64,32,128]{2,1,0:T(8,128)(2,1)}, u32[]{:S(2)}, u32[]{:S(2)}) async-start(bf16[64,32,128]{2,1,0:T(8,128)(2,1)} %bitcast.38), calls=%async_computation.1 | async-start | bytes 1048576 | tf_op jit(solution)/shard_map/all_to_all | solution.py:532
  60.5 0.4 collective-permute-start.10
  60.9 0.0 collective-permute-done.9.w_last_ref
  60.9 1.3 collective-permute-start.14
  62.2 15.9 %all-to-all-done.1 = bf16[64,32,128]{2,1,0:T(8,128)(2,1)} async-done(((bf16[64,32,128]{2,1,0:T(8,128)(2,1)}), bf16[64,32,128]{2,1,0:T(8,128)(2,1)}, u32[]{:S(2)}, u32[]{:S(2)}) %all-to-all-start.1) | async-done | bytes 524320 | tf_op jit(solution)/shard_map/all_to_all | solution.py:532
  78.1 1.1 fusion
  79.2 0.1 collective-permute-start.6
  79.3 0.2 collective-permute-start.7
  79.5 2.5 %collective-permute-start.4 = (bf16[1024,128]{1,0:T(8,128)(2,1)S(1)}, bf16[1024,128]{1,0:T(8,128)(2,1)S(1)}, u32[]{:S(2)}, u32[]{:S(2)}) collective-permute-start(bf16[1024,128]{1,0:T(8,128)(2,1)S(1)} %bitcast.33), channel_id=1, source_target_pairs={{0,3},{1,0},{2,1},{3,2},{4,7},{5,4},{6,5},{7,6},{8,11},{9,8},{10,9... | collective-permute-start | bytes 786440 | tf_op jit(solution)/shard_map/ppermute | solution.py:476
  82.0 9.8 %collective-permute-done.6.top_ref = bf16[1024,128]{1,0:T(8,128)(2,1)S(1)} collective-permute-done((bf16[1024,128]{1,0:T(8,128)(2,1)S(1)}, bf16[1024,128]{1,0:T(8,128)(2,1)S(1)}, u32[]{:S(2)}, u32[]{:S(2)}) %collective-permute-start.6) | collective-permute-done | bytes 262176 | tf_op jit(solution)/shard_map/ppermute | solution.py:476
  91.9 5.6 %collective-permute-done.7.low_ref = bf16[1024,128]{1,0:T(8,128)(2,1)S(1)} collective-permute-done((bf16[1024,128]{1,0:T(8,128)(2,1)S(1)}, bf16[1024,128]{1,0:T(8,128)(2,1)S(1)}, u32[]{:S(2)}, u32[]{:S(2)}) %collective-permute-start.7) | collective-permute-done | bytes 262176 | tf_op jit(solution)/shard_map/ppermute | solution.py:476
  97.5 0.1 collective-permute-start.11
  97.6 2.6 %collective-permute-start.12 = (bf16[1024,128]{1,0:T(8,128)(2,1)S(1)}, bf16[1024,128]{1,0:T(8,128)(2,1)S(1)}, u32[]{:S(2)}, u32[]{:S(2)}) collective-permute-start(bf16[1024,128]{1,0:T(8,128)(2,1)S(1)} %collective-permute-done.4.low_ref), channel_id=1, source_target_pairs={{0,3},{1,0},{2,1},{3,2},{4,7},{5,4},{6,5},{7,6},{8,11},{9,8},{10,9... | collective-permute-start | bytes 786440 | tf_op jit(solution)/shard_map/ppermute | solution.py:476
  100.2 0.8 shard_map.187
  101.0 0.1 collective-permute-start.8
  101.1 0.8 shard_map.186
  101.8 3.1 %collective-permute-done.11.top_ref = bf16[1024,128]{1,0:T(8,128)(2,1)S(1)} collective-permute-done((bf16[1024,128]{1,0:T(8,128)(2,1)S(1)}, bf16[1024,128]{1,0:T(8,128)(2,1)S(1)}, u32[]{:S(2)}, u32[]{:S(2)}) %collective-permute-start.11) | collective-permute-done | bytes 262176 | tf_op jit(solution)/shard_map/ppermute | solution.py:476
  104.9 0.8 shard_map.189
  105.7 1.3 collective-permute-start.13
  107.0 0.8 shard_map.185.own_ref
  107.7 0.0 collective-permute-done.10.w_next_ref
  107.7 1.5 %collective-permute-done.5.last_ref = bf16[128,256]{1,0:T(8,128)(2,1)S(1)} collective-permute-done((bf16[128,256]{1,0:T(8,128)(2,1)S(1)}, bf16[128,256]{1,0:T(8,128)(2,1)S(1)}, u32[]{:S(2)}, u32[]{:S(2)}) %collective-permute-start.5) | collective-permute-done | bytes 65568 | tf_op jit(solution)/shard_map/ppermute | solution.py:476
  109.2 2.2 %shard_map.188.sum_ref = f32[128,2048]{1,0:T(8,128)S(1)} custom-call(bf16[128,256]{1,0:T(8,128)(2,1)S(1)} %shard_map.185.own_ref, bf16[128,256]{1,0:T(8,128)(2,1)S(1)} %collective-permute-done.5.last_ref, bf16[128,256]{1,0:T(8,128)(2,1)S(1)} %collective-permute-done.8.next_ref, bf16[256,2048]{1,0:T(8,128)(2,1)S(1)} %bitcast.31, ...), custom_call_target="tpu_custom_call" | custom-call | flops 536870912 | bytes 1048576 | tf_op jit(solution)/shard_map/pallas_call | solution.py:448
  111.4 0.0 copy-start.11
  111.4 0.0 collective-permute-done.13.far_ref
  111.5 0.0 collective-permute-done.14.w_far_ref
  111.5 1.8 %shard_map.190 = bf16[2048,128]{1,0:T(8,128)(2,1)S(1)} custom-call(f32[128,2048]{1,0:T(8,128)S(1)} %shard_map.188.sum_ref, bf16[128,256]{1,0:T(8,128)(2,1)S(1)} %collective-permute-done.13.far_ref, bf16[256,2048]{1,0:T(8,128)(2,1)} %collective-permute-done.14.w_far_ref), custom_call_target="tpu_custom_call" | custom-call | flops 268435456 | bytes 1048576 | tf_op jit(solution)/shard_map/pallas_call | solution.py:448
  113.3 31.2 %all_to_all.15 = bf16[64,32,128]{2,1,0:T(8,128)(2,1)S(1)} all-to-all(bf16[64,32,128]{2,1,0:T(8,128)(2,1)S(1)} %bitcast.28), channel_id=1, replica_groups=mesh['sp'=64,'tp'=4] {'sp'}, dimensions={0} | all-to-all | bytes 1048576 | tf_op jit(solution)/shard_map/all_to_all | solution.py:532
  144.5 1.6 %shard_map.191 = bf16[48,2048]{1,0:T(8,128)(2,1)} custom-call(bf16[2048,128]{1,0:T(8,128)(2,1)S(1)} %bitcast.27, f32[48,128]{1,0:T(8,128)S(1)} %copy-done.9, f32[48,2048]{1,0:T(8,128)S(1)} %get-tuple-element.24.middle_ref, f32[1,2048]{1,0:T(1,128)S(1)} %bitcast.40), custom_call_target="tpu_custom_call" | custom-call | flops 268435456 | bytes 1048576 | tf_op jit(solution)/shard_map/pallas_call | solution.py:448
  (47 shorter events, 0.1 us)
Async XLA Ops:
  0.0 16.8 %copy-start.3 = (bf16[1,256,2048]{2,1,0:T(8,128)(2,1)S(1)}, bf16[1,256,2048]{2,1,0:T(8,128)(2,1)}, u32[]{:S(2)}) copy-start(bf16[1,256,2048]{2,1,0:T(8,128)(2,1)} %param.37) | copy-start | bytes 3145732
  0.0 18.1 %copy-start.12 = (f32[2,8,16,64]{3,2,1,0:T(8,128)S(1)}, f32[2,8,16,64]{3,2,1,0:T(8,128)}, u32[]{:S(2)}) copy-start(f32[2,8,16,64]{3,2,1,0:T(8,128)} %param.24) | copy-start | bytes 196612
  0.0 18.1 %copy-start.13 = (f32[2,8,16,64]{3,2,1,0:T(8,128)S(1)}, f32[2,8,16,64]{3,2,1,0:T(8,128)}, u32[]{:S(2)}) copy-start(f32[2,8,16,64]{3,2,1,0:T(8,128)} %param.25) | copy-start | bytes 196612
  0.0 18.1 %copy-start.14 = (f32[2,8,16,64]{3,2,1,0:T(8,128)S(1)}, f32[2,8,16,64]{3,2,1,0:T(8,128)}, u32[]{:S(2)}) copy-start(f32[2,8,16,64]{3,2,1,0:T(8,128)} %param.26) | copy-start | bytes 196612
  0.0 18.1 %copy-start.15 = (f32[2,8,16,64]{3,2,1,0:T(8,128)S(1)}, f32[2,8,16,64]{3,2,1,0:T(8,128)}, u32[]{:S(2)}) copy-start(f32[2,8,16,64]{3,2,1,0:T(8,128)} %param.27) | copy-start | bytes 196612
  0.0 18.1 %copy-start.16 = (bf16[192,128]{1,0:T(8,128)(2,1)S(1)}, bf16[192,128]{1,0:T(8,128)(2,1)}, u32[]{:S(2)}) copy-start(bf16[192,128]{1,0:T(8,128)(2,1)} %x_ref.3) | copy-start | bytes 147460
  0.0 18.1 %copy-start.17 = (f32[192,8]{0,1:T(8,128)S(1)}, f32[192,8]{0,1:T(8,128)}, u32[]{:S(2)}) copy-start(f32[192,8]{0,1:T(8,128)} %param.21) | copy-start | bytes 18436
  0.0 18.1 %copy-start.18 = (f32[2,8,64]{2,1,0:T(8,128)S(1)}, f32[2,8,64]{2,1,0:T(8,128)}, u32[]{:S(2)}) copy-start(f32[2,8,64]{2,1,0:T(8,128)} %rate_ref.5) | copy-start | bytes 12292
  0.1 18.1 %copy-start.19 = (f32[2,8,64]{2,1,0:T(8,128)S(1)}, f32[2,8,64]{2,1,0:T(8,128)}, u32[]{:S(2)}) copy-start(f32[2,8,64]{2,1,0:T(8,128)} %turn_ref.5) | copy-start | bytes 12292
  0.1 18.1 %copy-start.20 = (s32[192,2]{0,1:T(2,128)S(1)}, s32[192,2]{0,1:T(2,128)}, u32[]{:S(2)}) copy-start(s32[192,2]{0,1:T(2,128)} %param.32) | copy-start | bytes 4612
  0.1 18.1 %copy-start.21 = (f32[192,2]{0,1:T(2,128)S(1)}, f32[192,2]{0,1:T(2,128)}, u32[]{:S(2)}) copy-start(f32[192,2]{0,1:T(2,128)} %param.34) | copy-start | bytes 4612
  0.1 18.1 %copy-start.22 = (f32[192]{0:T(256)S(1)}, f32[192]{0:T(256)}, u32[]{:S(2)}) copy-start(f32[192]{0:T(256)} %param.33) | copy-start | bytes 2308
  0.1 18.1 %copy-start.23 = (f32[128]{0:T(128)S(1)}, f32[128]{0:T(128)}, u32[]{:S(2)}) copy-start(f32[128]{0:T(128)} %param.28) | copy-start | bytes 1540
  3.6 24.8 %all-to-all-start = ((bf16[64,2,640]{2,1,0:T(2,128)(2,1)}), bf16[64,2,640]{2,1,0:T(2,128)(2,1)S(1)}, u32[]{:S(2)}, u32[]{:S(2)}) async-start(bf16[64,2,640]{2,1,0:T(2,128)(2,1)} %shard_map.181), calls=%async_computation | async-start | bytes 327680 | tf_op jit(solution)/shard_map/all_to_all | solution.py:492
  16.8 44.1 %collective-permute-start.9 = (bf16[256,2048]{1,0:T(8,128)(2,1)S(1)}, bf16[256,2048]{1,0:T(8,128)(2,1)}, u32[]{:S(2)}, u32[]{:S(2)}) collective-permute-start(bf16[256,2048]{1,0:T(8,128)(2,1)S(1)} %bitcast.29), channel_id=1, source_target_pairs={{0,1},{1,2},{2,3},{3,0},{4,5},{5,6},{6,7},{7,4},{8,9},{9,10},{10,1... | collective-permute-start | bytes 3145736 | tf_op jit(solution)/shard_map/ppermute | solution.py:476
  18.2 25.4 %copy-start.10 = (f32[2048]{0:T(1024)S(1)}, f32[2048]{0:T(1024)}, u32[]{:S(2)}) copy-start(f32[2048]{0:T(1024)} %param.30) | copy-start | bytes 24580
  22.2 0.6 copy-start.6
  22.8 0.6 copy-start.8
  30.2 12.5 %collective-permute-start = (bf16[48,128]{1,0:T(8,128)(2,1)S(1)}, bf16[48,128]{1,0:T(8,128)(2,1)S(1)}, u32[]{:S(2)}, u32[]{:S(2)}) collective-permute-start(bf16[48,128]{1,0:T(8,128)(2,1)S(1)} %get-tuple-element.18), channel_id=1, source_target_pairs={{0,1},{1,2},{2,3},{3,0},{4,5},{5,6},{6,7},{7,4},{8,9},{9,10},{10,1... | collective-permute-start | bytes 36872 | tf_op jit(solution)/shard_map/ppermute | solution.py:476
  31.5 12.0 %collective-permute-start.1 = (bf16[48,128]{1,0:T(8,128)(2,1)S(1)}, bf16[48,128]{1,0:T(8,128)(2,1)S(1)}, u32[]{:S(2)}, u32[]{:S(2)}) collective-permute-start(bf16[48,128]{1,0:T(8,128)(2,1)S(1)} %get-tuple-element.19), channel_id=1, source_target_pairs={{0,2},{1,3},{2,0},{3,1},{4,6},{5,7},{6,4},{7,5},{8,10},{9,11},{10,... | collective-permute-start | bytes 36872 | tf_op jit(solution)/shard_map/ppermute | solution.py:476
  34.0 9.6 %collective-permute-start.2 = (bf16[48,128]{1,0:T(8,128)(2,1)S(1)}, bf16[48,128]{1,0:T(8,128)(2,1)S(1)}, u32[]{:S(2)}, u32[]{:S(2)}) collective-permute-start(bf16[48,128]{1,0:T(8,128)(2,1)S(1)} %get-tuple-element.20), channel_id=1, source_target_pairs={{0,3},{1,0},{2,1},{3,2},{4,7},{5,4},{6,5},{7,6},{8,11},{9,8},{10,9... | collective-permute-start | bytes 36872 | tf_op jit(solution)/shard_map/ppermute | solution.py:476
  43.6 1.6 %copy-start.2 = (bf16[512,2048]{1,0:T(8,128)(2,1)S(1)}, bf16[512,2048]{1,0:T(8,128)(2,1)}, u32[]{:S(2)}) copy-start(bf16[512,2048]{1,0:T(8,128)(2,1)} %weight_ref.1) | copy-start | bytes 6291460
  45.2 0.9 copy-start.5
  46.1 0.8 copy-start.7
  46.9 53.3 %copy-start = (bf16[1,2048,256]{2,1,0:T(8,128)(2,1)S(1)}, bf16[1,2048,256]{2,1,0:T(8,128)(2,1)}, u32[]{:S(2)}) copy-start(bf16[1,2048,256]{2,1,0:T(8,128)(2,1)} %param.35) | copy-start | bytes 3145732
  46.9 53.3 %copy-start.1 = (bf16[1,2048,256]{2,1,0:T(8,128)(2,1)S(1)}, bf16[1,2048,256]{2,1,0:T(8,128)(2,1)}, u32[]{:S(2)}) copy-start(bf16[1,2048,256]{2,1,0:T(8,128)(2,1)} %param.36) | copy-start | bytes 3145732
  48.0 0.8 copy-start.4
  48.8 29.3 %all-to-all-start.1 = ((bf16[64,32,128]{2,1,0:T(8,128)(2,1)}), bf16[64,32,128]{2,1,0:T(8,128)(2,1)}, u32[]{:S(2)}, u32[]{:S(2)}) async-start(bf16[64,32,128]{2,1,0:T(8,128)(2,1)} %bitcast.38), calls=%async_computation.1 | async-start | bytes 1048576 | tf_op jit(solution)/shard_map/all_to_all | solution.py:532
  60.5 47.2 %collective-permute-start.10 = (bf16[256,2048]{1,0:T(8,128)(2,1)S(1)}, bf16[256,2048]{1,0:T(8,128)(2,1)}, u32[]{:S(2)}, u32[]{:S(2)}) collective-permute-start(bf16[256,2048]{1,0:T(8,128)(2,1)S(1)} %bitcast.30), channel_id=1, source_target_pairs={{0,3},{1,0},{2,1},{3,2},{4,7},{5,4},{6,5},{7,6},{8,11},{9,8},{10,9... | collective-permute-start | bytes 3145736 | tf_op jit(solution)/shard_map/ppermute | solution.py:476
  60.9 50.5 %collective-permute-start.14 = (bf16[256,2048]{1,0:T(8,128)(2,1)}, bf16[256,2048]{1,0:T(8,128)(2,1)}, u32[]{:S(2)}, u32[]{:S(2)}) collective-permute-start(bf16[256,2048]{1,0:T(8,128)(2,1)} %collective-permute-done.9.w_last_ref), channel_id=1, source_target_pairs={{0,1},{1,2},{2,3},{3,0},{4,5},{5,6},{6,7},{7,4},{8,9},{9,10},{10,1... | collective-permute-start | bytes 3145736 | tf_op jit(solution)/shard_map/ppermute | solution.py:476
  79.2 12.7 %collective-permute-start.6 = (bf16[1024,128]{1,0:T(8,128)(2,1)S(1)}, bf16[1024,128]{1,0:T(8,128)(2,1)S(1)}, u32[]{:S(2)}, u32[]{:S(2)}) collective-permute-start(bf16[1024,128]{1,0:T(8,128)(2,1)S(1)} %bitcast.35), channel_id=1, source_target_pairs={{0,1},{1,2},{2,3},{3,0},{4,5},{5,6},{6,7},{7,4},{8,9},{9,10},{10,1... | collective-permute-start | bytes 786440 | tf_op jit(solution)/shard_map/ppermute | solution.py:476
  79.3 18.2 %collective-permute-start.7 = (bf16[1024,128]{1,0:T(8,128)(2,1)S(1)}, bf16[1024,128]{1,0:T(8,128)(2,1)S(1)}, u32[]{:S(2)}, u32[]{:S(2)}) collective-permute-start(bf16[1024,128]{1,0:T(8,128)(2,1)S(1)} %bitcast.32), channel_id=1, source_target_pairs={{0,1},{1,2},{2,3},{3,0},{4,5},{5,6},{6,7},{7,4},{8,9},{9,10},{10,1... | collective-permute-start | bytes 786440 | tf_op jit(solution)/shard_map/ppermute | solution.py:476
  79.5 18.1 %collective-permute-start.4 = (bf16[1024,128]{1,0:T(8,128)(2,1)S(1)}, bf16[1024,128]{1,0:T(8,128)(2,1)S(1)}, u32[]{:S(2)}, u32[]{:S(2)}) collective-permute-start(bf16[1024,128]{1,0:T(8,128)(2,1)S(1)} %bitcast.33), channel_id=1, source_target_pairs={{0,3},{1,0},{2,1},{3,2},{4,7},{5,4},{6,5},{7,6},{8,11},{9,8},{10,9... | collective-permute-start | bytes 786440 | tf_op jit(solution)/shard_map/ppermute | solution.py:476
  91.9 9.1 %collective-permute-start.3 = (bf16[1024,128]{1,0:T(8,128)(2,1)S(1)}, bf16[1024,128]{1,0:T(8,128)(2,1)S(1)}, u32[]{:S(2)}, u32[]{:S(2)}) collective-permute-start(bf16[1024,128]{1,0:T(8,128)(2,1)S(1)} %bitcast.36), channel_id=1, source_target_pairs={{0,3},{1,0},{2,1},{3,2},{4,7},{5,4},{6,5},{7,6},{8,11},{9,8},{10,9... | collective-permute-start | bytes 786440 | tf_op jit(solution)/shard_map/ppermute | solution.py:476
  97.5 7.4 %collective-permute-start.11 = (bf16[1024,128]{1,0:T(8,128)(2,1)S(1)}, bf16[1024,128]{1,0:T(8,128)(2,1)S(1)}, u32[]{:S(2)}, u32[]{:S(2)}) collective-permute-start(bf16[1024,128]{1,0:T(8,128)(2,1)S(1)} %collective-permute-done.6.top_ref), channel_id=1, source_target_pairs={{0,1},{1,2},{2,3},{3,0},{4,5},{5,6},{6,7},{7,4},{8,9},{9,10},{10,1... | collective-permute-start | bytes 786440 | tf_op jit(solution)/shard_map/ppermute | solution.py:476
  97.6 7.3 %collective-permute-start.12 = (bf16[1024,128]{1,0:T(8,128)(2,1)S(1)}, bf16[1024,128]{1,0:T(8,128)(2,1)S(1)}, u32[]{:S(2)}, u32[]{:S(2)}) collective-permute-start(bf16[1024,128]{1,0:T(8,128)(2,1)S(1)} %collective-permute-done.4.low_ref), channel_id=1, source_target_pairs={{0,3},{1,0},{2,1},{3,2},{4,7},{5,4},{6,5},{7,6},{8,11},{9,8},{10,9... | collective-permute-start | bytes 786440 | tf_op jit(solution)/shard_map/ppermute | solution.py:476
  101.0 6.8 %collective-permute-start.8 = (bf16[128,256]{1,0:T(8,128)(2,1)S(1)}, bf16[128,256]{1,0:T(8,128)(2,1)S(1)}, u32[]{:S(2)}, u32[]{:S(2)}) collective-permute-start(bf16[128,256]{1,0:T(8,128)(2,1)S(1)} %shard_map.187), channel_id=1, source_target_pairs={{0,3},{1,0},{2,1},{3,2},{4,7},{5,4},{6,5},{7,6},{8,11},{9,8},{10,9... | collective-permute-start | bytes 196616 | tf_op jit(solution)/shard_map/ppermute | solution.py:476
  104.9 4.3 %collective-permute-start.5 = (bf16[128,256]{1,0:T(8,128)(2,1)S(1)}, bf16[128,256]{1,0:T(8,128)(2,1)S(1)}, u32[]{:S(2)}, u32[]{:S(2)}) collective-permute-start(bf16[128,256]{1,0:T(8,128)(2,1)S(1)} %shard_map.186), channel_id=1, source_target_pairs={{0,1},{1,2},{2,3},{3,0},{4,5},{5,6},{6,7},{7,4},{8,9},{9,10},{10,1... | collective-permute-start | bytes 196616 | tf_op jit(solution)/shard_map/ppermute | solution.py:476
  105.7 5.8 %collective-permute-start.13 = (bf16[128,256]{1,0:T(8,128)(2,1)S(1)}, bf16[128,256]{1,0:T(8,128)(2,1)S(1)}, u32[]{:S(2)}, u32[]{:S(2)}) collective-permute-start(bf16[128,256]{1,0:T(8,128)(2,1)S(1)} %shard_map.189), channel_id=1, source_target_pairs={{0,2},{1,3},{2,0},{3,1},{4,6},{5,7},{6,4},{7,5},{8,10},{9,11},{10,... | collective-permute-start | bytes 196616 | tf_op jit(solution)/shard_map/ppermute | solution.py:476
  111.4 33.1 %copy-start.9 = (f32[48,128]{1,0:T(8,128)S(1)}, f32[48,128]{1,0:T(8,128)}, u32[]{:S(2)}) copy-start(f32[48,128]{1,0:T(8,128)} %copy-done.8) | copy-start | bytes 73732
  111.4 33.1 %copy-start.11 = (f32[2048]{0:T(1024)S(1)}, f32[2048]{0:T(1024)}, u32[]{:S(2)}) copy-start(f32[2048]{0:T(1024)} %param.31) | copy-start | bytes 24580

commit v3 on v2

--- a/solution.py
+++ b/solution.py
@@ -423,8 +423,9 @@
     out_ref[...] = total + mm(next_ref[...], w_next_ref[...]).astype(bf16).astype(f32)
 
 
-def answer_kernel(sum_ref, far_ref, w_far_ref, out_ref, rows_ref):
-    far = mm(far_ref[...], w_far_ref[...])
+def answer_kernel(sum_ref, far_ref, w_far_top_ref, w_far_low_ref, out_ref, rows_ref):
+    half = w_far_top_ref.shape[0]
+    far = mm(far_ref[:, :half], w_far_top_ref[...]) + mm(far_ref[:, half:], w_far_low_ref[...])
     to_lines(sum_ref[...] + far.astype(bf16).astype(f32), rows_ref, out_ref)
 
 
@@ -476,6 +477,7 @@
         return lax.ppermute(array, "tp", way)
 
     down = down_weight[0]
+    half_down = down.shape[0] // 2
     down_last = moved(down, right)
     down_next = moved(down, left)
 
@@ -485,8 +487,7 @@
     send = call(
         local_kernel, shape((blocks, 2, width + lanes), bf16),
         swept + [pltpu.VMEM((8, width + lanes), f32)], 1 << 30,
-        mixer_input, log_gate.T, decay_rate, turn_rate, flat(drive_real),
-        flat(drive_imaginary),
+        mixer_input, log_gate.T, decay_rate, turn_rate, flat(drive_real), flat(drive_imaginary),
         room=60,
     )
     come = lax.all_to_all(send, "sp", split_axis=0, concat_axis=0, tiled=True)
@@ -518,7 +519,8 @@
     from_far = moved(to_far, across)
     from_last = moved(to_next, right)
     from_next = moved(to_last, left)
-    down_far = moved(down_last, right)
+    down_far_top = moved(down_last[:half_down], right)
+    down_far_low = moved(down_next[half_down:], left)
     lines = slots * model // lanes
     middle, outgoing = call(
         branch_kernel,
@@ -560,7 +562,7 @@
     )
     answers = call(
         answer_kernel, shape((lines, lanes), bf16), [pltpu.VMEM((lines, lanes), f32)], 1 << 28,
-        summed, hidden_far, down_far,
+        summed, hidden_far, down_far_top, down_far_low,
     )
     returned = exchanged(answers)
     return call(

time: 147 us -> 141 us (0.959)
  local copies, waits for them, and re-layouts: 6.43 us -> 2.87 us
  waiting for transfers between devices: 49.5 us -> 48 us
    ppermute x15 -> x16, starting transfers between devices: 14.8 us -> 20.3 us  [moved(): return lax.ppermute(array, 'tp', way)]
    all_to_all x1, starting transfers between devices: 11.7 us -> 6.79 us  [exchanged(): lax.all_to_all(array.reshape(blocks, lines // blocks, lanes), 'sp', split...]
    unnamed x48 -> x42, local copies, waits for them, and re-layouts: 5.37 us -> 0.69 us
    ppermute x15 -> x16, waiting for transfers between devices: 28.5 us -> 25.7 us  [moved(): return lax.ppermute(array, 'tp', way)]
    all_to_all x1, waiting for transfers between devices: 5.08 us -> 6.95 us  [on_device(): come = lax.all_to_all(send, 'sp', split_axis=0, concat_axis=0, tiled=True)]
  transfers between devices with their start and end apart: 17 -> 18, of which waited for: 8 -> 10; matrix products, arithmetic and copies ran while one was open for 1% -> 2% of each run, Pallas kernels for 8% -> 6%
where the time goes in v3:
time: 141 us; the launch traced here: 140 us
  waiting for transfers between devices  48 us (34%)
  starting transfers between devices  40.3 us (29%)
  blocking collectives  30.4 us (22%)
  Pallas kernels  18.4 us (13%)
  local copies, waits for them, and re-layouts  2.87 us (2%)
    all_to_all x1, blocking collectives, exchanged(): lax.all_to_all(array.reshape(blocks, lines // blocks, lanes), 'sp', split...  30.4 us
    ppermute x16, waiting for transfers between devices, moved(): return lax.ppermute(array, 'tp', way)  25.7 us
    ppermute x16, starting transfers between devices, moved(): return lax.ppermute(array, 'tp', way)  20.3 us
    pallas_call x11, Pallas kernels, call(): pl.pallas_call(kernel, out_shape=outs, in_specs=[pl.BlockSpec(memory_spac...  18.4 us
    all_to_all x1, waiting for transfers between devices, exchanged(): lax.all_to_all(array.reshape(blocks, lines // blocks, lanes), 'sp', split...  15.3 us
    all_to_all x1, starting transfers between devices, on_device(): come = lax.all_to_all(send, 'sp', split_axis=0, concat_axis=0, tiled=True)  13.1 us
    all_to_all x1, waiting for transfers between devices, on_device(): come = lax.all_to_all(send, 'sp', split_axis=0, concat_axis=0, tiled=True)  6.95 us
    all_to_all x1, starting transfers between devices, exchanged(): lax.all_to_all(array.reshape(blocks, lines // blocks, lanes), 'sp', split...  6.79 us
  transfers between devices with their start and end apart: 18, of which 10 were waited for; matrix products, arithmetic and copies ran while one was open for 2% of the time, Pallas kernels for 6%

profile of v3, /device:TPU:1, one launch (start us, length us, event | category | flops | bytes accessed | tf_op | source)
XLA Modules:
  0.0 140.3 jit_solution(14572387827264589104)
XLA Ops:
  0.1 3.6 %shard_map.181 = bf16[64,2,640]{2,1,0:T(2,128)(2,1)} custom-call(bf16[192,128]{1,0:T(8,128)(2,1)} %x_ref.3, f32[8,192]{1,0:T(8,128)} %bitcast.48, f32[2,8,64]{2,1,0:T(8,128)} %rate_ref.5, f32[2,8,64]{2,1,0:T(8,128)} %turn_ref.5, f32[2,128,64]{2,1,0:T(8,128)} %bitcast.40, f32[2,128,64]{2,1,0:T(8,128)} %bitcast.42), custom_call_target="tpu_custom_call" | custom-call | flops 1073741824 | bytes 1048576 | tf_op jit(solution)/shard_map/pallas_call | solution.py:449
  3.7 13.1 %all-to-all-start = ((bf16[64,2,640]{2,1,0:T(2,128)(2,1)}), bf16[64,2,640]{2,1,0:T(2,128)(2,1)S(1)}, u32[]{:S(2)}, u32[]{:S(2)}) async-start(bf16[64,2,640]{2,1,0:T(2,128)(2,1)} %shard_map.181), calls=%async_computation | async-start | bytes 327680 | tf_op jit(solution)/shard_map/all_to_all | solution.py:493
  16.9 0.0 copy-start.2
  17.0 0.0 copy-start.4
  17.0 0.0 copy-start.7
  17.0 3.9 %shard_map.182 = (f32[192,128]{1,0:T(8,128)S(1)}, f32[2,64,512]{2,1,0:T(8,128)S(1)}, bf16[128,48]{1,0:T(8,128)(2,1)S(1)}, f32[48,128]{1,0:T(8,128)S(1)}) custom-call(bf16[192,128]{1,0:T(8,128)(2,1)S(1)} %copy-done.13, f32[8,192]{1,0:T(8,128)S(1)} %bitcast.49, f32[2,8,64]{2,1,0:T(8,128)S(1)} %copy-done.15, f32[2,8,64]{2,1,0:T(8,128)S(1)} %copy-done.16, ...), custom_call_target="tpu_custom_call" | custom-call | flops 1073741824 | bytes 1048576 | tf_op jit(solution)/shard_map/pallas_call | solution.py:449
  20.9 0.6 copy-done.5
  21.5 6.9 %all-to-all-done.come_ref = bf16[64,2,640]{2,1,0:T(2,128)(2,1)S(1)} async-done(((bf16[64,2,640]{2,1,0:T(2,128)(2,1)}), bf16[64,2,640]{2,1,0:T(2,128)(2,1)S(1)}, u32[]{:S(2)}, u32[]{:S(2)}) %all-to-all-start) | async-done | bytes 163872 | tf_op jit(solution)/shard_map/all_to_all | solution.py:493
  28.5 1.8 %shard_map.183 = (bf16[48,128]{1,0:T(8,128)(2,1)S(1)}, bf16[48,128]{1,0:T(8,128)(2,1)S(1)}, bf16[48,128]{1,0:T(8,128)(2,1)S(1)}, bf16[48,128]{1,0:T(8,128)(2,1)S(1)}) custom-call(bf16[64,2,640]{2,1,0:T(2,128)(2,1)S(1)} %all-to-all-done.come_ref, f32[192,128]{1,0:T(8,128)S(1)} %get-tuple-element.15.local_ref, f32[8,192]{1,0:T(8,128)S(1)} %bitcast.50, ...), custom_call_target="tpu_custom_call" | custom-call | flops 536870912 | bytes 1048576 | tf_op jit(solution)/shard_map/pallas_call | solution.py:449
  30.3 1.3 collective-permute-start
  31.6 2.4 %collective-permute-start.1 = (bf16[48,128]{1,0:T(8,128)(2,1)S(1)}, bf16[48,128]{1,0:T(8,128)(2,1)S(1)}, u32[]{:S(2)}, u32[]{:S(2)}) collective-permute-start(bf16[48,128]{1,0:T(8,128)(2,1)S(1)} %get-tuple-element.19), channel_id=1, source_target_pairs={{0,2},{1,3},{2,0},{3,1},{4,6},{5,7},{6,4},{7,5},{8,10},{9,11},{10,... | collective-permute-start | bytes 36872 | tf_op jit(solution)/shard_map/ppermute | solution.py:477
  34.0 1.1 collective-permute-start.2
  35.2 0.0 collective-permute-done.from_last_ref
  35.2 0.4 collective-permute-done.1.from_far_ref
  35.6 1.2 collective-permute-done.2.from_next_ref
  36.9 1.9 %shard_map.184 = (f32[48,2048]{1,0:T(8,128)S(1)}, bf16[2048,128]{1,0:T(8,128)(2,1)}) custom-call(bf16[48,128]{1,0:T(8,128)(2,1)S(1)} %get-tuple-element.17.own_ref, bf16[48,128]{1,0:T(8,128)(2,1)S(1)} %collective-permute-done.from_last_ref, bf16[48,128]{1,0:T(8,128)(2,1)S(1)} %collective-permute-done.1.from_far_ref, ...), custom_call_target="tpu_custom_call" | custom-call | flops 536870912 | bytes 1048576 | tf_op jit(solution)/shard_map/pallas_call | solution.py:449
  38.8 6.8 %all-to-all-start.1 = ((bf16[64,32,128]{2,1,0:T(8,128)(2,1)}), bf16[64,32,128]{2,1,0:T(8,128)(2,1)}, u32[]{:S(2)}, u32[]{:S(2)}) async-start(bf16[64,32,128]{2,1,0:T(8,128)(2,1)} %bitcast.10), calls=%async_computation.1 | async-start | bytes 1048576 | tf_op jit(solution)/shard_map/all_to_all | solution.py:534
  45.6 2.4 %collective-permute-start.10 = (bf16[256,2048]{1,0:T(8,128)(2,1)}, bf16[256,2048]{1,0:T(8,128)(2,1)S(1)}, u32[]{:S(2)}, u32[]{:S(2)}) collective-permute-start(bf16[256,2048]{1,0:T(8,128)(2,1)} %bitcast.29), channel_id=1, source_target_pairs={{0,3},{1,0},{2,1},{3,2},{4,7},{5,4},{6,5},{7,6},{8,11},{9,8},{10,9... | collective-permute-start | bytes 3145736 | tf_op jit(solution)/shard_map/ppermute | solution.py:477
  48.0 0.0 collective-permute-start.9
  48.0 15.3 %all-to-all-done.1 = bf16[64,32,128]{2,1,0:T(8,128)(2,1)} async-done(((bf16[64,32,128]{2,1,0:T(8,128)(2,1)}), bf16[64,32,128]{2,1,0:T(8,128)(2,1)}, u32[]{:S(2)}, u32[]{:S(2)}) %all-to-all-start.1) | async-done | bytes 524320 | tf_op jit(solution)/shard_map/all_to_all | solution.py:534
  63.3 1.1 fusion
  64.4 0.1 collective-permute-start.6
  64.5 0.9 collective-permute-start.7
  65.4 1.9 %collective-permute-start.4 = (bf16[1024,128]{1,0:T(8,128)(2,1)S(1)}, bf16[1024,128]{1,0:T(8,128)(2,1)S(1)}, u32[]{:S(2)}, u32[]{:S(2)}) collective-permute-start(bf16[1024,128]{1,0:T(8,128)(2,1)S(1)} %bitcast.33), channel_id=1, source_target_pairs={{0,3},{1,0},{2,1},{3,2},{4,7},{5,4},{6,5},{7,6},{8,11},{9,8},{10,9... | collective-permute-start | bytes 786440 | tf_op jit(solution)/shard_map/ppermute | solution.py:477
  67.2 3.0 %collective-permute-done.10.w_next_ref = bf16[256,2048]{1,0:T(8,128)(2,1)S(1)} collective-permute-done((bf16[256,2048]{1,0:T(8,128)(2,1)}, bf16[256,2048]{1,0:T(8,128)(2,1)S(1)}, u32[]{:S(2)}, u32[]{:S(2)}) %collective-permute-start.10) | collective-permute-done | bytes 1048608 | tf_op jit(solution)/shard_map/ppermute | solution.py:477
  70.3 3.4 %collective-permute-start.15 = (bf16[128,2048]{1,0:T(8,128)(2,1)S(1)}, bf16[128,2048]{1,0:T(8,128)(2,1)S(1)}, u32[]{:S(2)}, u32[]{:S(2)}) collective-permute-start(bf16[128,2048]{1,0:T(8,128)(2,1)S(1)} %slice.27), channel_id=1, source_target_pairs={{0,3},{1,0},{2,1},{3,2},{4,7},{5,4},{6,5},{7,6},{8,11},{9,8},{10,9... | collective-permute-start | bytes 1572872 | tf_op jit(solution)/shard_map/ppermute | solution.py:477
  73.6 0.0 collective-permute-done.9.w_last_ref
  73.6 1.1 slice.26
  74.7 0.1 collective-permute-start.14
  74.8 4.0 %collective-permute-done.6.top_ref = bf16[1024,128]{1,0:T(8,128)(2,1)S(1)} collective-permute-done((bf16[1024,128]{1,0:T(8,128)(2,1)S(1)}, bf16[1024,128]{1,0:T(8,128)(2,1)S(1)}, u32[]{:S(2)}, u32[]{:S(2)}) %collective-permute-start.6) | collective-permute-done | bytes 262176 | tf_op jit(solution)/shard_map/ppermute | solution.py:477
  78.9 5.6 %collective-permute-done.7.low_ref = bf16[1024,128]{1,0:T(8,128)(2,1)S(1)} collective-permute-done((bf16[1024,128]{1,0:T(8,128)(2,1)S(1)}, bf16[1024,128]{1,0:T(8,128)(2,1)S(1)}, u32[]{:S(2)}, u32[]{:S(2)}) %collective-permute-start.7) | collective-permute-done | bytes 262176 | tf_op jit(solution)/shard_map/ppermute | solution.py:477
  84.5 0.0 collective-permute-start.11
  84.5 2.7 %collective-permute-start.12 = (bf16[1024,128]{1,0:T(8,128)(2,1)S(1)}, bf16[1024,128]{1,0:T(8,128)(2,1)S(1)}, u32[]{:S(2)}, u32[]{:S(2)}) collective-permute-start(bf16[1024,128]{1,0:T(8,128)(2,1)S(1)} %collective-permute-done.4.low_ref), channel_id=1, source_target_pairs={{0,3},{1,0},{2,1},{3,2},{4,7},{5,4},{6,5},{7,6},{8,11},{9,8},{10,9... | collective-permute-start | bytes 786440 | tf_op jit(solution)/shard_map/ppermute | solution.py:477
  87.2 0.8 shard_map.187
  87.9 4.6 %collective-permute-done.3.top_ref = bf16[1024,128]{1,0:T(8,128)(2,1)S(1)} collective-permute-done((bf16[1024,128]{1,0:T(8,128)(2,1)S(1)}, bf16[1024,128]{1,0:T(8,128)(2,1)S(1)}, u32[]{:S(2)}, u32[]{:S(2)}) %collective-permute-start.3) | collective-permute-done | bytes 262176 | tf_op jit(solution)/shard_map/ppermute | solution.py:477
  92.6 3.4 %collective-permute-start.8 = (bf16[128,256]{1,0:T(8,128)(2,1)S(1)}, bf16[128,256]{1,0:T(8,128)(2,1)S(1)}, u32[]{:S(2)}, u32[]{:S(2)}) collective-permute-start(bf16[128,256]{1,0:T(8,128)(2,1)S(1)} %shard_map.187), channel_id=1, source_target_pairs={{0,3},{1,0},{2,1},{3,2},{4,7},{5,4},{6,5},{7,6},{8,11},{9,8},{10,9... | collective-permute-start | bytes 196616 | tf_op jit(solution)/shard_map/ppermute | solution.py:477
  96.0 0.8 shard_map.186
  96.8 0.0 copy-start.3
  96.8 4.6 %collective-permute-done.11.top_ref = bf16[1024,128]{1,0:T(8,128)(2,1)S(1)} collective-permute-done((bf16[1024,128]{1,0:T(8,128)(2,1)S(1)}, bf16[1024,128]{1,0:T(8,128)(2,1)S(1)}, u32[]{:S(2)}, u32[]{:S(2)}) %collective-permute-start.11) | collective-permute-done | bytes 262176 | tf_op jit(solution)/shard_map/ppermute | solution.py:477
  101.3 0.8 shard_map.189
  102.1 0.6 collective-permute-start.13
  102.7 0.8 shard_map.185.own_ref
  103.5 2.2 %collective-permute-done.5.last_ref = bf16[128,256]{1,0:T(8,128)(2,1)S(1)} collective-permute-done((bf16[128,256]{1,0:T(8,128)(2,1)S(1)}, bf16[128,256]{1,0:T(8,128)(2,1)S(1)}, u32[]{:S(2)}, u32[]{:S(2)}) %collective-permute-start.5) | collective-permute-done | bytes 65568 | tf_op jit(solution)/shard_map/ppermute | solution.py:477
  105.7 1.9 %shard_map.188.sum_ref = f32[128,2048]{1,0:T(8,128)S(1)} custom-call(bf16[128,256]{1,0:T(8,128)(2,1)S(1)} %shard_map.185.own_ref, bf16[128,256]{1,0:T(8,128)(2,1)S(1)} %collective-permute-done.5.last_ref, bf16[128,256]{1,0:T(8,128)(2,1)S(1)} %collective-permute-done.8.next_ref, bf16[256,2048]{1,0:T(8,128)(2,1)S(1)} %bitcast.31, ...), custom_call_target="tpu_custom_call" | custom-call | flops 536870912 | bytes 1048576 | tf_op jit(solution)/shard_map/pallas_call | solution.py:449
  107.5 0.0 copy-start.8
  107.6 0.7 shard_map.190
  108.3 30.4 %all_to_all.15 = bf16[64,32,128]{2,1,0:T(8,128)(2,1)S(1)} all-to-all(bf16[64,32,128]{2,1,0:T(8,128)(2,1)S(1)} %bitcast.28), channel_id=1, replica_groups=mesh['sp'=64,'tp'=4] {'sp'}, dimensions={0} | all-to-all | bytes 1048576 | tf_op jit(solution)/shard_map/all_to_all | solution.py:534
  138.7 1.6 %shard_map.191 = bf16[48,2048]{1,0:T(8,128)(2,1)} custom-call(bf16[2048,128]{1,0:T(8,128)(2,1)S(1)} %bitcast.27, f32[48,128]{1,0:T(8,128)S(1)} %copy-done.6, f32[48,2048]{1,0:T(8,128)S(1)} %get-tuple-element.24.middle_ref, f32[1,2048]{1,0:T(1,128)S(1)} %bitcast.39), custom_call_target="tpu_custom_call" | custom-call | flops 268435456 | bytes 1048576 | tf_op jit(solution)/shard_map/pallas_call | solution.py:449
  (45 shorter events, 0.1 us)
Async XLA Ops:
  0.0 16.8 %copy-start.9 = (f32[2,8,16,64]{3,2,1,0:T(8,128)S(1)}, f32[2,8,16,64]{3,2,1,0:T(8,128)}, u32[]{:S(2)}) copy-start(f32[2,8,16,64]{3,2,1,0:T(8,128)} %param.24) | copy-start | bytes 196612
  0.0 16.8 %copy-start.10 = (f32[2,8,16,64]{3,2,1,0:T(8,128)S(1)}, f32[2,8,16,64]{3,2,1,0:T(8,128)}, u32[]{:S(2)}) copy-start(f32[2,8,16,64]{3,2,1,0:T(8,128)} %param.25) | copy-start | bytes 196612
  0.0 16.8 %copy-start.11 = (f32[2,8,16,64]{3,2,1,0:T(8,128)S(1)}, f32[2,8,16,64]{3,2,1,0:T(8,128)}, u32[]{:S(2)}) copy-start(f32[2,8,16,64]{3,2,1,0:T(8,128)} %param.26) | copy-start | bytes 196612
  0.0 16.8 %copy-start.12 = (f32[2,8,16,64]{3,2,1,0:T(8,128)S(1)}, f32[2,8,16,64]{3,2,1,0:T(8,128)}, u32[]{:S(2)}) copy-start(f32[2,8,16,64]{3,2,1,0:T(8,128)} %param.27) | copy-start | bytes 196612
  0.0 16.8 %copy-start.13 = (bf16[192,128]{1,0:T(8,128)(2,1)S(1)}, bf16[192,128]{1,0:T(8,128)(2,1)}, u32[]{:S(2)}) copy-start(bf16[192,128]{1,0:T(8,128)(2,1)} %x_ref.3) | copy-start | bytes 147460
  0.0 16.8 %copy-start.14 = (f32[192,8]{0,1:T(8,128)S(1)}, f32[192,8]{0,1:T(8,128)}, u32[]{:S(2)}) copy-start(f32[192,8]{0,1:T(8,128)} %param.21) | copy-start | bytes 18436
  0.0 16.8 %copy-start.15 = (f32[2,8,64]{2,1,0:T(8,128)S(1)}, f32[2,8,64]{2,1,0:T(8,128)}, u32[]{:S(2)}) copy-start(f32[2,8,64]{2,1,0:T(8,128)} %rate_ref.5) | copy-start | bytes 12292
  0.0 16.8 %copy-start.16 = (f32[2,8,64]{2,1,0:T(8,128)S(1)}, f32[2,8,64]{2,1,0:T(8,128)}, u32[]{:S(2)}) copy-start(f32[2,8,64]{2,1,0:T(8,128)} %turn_ref.5) | copy-start | bytes 12292
  0.1 16.8 %copy-start.17 = (s32[192,2]{0,1:T(2,128)S(1)}, s32[192,2]{0,1:T(2,128)}, u32[]{:S(2)}) copy-start(s32[192,2]{0,1:T(2,128)} %param.32) | copy-start | bytes 4612
  0.1 16.8 %copy-start.18 = (f32[192,2]{0,1:T(2,128)S(1)}, f32[192,2]{0,1:T(2,128)}, u32[]{:S(2)}) copy-start(f32[192,2]{0,1:T(2,128)} %param.34) | copy-start | bytes 4612
  0.1 16.8 %copy-start.19 = (f32[192]{0:T(256)S(1)}, f32[192]{0:T(256)}, u32[]{:S(2)}) copy-start(f32[192]{0:T(256)} %param.33) | copy-start | bytes 2308
  0.1 16.8 %copy-start.20 = (f32[128]{0:T(128)S(1)}, f32[128]{0:T(128)}, u32[]{:S(2)}) copy-start(f32[128]{0:T(128)} %param.28) | copy-start | bytes 1540
  3.7 24.8 %all-to-all-start = ((bf16[64,2,640]{2,1,0:T(2,128)(2,1)}), bf16[64,2,640]{2,1,0:T(2,128)(2,1)S(1)}, u32[]{:S(2)}, u32[]{:S(2)}) async-start(bf16[64,2,640]{2,1,0:T(2,128)(2,1)} %shard_map.181), calls=%async_computation | async-start | bytes 327680 | tf_op jit(solution)/shard_map/all_to_all | solution.py:493
  16.9 19.9 %copy-start.2 = (bf16[512,2048]{1,0:T(8,128)(2,1)S(1)}, bf16[512,2048]{1,0:T(8,128)(2,1)}, u32[]{:S(2)}) copy-start(bf16[512,2048]{1,0:T(8,128)(2,1)} %weight_ref.1) | copy-start | bytes 6291460
  17.0 19.9 %copy-start.4 = (bf16[48,2048]{1,0:T(8,128)(2,1)S(1)}, bf16[48,2048]{1,0:T(8,128)(2,1)}, u32[]{:S(2)}) copy-start(bf16[48,2048]{1,0:T(8,128)(2,1)} %residual_ref.1) | copy-start | bytes 589828
  17.0 19.9 %copy-start.7 = (f32[2048]{0:T(1024)S(1)}, f32[2048]{0:T(1024)}, u32[]{:S(2)}) copy-start(f32[2048]{0:T(1024)} %param.30) | copy-start | bytes 24580
  20.9 0.6 copy-start.5
  30.3 4.9 %collective-permute-start = (bf16[48,128]{1,0:T(8,128)(2,1)S(1)}, bf16[48,128]{1,0:T(8,128)(2,1)S(1)}, u32[]{:S(2)}, u32[]{:S(2)}) collective-permute-start(bf16[48,128]{1,0:T(8,128)(2,1)S(1)} %get-tuple-element.18), channel_id=1, source_target_pairs={{0,1},{1,2},{2,3},{3,0},{4,5},{5,6},{6,7},{7,4},{8,9},{9,10},{10,1... | collective-permute-start | bytes 36872 | tf_op jit(solution)/shard_map/ppermute | solution.py:477
  31.6 4.0 %collective-permute-start.1 = (bf16[48,128]{1,0:T(8,128)(2,1)S(1)}, bf16[48,128]{1,0:T(8,128)(2,1)S(1)}, u32[]{:S(2)}, u32[]{:S(2)}) collective-permute-start(bf16[48,128]{1,0:T(8,128)(2,1)S(1)} %get-tuple-element.19), channel_id=1, source_target_pairs={{0,2},{1,3},{2,0},{3,1},{4,6},{5,7},{6,4},{7,5},{8,10},{9,11},{10,... | collective-permute-start | bytes 36872 | tf_op jit(solution)/shard_map/ppermute | solution.py:477
  34.0 2.8 %collective-permute-start.2 = (bf16[48,128]{1,0:T(8,128)(2,1)S(1)}, bf16[48,128]{1,0:T(8,128)(2,1)S(1)}, u32[]{:S(2)}, u32[]{:S(2)}) collective-permute-start(bf16[48,128]{1,0:T(8,128)(2,1)S(1)} %get-tuple-element.20), channel_id=1, source_target_pairs={{0,3},{1,0},{2,1},{3,2},{4,7},{5,4},{6,5},{7,6},{8,11},{9,8},{10,9... | collective-permute-start | bytes 36872 | tf_op jit(solution)/shard_map/ppermute | solution.py:477
  38.8 48.4 %copy-start = (bf16[1,2048,256]{2,1,0:T(8,128)(2,1)S(1)}, bf16[1,2048,256]{2,1,0:T(8,128)(2,1)}, u32[]{:S(2)}) copy-start(bf16[1,2048,256]{2,1,0:T(8,128)(2,1)} %param.35) | copy-start | bytes 3145732
  38.8 48.4 %copy-start.1 = (bf16[1,2048,256]{2,1,0:T(8,128)(2,1)S(1)}, bf16[1,2048,256]{2,1,0:T(8,128)(2,1)}, u32[]{:S(2)}) copy-start(bf16[1,2048,256]{2,1,0:T(8,128)(2,1)} %param.36) | copy-start | bytes 3145732
  38.8 24.5 %all-to-all-start.1 = ((bf16[64,32,128]{2,1,0:T(8,128)(2,1)}), bf16[64,32,128]{2,1,0:T(8,128)(2,1)}, u32[]{:S(2)}, u32[]{:S(2)}) async-start(bf16[64,32,128]{2,1,0:T(8,128)(2,1)} %bitcast.10), calls=%async_computation.1 | async-start | bytes 1048576 | tf_op jit(solution)/shard_map/all_to_all | solution.py:534
  45.6 24.6 %collective-permute-start.10 = (bf16[256,2048]{1,0:T(8,128)(2,1)}, bf16[256,2048]{1,0:T(8,128)(2,1)S(1)}, u32[]{:S(2)}, u32[]{:S(2)}) collective-permute-start(bf16[256,2048]{1,0:T(8,128)(2,1)} %bitcast.29), channel_id=1, source_target_pairs={{0,3},{1,0},{2,1},{3,2},{4,7},{5,4},{6,5},{7,6},{8,11},{9,8},{10,9... | collective-permute-start | bytes 3145736 | tf_op jit(solution)/shard_map/ppermute | solution.py:477
  48.0 25.6 %collective-permute-start.9 = (bf16[256,2048]{1,0:T(8,128)(2,1)}, bf16[256,2048]{1,0:T(8,128)(2,1)}, u32[]{:S(2)}, u32[]{:S(2)}) collective-permute-start(bf16[256,2048]{1,0:T(8,128)(2,1)} %bitcast.30), channel_id=1, source_target_pairs={{0,1},{1,2},{2,3},{3,0},{4,5},{5,6},{6,7},{7,4},{8,9},{9,10},{10,1... | collective-permute-start | bytes 3145736 | tf_op jit(solution)/shard_map/ppermute | solution.py:477
  64.4 14.5 %collective-permute-start.6 = (bf16[1024,128]{1,0:T(8,128)(2,1)S(1)}, bf16[1024,128]{1,0:T(8,128)(2,1)S(1)}, u32[]{:S(2)}, u32[]{:S(2)}) collective-permute-start(bf16[1024,128]{1,0:T(8,128)(2,1)S(1)} %bitcast.35), channel_id=1, source_target_pairs={{0,1},{1,2},{2,3},{3,0},{4,5},{5,6},{6,7},{7,4},{8,9},{9,10},{10,1... | collective-permute-start | bytes 786440 | tf_op jit(solution)/shard_map/ppermute | solution.py:477
  64.5 20.0 %collective-permute-start.7 = (bf16[1024,128]{1,0:T(8,128)(2,1)S(1)}, bf16[1024,128]{1,0:T(8,128)(2,1)S(1)}, u32[]{:S(2)}, u32[]{:S(2)}) collective-permute-start(bf16[1024,128]{1,0:T(8,128)(2,1)S(1)} %bitcast.32), channel_id=1, source_target_pairs={{0,1},{1,2},{2,3},{3,0},{4,5},{5,6},{6,7},{7,4},{8,9},{9,10},{10,1... | collective-permute-start | bytes 786440 | tf_op jit(solution)/shard_map/ppermute | solution.py:477
  65.4 19.1 %collective-permute-start.4 = (bf16[1024,128]{1,0:T(8,128)(2,1)S(1)}, bf16[1024,128]{1,0:T(8,128)(2,1)S(1)}, u32[]{:S(2)}, u32[]{:S(2)}) collective-permute-start(bf16[1024,128]{1,0:T(8,128)(2,1)S(1)} %bitcast.33), channel_id=1, source_target_pairs={{0,3},{1,0},{2,1},{3,2},{4,7},{5,4},{6,5},{7,6},{8,11},{9,8},{10,9... | collective-permute-start | bytes 786440 | tf_op jit(solution)/shard_map/ppermute | solution.py:477
  70.3 37.3 %collective-permute-start.15 = (bf16[128,2048]{1,0:T(8,128)(2,1)S(1)}, bf16[128,2048]{1,0:T(8,128)(2,1)S(1)}, u32[]{:S(2)}, u32[]{:S(2)}) collective-permute-start(bf16[128,2048]{1,0:T(8,128)(2,1)S(1)} %slice.27), channel_id=1, source_target_pairs={{0,3},{1,0},{2,1},{3,2},{4,7},{5,4},{6,5},{7,6},{8,11},{9,8},{10,9... | collective-permute-start | bytes 1572872 | tf_op jit(solution)/shard_map/ppermute | solution.py:477
  74.7 32.8 %collective-permute-start.14 = (bf16[128,2048]{1,0:T(8,128)(2,1)S(1)}, bf16[128,2048]{1,0:T(8,128)(2,1)S(1)}, u32[]{:S(2)}, u32[]{:S(2)}) collective-permute-start(bf16[128,2048]{1,0:T(8,128)(2,1)S(1)} %slice.26), channel_id=1, source_target_pairs={{0,1},{1,2},{2,3},{3,0},{4,5},{5,6},{6,7},{7,4},{8,9},{9,10},{10,1... | collective-permute-start | bytes 1572872 | tf_op jit(solution)/shard_map/ppermute | solution.py:477
  78.9 13.7 %collective-permute-start.3 = (bf16[1024,128]{1,0:T(8,128)(2,1)S(1)}, bf16[1024,128]{1,0:T(8,128)(2,1)S(1)}, u32[]{:S(2)}, u32[]{:S(2)}) collective-permute-start(bf16[1024,128]{1,0:T(8,128)(2,1)S(1)} %bitcast.36), channel_id=1, source_target_pairs={{0,3},{1,0},{2,1},{3,2},{4,7},{5,4},{6,5},{7,6},{8,11},{9,8},{10,9... | collective-permute-start | bytes 786440 | tf_op jit(solution)/shard_map/ppermute | solution.py:477
  84.5 16.9 %collective-permute-start.11 = (bf16[1024,128]{1,0:T(8,128)(2,1)S(1)}, bf16[1024,128]{1,0:T(8,128)(2,1)S(1)}, u32[]{:S(2)}, u32[]{:S(2)}) collective-permute-start(bf16[1024,128]{1,0:T(8,128)(2,1)S(1)} %collective-permute-done.6.top_ref), channel_id=1, source_target_pairs={{0,1},{1,2},{2,3},{3,0},{4,5},{5,6},{6,7},{7,4},{8,9},{9,10},{10,1... | collective-permute-start | bytes 786440 | tf_op jit(solution)/shard_map/ppermute | solution.py:477
  84.5 16.9 %collective-permute-start.12 = (bf16[1024,128]{1,0:T(8,128)(2,1)S(1)}, bf16[1024,128]{1,0:T(8,128)(2,1)S(1)}, u32[]{:S(2)}, u32[]{:S(2)}) collective-permute-start(bf16[1024,128]{1,0:T(8,128)(2,1)S(1)} %collective-permute-done.4.low_ref), channel_id=1, source_target_pairs={{0,3},{1,0},{2,1},{3,2},{4,7},{5,4},{6,5},{7,6},{8,11},{9,8},{10,9... | collective-permute-start | bytes 786440 | tf_op jit(solution)/shard_map/ppermute | solution.py:477
  92.6 10.9 %collective-permute-start.8 = (bf16[128,256]{1,0:T(8,128)(2,1)S(1)}, bf16[128,256]{1,0:T(8,128)(2,1)S(1)}, u32[]{:S(2)}, u32[]{:S(2)}) collective-permute-start(bf16[128,256]{1,0:T(8,128)(2,1)S(1)} %shard_map.187), channel_id=1, source_target_pairs={{0,3},{1,0},{2,1},{3,2},{4,7},{5,4},{6,5},{7,6},{8,11},{9,8},{10,9... | collective-permute-start | bytes 196616 | tf_op jit(solution)/shard_map/ppermute | solution.py:477
  96.8 8.9 %copy-start.3 = (bf16[1,256,2048]{2,1,0:T(8,128)(2,1)S(1)}, bf16[1,256,2048]{2,1,0:T(8,128)(2,1)}, u32[]{:S(2)}) copy-start(bf16[1,256,2048]{2,1,0:T(8,128)(2,1)} %param.37) | copy-start | bytes 3145732
  101.3 4.3 %collective-permute-start.5 = (bf16[128,256]{1,0:T(8,128)(2,1)S(1)}, bf16[128,256]{1,0:T(8,128)(2,1)S(1)}, u32[]{:S(2)}, u32[]{:S(2)}) collective-permute-start(bf16[128,256]{1,0:T(8,128)(2,1)S(1)} %shard_map.186), channel_id=1, source_target_pairs={{0,1},{1,2},{2,3},{3,0},{4,5},{5,6},{6,7},{7,4},{8,9},{9,10},{10,1... | collective-permute-start | bytes 196616 | tf_op jit(solution)/shard_map/ppermute | solution.py:477
  102.1 5.5 %collective-permute-start.13 = (bf16[128,256]{1,0:T(8,128)(2,1)S(1)}, bf16[128,256]{1,0:T(8,128)(2,1)S(1)}, u32[]{:S(2)}, u32[]{:S(2)}) collective-permute-start(bf16[128,256]{1,0:T(8,128)(2,1)S(1)} %shard_map.189), channel_id=1, source_target_pairs={{0,2},{1,3},{2,0},{3,1},{4,6},{5,7},{6,4},{7,5},{8,10},{9,11},{10,... | collective-permute-start | bytes 196616 | tf_op jit(solution)/shard_map/ppermute | solution.py:477
  107.5 31.2 %copy-start.6 = (f32[48,128]{1,0:T(8,128)S(1)}, f32[48,128]{1,0:T(8,128)}, u32[]{:S(2)}) copy-start(f32[48,128]{1,0:T(8,128)} %copy-done.5) | copy-start | bytes 73732
  107.5 31.2 %copy-start.8 = (f32[2048]{0:T(1024)S(1)}, f32[2048]{0:T(1024)}, u32[]{:S(2)}) copy-start(f32[2048]{0:T(1024)} %param.31) | copy-start | bytes 24580

commit v4 on v3

--- a/solution.py
+++ b/solution.py
@@ -133,30 +133,36 @@
     groups = rate_ref.shape[1]
     high = step_ref.shape[0] // 2
     tiles = high // 2
-    half = x_ref.shape[0] // 2
+    parts = 4
+    span = x_ref.shape[0] // parts
     w = (step_ref[0:high, :], step_ref[high : 2 * high, :])
 
     def advance(t, carried):
-        states = []
-        for side, (re, im) in enumerate(carried[:2]):
-            at = pl.ds(pl.multiple_of((t + side * half) * high, high), high)
+        states, faded = carried
+        new_states, new_faded = [], []
+        for side, (re, im) in enumerate(states):
+            at = pl.ds(pl.multiple_of((t + side * span) * high, high), high)
             factor = wide_ref[at, :]
             a_re, a_im = factor * w[0], factor * w[1]
-            states.append(
+            new_states.append(
                 (
                     (push_re_ref[at, :] + a_re * re) - a_im * im,
                     (push_im_ref[at, :] + a_re * im) + a_im * re,
                 )
             )
-        return (*states, cmul((a_re, a_im), carried[2]))
+            if side:
+                new_faded.append(cmul((a_re, a_im), faded[side - 1]))
+        return tuple(new_states), tuple(new_faded)
 
     zero, one = jnp.zeros((high, lanes), f32), jnp.ones((high, lanes), f32)
-    early, late, faded = lax.fori_loop(
-        0, half, advance, ((zero, zero), (zero, zero), (one, zero)), unroll=8
-    )
-    whole = cmul(faded, early)
-    step_ref[0:high, :] = late[0] + whole[0]
-    step_ref[high : 2 * high, :] = late[1] + whole[1]
+    states, faded = lax.fori_loop(
+        0, span, advance, (((zero, zero),) * parts, ((one, zero),) * (parts - 1)), unroll=4
+    )
+    last = states[0]
+    for state, fade in zip(states[1:], faded):
+        last = tuple(s + f for s, f in zip(state, cmul(fade, last)))
+    step_ref[0:high, :] = last[0]
+    step_ref[high : 2 * high, :] = last[1]
     total = jnp.sum(gate_ref[...], axis=1, keepdims=True)
     thin = iota((groups, lanes), 0) == iota((groups, lanes), 1) // (lanes // groups)
     total = jnp.sum(jnp.where(thin, total, 0.0), axis=0, keepdims=True)
@@ -353,7 +359,8 @@
         for part, side in enumerate((first, second)):
             side_high, side_low = split(side, 2)
             high, low = split(grown[part], 2)
-            more = mm_nt(high, side_high) + mm_nt(low, side_high) + mm_nt(high, side_low)
+            two = mm_nt(jnp.concatenate([high, low], axis=0), side_high)
+            more = two[:length] + two[length:] + mm_nt(high, side_low)
             value = more if value is None else value + more
         seen = (rows <= cols) if k == 0 else (rows >= cols)
         fade = jnp.exp(exact_right(gate_ref[...], seen.astype(f32).astype(bf16)))
@@ -407,14 +414,18 @@
     to_lines(mm(pick_ref[...], middle.astype(bf16)), rows_ref, out_ref)
 
 
-def hidden_kernel(top_ref, low_ref, gate_ref, linear_ref, out_ref, rows_ref):
+def hidden_kernel(top_ref, low_ref, gate_ref, linear_ref, out_ref, top_rows, low_rows):
     each = gate_ref.shape[0] // lanes
-    half = top_ref.shape[0] // each
-    for at, ref in ((0, top_ref), (half, low_ref)):
-        rows = jnp.concatenate(from_lines(ref, rows_ref, each), axis=1)
-        gate = mm(rows, gate_ref[...])
-        linear = mm(rows, linear_ref[...])
-        out_ref[at : at + half, :] = (jax.nn.silu(gate) * linear).astype(bf16)
+    rows = jnp.concatenate(
+        [
+            jnp.concatenate(from_lines(ref, rows_ref, each), axis=1)
+            for ref, rows_ref in ((top_ref, top_rows), (low_ref, low_rows))
+        ],
+        axis=0,
+    )
+    gate = mm(rows, gate_ref[...])
+    linear = mm(rows, linear_ref[...])
+    out_ref[...] = (jax.nn.silu(gate) * linear).astype(bf16)
 
 
 def down_kernel(own_ref, last_ref, next_ref, w_own_ref, w_last_ref, w_next_ref, out_ref):
@@ -430,11 +441,12 @@
 
 
 def final_kernel(answers_ref, mix_ref, middle_ref, gain_ref, out_ref, rows_ref):
-    each = middle_ref.shape[1] // lanes
-    mixing = split(mix_ref[...], 3)
+    share, width = middle_ref.shape
+    mixing = jnp.concatenate(split(mix_ref[...], 3), axis=0)
     routed = []
-    for answers in from_lines(answers_ref, rows_ref, each):
-        routed.append(mm(mixing[0], answers) + mm(mixing[1], answers) + mm(mixing[2], answers))
+    for answers in from_lines(answers_ref, rows_ref, width // lanes):
+        three = mm(mixing, answers)
+        routed.append(three[:share] + three[share : 2 * share] + three[2 * share :])
     routed = jnp.concatenate(routed, axis=1)
     out_ref[...] = normed(deep_alpha * middle_ref[...] + routed, gain_ref[...]).astype(bf16)
 
@@ -548,7 +560,7 @@
     def hidden_of(upper, lower):
         return call(
             hidden_kernel, shape((slots, gate_weight.shape[2]), bf16),
-            [pltpu.VMEM((lines // 2, lanes), f32)], 1 << 29,
+            [pltpu.VMEM((lines // 2, lanes), f32)] * 2, 1 << 29,
             upper, lower, gate_weight[0], linear_weight[0],
         )
 

time: 141 us -> 141 us (level)
  no operation moved by 1% of the time
where the time goes in v4:
time: 141 us; the launch traced here: 140 us
  waiting for transfers between devices  48.7 us (35%)
  starting transfers between devices  40.3 us (29%)
  blocking collectives  30.4 us (22%)
  Pallas kernels  17.6 us (12%)
  local copies, waits for them, and re-layouts  2.87 us (2%)
    all_to_all x1, blocking collectives, exchanged(): lax.all_to_all(array.reshape(blocks, lines // blocks, lanes), 'sp', split...  30.4 us
    ppermute x16, waiting for transfers between devices, moved(): return lax.ppermute(array, 'tp', way)  26.4 us
    ppermute x16, starting transfers between devices, moved(): return lax.ppermute(array, 'tp', way)  20.3 us
    pallas_call x11, Pallas kernels, call(): pl.pallas_call(kernel, out_shape=outs, in_specs=[pl.BlockSpec(memory_spac...  17.6 us
    all_to_all x1, waiting for transfers between devices, exchanged(): lax.all_to_all(array.reshape(blocks, lines // blocks, lanes), 'sp', split...  15.3 us
    all_to_all x1, starting transfers between devices, on_device(): come = lax.all_to_all(send, 'sp', split_axis=0, concat_axis=0, tiled=True)  13.1 us
    all_to_all x1, waiting for transfers between devices, on_device(): come = lax.all_to_all(send, 'sp', split_axis=0, concat_axis=0, tiled=True)  6.95 us
    all_to_all x1, starting transfers between devices, exchanged(): lax.all_to_all(array.reshape(blocks, lines // blocks, lanes), 'sp', split...  6.79 us
  transfers between devices with their start and end apart: 18, of which 10 were waited for; matrix products, arithmetic and copies ran while one was open for 2% of the time, Pallas kernels for 6%

profile of v4, /device:TPU:1, one launch (start us, length us, event | category | flops | bytes accessed | tf_op | source)
XLA Modules:
  0.0 140.2 jit_solution(9648999446026201500)
XLA Ops:
  0.1 3.6 %shard_map.181 = bf16[64,2,640]{2,1,0:T(2,128)(2,1)} custom-call(bf16[192,128]{1,0:T(8,128)(2,1)} %x_ref.3, f32[8,192]{1,0:T(8,128)} %bitcast.48, f32[2,8,64]{2,1,0:T(8,128)} %rate_ref.5, f32[2,8,64]{2,1,0:T(8,128)} %turn_ref.5, f32[2,128,64]{2,1,0:T(8,128)} %bitcast.40, f32[2,128,64]{2,1,0:T(8,128)} %bitcast.42), custom_call_target="tpu_custom_call" | custom-call | flops 1073741824 | bytes 1048576 | tf_op jit(solution)/shard_map/pallas_call | solution.py:461
  3.7 13.1 %all-to-all-start = ((bf16[64,2,640]{2,1,0:T(2,128)(2,1)}), bf16[64,2,640]{2,1,0:T(2,128)(2,1)S(1)}, u32[]{:S(2)}, u32[]{:S(2)}) async-start(bf16[64,2,640]{2,1,0:T(2,128)(2,1)} %shard_map.181), calls=%async_computation | async-start | bytes 327680 | tf_op jit(solution)/shard_map/all_to_all | solution.py:505
  17.0 0.0 copy-start.2
  17.0 0.0 copy-start.4
  17.0 0.0 copy-start.7
  17.0 3.9 %shard_map.182 = (f32[192,128]{1,0:T(8,128)S(1)}, f32[2,64,512]{2,1,0:T(8,128)S(1)}, bf16[128,48]{1,0:T(8,128)(2,1)S(1)}, f32[48,128]{1,0:T(8,128)S(1)}) custom-call(bf16[192,128]{1,0:T(8,128)(2,1)S(1)} %copy-done.13, f32[8,192]{1,0:T(8,128)S(1)} %bitcast.49, f32[2,8,64]{2,1,0:T(8,128)S(1)} %copy-done.15, f32[2,8,64]{2,1,0:T(8,128)S(1)} %copy-done.16, ...), custom_call_target="tpu_custom_call" | custom-call | flops 1073741824 | bytes 1048576 | tf_op jit(solution)/shard_map/pallas_call | solution.py:461
  21.0 0.6 copy-done.5
  21.6 7.0 %all-to-all-done.come_ref = bf16[64,2,640]{2,1,0:T(2,128)(2,1)S(1)} async-done(((bf16[64,2,640]{2,1,0:T(2,128)(2,1)}), bf16[64,2,640]{2,1,0:T(2,128)(2,1)S(1)}, u32[]{:S(2)}, u32[]{:S(2)}) %all-to-all-start) | async-done | bytes 163872 | tf_op jit(solution)/shard_map/all_to_all | solution.py:505
  28.5 1.7 %shard_map.183 = (bf16[48,128]{1,0:T(8,128)(2,1)S(1)}, bf16[48,128]{1,0:T(8,128)(2,1)S(1)}, bf16[48,128]{1,0:T(8,128)(2,1)S(1)}, bf16[48,128]{1,0:T(8,128)(2,1)S(1)}) custom-call(bf16[64,2,640]{2,1,0:T(2,128)(2,1)S(1)} %all-to-all-done.come_ref, f32[192,128]{1,0:T(8,128)S(1)} %get-tuple-element.15.local_ref, f32[8,192]{1,0:T(8,128)S(1)} %bitcast.50, ...), custom_call_target="tpu_custom_call" | custom-call | flops 536870912 | bytes 1048576 | tf_op jit(solution)/shard_map/pallas_call | solution.py:461
  30.3 1.3 collective-permute-start
  31.6 2.4 %collective-permute-start.1 = (bf16[48,128]{1,0:T(8,128)(2,1)S(1)}, bf16[48,128]{1,0:T(8,128)(2,1)S(1)}, u32[]{:S(2)}, u32[]{:S(2)}) collective-permute-start(bf16[48,128]{1,0:T(8,128)(2,1)S(1)} %get-tuple-element.19), channel_id=1, source_target_pairs={{0,2},{1,3},{2,0},{3,1},{4,6},{5,7},{6,4},{7,5},{8,10},{9,11},{10,... | collective-permute-start | bytes 36872 | tf_op jit(solution)/shard_map/ppermute | solution.py:489
  34.0 1.1 collective-permute-start.2
  35.2 0.5 collective-permute-done.1.from_far_ref
  35.6 1.2 collective-permute-done.2.from_next_ref
  36.9 1.9 %shard_map.184 = (f32[48,2048]{1,0:T(8,128)S(1)}, bf16[2048,128]{1,0:T(8,128)(2,1)}) custom-call(bf16[48,128]{1,0:T(8,128)(2,1)S(1)} %get-tuple-element.17.own_ref, bf16[48,128]{1,0:T(8,128)(2,1)S(1)} %collective-permute-done.from_last_ref, bf16[48,128]{1,0:T(8,128)(2,1)S(1)} %collective-permute-done.1.from_far_ref, ...), custom_call_target="tpu_custom_call" | custom-call | flops 536870912 | bytes 1048576 | tf_op jit(solution)/shard_map/pallas_call | solution.py:461
  38.8 6.8 %all-to-all-start.1 = ((bf16[64,32,128]{2,1,0:T(8,128)(2,1)}), bf16[64,32,128]{2,1,0:T(8,128)(2,1)}, u32[]{:S(2)}, u32[]{:S(2)}) async-start(bf16[64,32,128]{2,1,0:T(8,128)(2,1)} %bitcast.10), calls=%async_computation.1 | async-start | bytes 1048576 | tf_op jit(solution)/shard_map/all_to_all | solution.py:546
  45.6 2.4 %collective-permute-start.10 = (bf16[256,2048]{1,0:T(8,128)(2,1)}, bf16[256,2048]{1,0:T(8,128)(2,1)S(1)}, u32[]{:S(2)}, u32[]{:S(2)}) collective-permute-start(bf16[256,2048]{1,0:T(8,128)(2,1)} %bitcast.29), channel_id=1, source_target_pairs={{0,3},{1,0},{2,1},{3,2},{4,7},{5,4},{6,5},{7,6},{8,11},{9,8},{10,9... | collective-permute-start | bytes 3145736 | tf_op jit(solution)/shard_map/ppermute | solution.py:489
  48.0 0.0 collective-permute-start.9
  48.0 15.3 %all-to-all-done.1 = bf16[64,32,128]{2,1,0:T(8,128)(2,1)} async-done(((bf16[64,32,128]{2,1,0:T(8,128)(2,1)}), bf16[64,32,128]{2,1,0:T(8,128)(2,1)}, u32[]{:S(2)}, u32[]{:S(2)}) %all-to-all-start.1) | async-done | bytes 524320 | tf_op jit(solution)/shard_map/all_to_all | solution.py:546
  63.3 1.1 fusion
  64.4 0.1 collective-permute-start.6
  64.5 0.9 collective-permute-start.7
  65.4 1.9 %collective-permute-start.4 = (bf16[1024,128]{1,0:T(8,128)(2,1)S(1)}, bf16[1024,128]{1,0:T(8,128)(2,1)S(1)}, u32[]{:S(2)}, u32[]{:S(2)}) collective-permute-start(bf16[1024,128]{1,0:T(8,128)(2,1)S(1)} %bitcast.33), channel_id=1, source_target_pairs={{0,3},{1,0},{2,1},{3,2},{4,7},{5,4},{6,5},{7,6},{8,11},{9,8},{10,9... | collective-permute-start | bytes 786440 | tf_op jit(solution)/shard_map/ppermute | solution.py:489
  67.2 3.0 %collective-permute-done.10.w_next_ref = bf16[256,2048]{1,0:T(8,128)(2,1)S(1)} collective-permute-done((bf16[256,2048]{1,0:T(8,128)(2,1)}, bf16[256,2048]{1,0:T(8,128)(2,1)S(1)}, u32[]{:S(2)}, u32[]{:S(2)}) %collective-permute-start.10) | collective-permute-done | bytes 1048608 | tf_op jit(solution)/shard_map/ppermute | solution.py:489
  70.3 3.4 %collective-permute-start.15 = (bf16[128,2048]{1,0:T(8,128)(2,1)S(1)}, bf16[128,2048]{1,0:T(8,128)(2,1)S(1)}, u32[]{:S(2)}, u32[]{:S(2)}) collective-permute-start(bf16[128,2048]{1,0:T(8,128)(2,1)S(1)} %slice.27), channel_id=1, source_target_pairs={{0,3},{1,0},{2,1},{3,2},{4,7},{5,4},{6,5},{7,6},{8,11},{9,8},{10,9... | collective-permute-start | bytes 1572872 | tf_op jit(solution)/shard_map/ppermute | solution.py:489
  73.6 0.0 collective-permute-done.9.w_last_ref
  73.6 1.1 slice.26
  74.7 0.1 collective-permute-start.14
  74.8 4.0 %collective-permute-done.6.top_ref = bf16[1024,128]{1,0:T(8,128)(2,1)S(1)} collective-permute-done((bf16[1024,128]{1,0:T(8,128)(2,1)S(1)}, bf16[1024,128]{1,0:T(8,128)(2,1)S(1)}, u32[]{:S(2)}, u32[]{:S(2)}) %collective-permute-start.6) | collective-permute-done | bytes 262176 | tf_op jit(solution)/shard_map/ppermute | solution.py:489
  78.9 5.6 %collective-permute-done.7.low_ref = bf16[1024,128]{1,0:T(8,128)(2,1)S(1)} collective-permute-done((bf16[1024,128]{1,0:T(8,128)(2,1)S(1)}, bf16[1024,128]{1,0:T(8,128)(2,1)S(1)}, u32[]{:S(2)}, u32[]{:S(2)}) %collective-permute-start.7) | collective-permute-done | bytes 262176 | tf_op jit(solution)/shard_map/ppermute | solution.py:489
  84.5 0.0 collective-permute-start.11
  84.5 2.7 %collective-permute-start.12 = (bf16[1024,128]{1,0:T(8,128)(2,1)S(1)}, bf16[1024,128]{1,0:T(8,128)(2,1)S(1)}, u32[]{:S(2)}, u32[]{:S(2)}) collective-permute-start(bf16[1024,128]{1,0:T(8,128)(2,1)S(1)} %collective-permute-done.4.low_ref), channel_id=1, source_target_pairs={{0,3},{1,0},{2,1},{3,2},{4,7},{5,4},{6,5},{7,6},{8,11},{9,8},{10,9... | collective-permute-start | bytes 786440 | tf_op jit(solution)/shard_map/ppermute | solution.py:489
  87.2 0.6 shard_map.187
  87.8 4.8 %collective-permute-done.3.top_ref = bf16[1024,128]{1,0:T(8,128)(2,1)S(1)} collective-permute-done((bf16[1024,128]{1,0:T(8,128)(2,1)S(1)}, bf16[1024,128]{1,0:T(8,128)(2,1)S(1)}, u32[]{:S(2)}, u32[]{:S(2)}) %collective-permute-start.3) | collective-permute-done | bytes 262176 | tf_op jit(solution)/shard_map/ppermute | solution.py:489
  92.6 3.4 %collective-permute-start.8 = (bf16[128,256]{1,0:T(8,128)(2,1)S(1)}, bf16[128,256]{1,0:T(8,128)(2,1)S(1)}, u32[]{:S(2)}, u32[]{:S(2)}) collective-permute-start(bf16[128,256]{1,0:T(8,128)(2,1)S(1)} %shard_map.187), channel_id=1, source_target_pairs={{0,3},{1,0},{2,1},{3,2},{4,7},{5,4},{6,5},{7,6},{8,11},{9,8},{10,9... | collective-permute-start | bytes 196616 | tf_op jit(solution)/shard_map/ppermute | solution.py:489
  96.0 0.6 shard_map.186
  96.6 0.0 copy-start.3
  96.6 4.7 %collective-permute-done.11.top_ref = bf16[1024,128]{1,0:T(8,128)(2,1)S(1)} collective-permute-done((bf16[1024,128]{1,0:T(8,128)(2,1)S(1)}, bf16[1024,128]{1,0:T(8,128)(2,1)S(1)}, u32[]{:S(2)}, u32[]{:S(2)}) %collective-permute-start.11) | collective-permute-done | bytes 262176 | tf_op jit(solution)/shard_map/ppermute | solution.py:489
  101.3 0.6 shard_map.189
  101.9 0.6 collective-permute-start.13
  102.5 0.6 shard_map.185.own_ref
  103.1 0.0 collective-permute-done.8.next_ref
  103.2 2.5 %collective-permute-done.5.last_ref = bf16[128,256]{1,0:T(8,128)(2,1)S(1)} collective-permute-done((bf16[128,256]{1,0:T(8,128)(2,1)S(1)}, bf16[128,256]{1,0:T(8,128)(2,1)S(1)}, u32[]{:S(2)}, u32[]{:S(2)}) %collective-permute-start.5) | collective-permute-done | bytes 65568 | tf_op jit(solution)/shard_map/ppermute | solution.py:489
  105.7 1.9 %shard_map.188.sum_ref = f32[128,2048]{1,0:T(8,128)S(1)} custom-call(bf16[128,256]{1,0:T(8,128)(2,1)S(1)} %shard_map.185.own_ref, bf16[128,256]{1,0:T(8,128)(2,1)S(1)} %collective-permute-done.5.last_ref, bf16[128,256]{1,0:T(8,128)(2,1)S(1)} %collective-permute-done.8.next_ref, bf16[256,2048]{1,0:T(8,128)(2,1)S(1)} %bitcast.31, ...), custom_call_target="tpu_custom_call" | custom-call | flops 536870912 | bytes 1048576 | tf_op jit(solution)/shard_map/pallas_call | solution.py:461
  107.5 0.0 copy-start.8
  107.6 0.7 shard_map.190
  108.3 30.4 %all_to_all.15 = bf16[64,32,128]{2,1,0:T(8,128)(2,1)S(1)} all-to-all(bf16[64,32,128]{2,1,0:T(8,128)(2,1)S(1)} %bitcast.28), channel_id=1, replica_groups=mesh['sp'=64,'tp'=4] {'sp'}, dimensions={0} | all-to-all | bytes 1048576 | tf_op jit(solution)/shard_map/all_to_all | solution.py:546
  138.7 1.5 %shard_map.191 = bf16[48,2048]{1,0:T(8,128)(2,1)} custom-call(bf16[2048,128]{1,0:T(8,128)(2,1)S(1)} %bitcast.27, f32[48,128]{1,0:T(8,128)S(1)} %copy-done.6, f32[48,2048]{1,0:T(8,128)S(1)} %get-tuple-element.24.middle_ref, f32[1,2048]{1,0:T(1,128)S(1)} %bitcast.39), custom_call_target="tpu_custom_call" | custom-call | flops 268435456 | bytes 1048576 | tf_op jit(solution)/shard_map/pallas_call | solution.py:461
  (45 shorter events, 0.1 us)
Async XLA Ops:
  0.0 16.9 %copy-start.9 = (f32[2,8,16,64]{3,2,1,0:T(8,128)S(1)}, f32[2,8,16,64]{3,2,1,0:T(8,128)}, u32[]{:S(2)}) copy-start(f32[2,8,16,64]{3,2,1,0:T(8,128)} %param.24) | copy-start | bytes 196612
  0.0 16.9 %copy-start.10 = (f32[2,8,16,64]{3,2,1,0:T(8,128)S(1)}, f32[2,8,16,64]{3,2,1,0:T(8,128)}, u32[]{:S(2)}) copy-start(f32[2,8,16,64]{3,2,1,0:T(8,128)} %param.25) | copy-start | bytes 196612
  0.0 16.9 %copy-start.11 = (f32[2,8,16,64]{3,2,1,0:T(8,128)S(1)}, f32[2,8,16,64]{3,2,1,0:T(8,128)}, u32[]{:S(2)}) copy-start(f32[2,8,16,64]{3,2,1,0:T(8,128)} %param.26) | copy-start | bytes 196612
  0.0 16.9 %copy-start.12 = (f32[2,8,16,64]{3,2,1,0:T(8,128)S(1)}, f32[2,8,16,64]{3,2,1,0:T(8,128)}, u32[]{:S(2)}) copy-start(f32[2,8,16,64]{3,2,1,0:T(8,128)} %param.27) | copy-start | bytes 196612
  0.0 16.9 %copy-start.13 = (bf16[192,128]{1,0:T(8,128)(2,1)S(1)}, bf16[192,128]{1,0:T(8,128)(2,1)}, u32[]{:S(2)}) copy-start(bf16[192,128]{1,0:T(8,128)(2,1)} %x_ref.3) | copy-start | bytes 147460
  0.0 16.9 %copy-start.14 = (f32[192,8]{0,1:T(8,128)S(1)}, f32[192,8]{0,1:T(8,128)}, u32[]{:S(2)}) copy-start(f32[192,8]{0,1:T(8,128)} %param.21) | copy-start | bytes 18436
  0.0 16.9 %copy-start.15 = (f32[2,8,64]{2,1,0:T(8,128)S(1)}, f32[2,8,64]{2,1,0:T(8,128)}, u32[]{:S(2)}) copy-start(f32[2,8,64]{2,1,0:T(8,128)} %rate_ref.5) | copy-start | bytes 12292
  0.0 16.9 %copy-start.16 = (f32[2,8,64]{2,1,0:T(8,128)S(1)}, f32[2,8,64]{2,1,0:T(8,128)}, u32[]{:S(2)}) copy-start(f32[2,8,64]{2,1,0:T(8,128)} %turn_ref.5) | copy-start | bytes 12292
  0.1 16.9 %copy-start.17 = (s32[192,2]{0,1:T(2,128)S(1)}, s32[192,2]{0,1:T(2,128)}, u32[]{:S(2)}) copy-start(s32[192,2]{0,1:T(2,128)} %param.32) | copy-start | bytes 4612
  0.1 16.9 %copy-start.18 = (f32[192,2]{0,1:T(2,128)S(1)}, f32[192,2]{0,1:T(2,128)}, u32[]{:S(2)}) copy-start(f32[192,2]{0,1:T(2,128)} %param.34) | copy-start | bytes 4612
  0.1 16.9 %copy-start.19 = (f32[192]{0:T(256)S(1)}, f32[192]{0:T(256)}, u32[]{:S(2)}) copy-start(f32[192]{0:T(256)} %param.33) | copy-start | bytes 2308
  0.1 16.9 %copy-start.20 = (f32[128]{0:T(128)S(1)}, f32[128]{0:T(128)}, u32[]{:S(2)}) copy-start(f32[128]{0:T(128)} %param.28) | copy-start | bytes 1540
  3.7 24.8 %all-to-all-start = ((bf16[64,2,640]{2,1,0:T(2,128)(2,1)}), bf16[64,2,640]{2,1,0:T(2,128)(2,1)S(1)}, u32[]{:S(2)}, u32[]{:S(2)}) async-start(bf16[64,2,640]{2,1,0:T(2,128)(2,1)} %shard_map.181), calls=%async_computation | async-start | bytes 327680 | tf_op jit(solution)/shard_map/all_to_all | solution.py:505
  17.0 19.9 %copy-start.2 = (bf16[512,2048]{1,0:T(8,128)(2,1)S(1)}, bf16[512,2048]{1,0:T(8,128)(2,1)}, u32[]{:S(2)}) copy-start(bf16[512,2048]{1,0:T(8,128)(2,1)} %weight_ref.1) | copy-start | bytes 6291460
  17.0 19.8 %copy-start.4 = (bf16[48,2048]{1,0:T(8,128)(2,1)S(1)}, bf16[48,2048]{1,0:T(8,128)(2,1)}, u32[]{:S(2)}) copy-start(bf16[48,2048]{1,0:T(8,128)(2,1)} %residual_ref.1) | copy-start | bytes 589828
  17.0 19.8 %copy-start.7 = (f32[2048]{0:T(1024)S(1)}, f32[2048]{0:T(1024)}, u32[]{:S(2)}) copy-start(f32[2048]{0:T(1024)} %param.30) | copy-start | bytes 24580
  21.0 0.6 copy-start.5
  30.3 4.9 %collective-permute-start = (bf16[48,128]{1,0:T(8,128)(2,1)S(1)}, bf16[48,128]{1,0:T(8,128)(2,1)S(1)}, u32[]{:S(2)}, u32[]{:S(2)}) collective-permute-start(bf16[48,128]{1,0:T(8,128)(2,1)S(1)} %get-tuple-element.18), channel_id=1, source_target_pairs={{0,1},{1,2},{2,3},{3,0},{4,5},{5,6},{6,7},{7,4},{8,9},{9,10},{10,1... | collective-permute-start | bytes 36872 | tf_op jit(solution)/shard_map/ppermute | solution.py:489
  31.6 4.0 %collective-permute-start.1 = (bf16[48,128]{1,0:T(8,128)(2,1)S(1)}, bf16[48,128]{1,0:T(8,128)(2,1)S(1)}, u32[]{:S(2)}, u32[]{:S(2)}) collective-permute-start(bf16[48,128]{1,0:T(8,128)(2,1)S(1)} %get-tuple-element.19), channel_id=1, source_target_pairs={{0,2},{1,3},{2,0},{3,1},{4,6},{5,7},{6,4},{7,5},{8,10},{9,11},{10,... | collective-permute-start | bytes 36872 | tf_op jit(solution)/shard_map/ppermute | solution.py:489
  34.0 2.8 %collective-permute-start.2 = (bf16[48,128]{1,0:T(8,128)(2,1)S(1)}, bf16[48,128]{1,0:T(8,128)(2,1)S(1)}, u32[]{:S(2)}, u32[]{:S(2)}) collective-permute-start(bf16[48,128]{1,0:T(8,128)(2,1)S(1)} %get-tuple-element.20), channel_id=1, source_target_pairs={{0,3},{1,0},{2,1},{3,2},{4,7},{5,4},{6,5},{7,6},{8,11},{9,8},{10,9... | collective-permute-start | bytes 36872 | tf_op jit(solution)/shard_map/ppermute | solution.py:489
  38.8 48.4 %copy-start = (bf16[1,2048,256]{2,1,0:T(8,128)(2,1)S(1)}, bf16[1,2048,256]{2,1,0:T(8,128)(2,1)}, u32[]{:S(2)}) copy-start(bf16[1,2048,256]{2,1,0:T(8,128)(2,1)} %param.35) | copy-start | bytes 3145732
  38.8 48.4 %copy-start.1 = (bf16[1,2048,256]{2,1,0:T(8,128)(2,1)S(1)}, bf16[1,2048,256]{2,1,0:T(8,128)(2,1)}, u32[]{:S(2)}) copy-start(bf16[1,2048,256]{2,1,0:T(8,128)(2,1)} %param.36) | copy-start | bytes 3145732
  38.8 24.5 %all-to-all-start.1 = ((bf16[64,32,128]{2,1,0:T(8,128)(2,1)}), bf16[64,32,128]{2,1,0:T(8,128)(2,1)}, u32[]{:S(2)}, u32[]{:S(2)}) async-start(bf16[64,32,128]{2,1,0:T(8,128)(2,1)} %bitcast.10), calls=%async_computation.1 | async-start | bytes 1048576 | tf_op jit(solution)/shard_map/all_to_all | solution.py:546
  45.6 24.6 %collective-permute-start.10 = (bf16[256,2048]{1,0:T(8,128)(2,1)}, bf16[256,2048]{1,0:T(8,128)(2,1)S(1)}, u32[]{:S(2)}, u32[]{:S(2)}) collective-permute-start(bf16[256,2048]{1,0:T(8,128)(2,1)} %bitcast.29), channel_id=1, source_target_pairs={{0,3},{1,0},{2,1},{3,2},{4,7},{5,4},{6,5},{7,6},{8,11},{9,8},{10,9... | collective-permute-start | bytes 3145736 | tf_op jit(solution)/shard_map/ppermute | solution.py:489
  48.0 25.6 %collective-permute-start.9 = (bf16[256,2048]{1,0:T(8,128)(2,1)}, bf16[256,2048]{1,0:T(8,128)(2,1)}, u32[]{:S(2)}, u32[]{:S(2)}) collective-permute-start(bf16[256,2048]{1,0:T(8,128)(2,1)} %bitcast.30), channel_id=1, source_target_pairs={{0,1},{1,2},{2,3},{3,0},{4,5},{5,6},{6,7},{7,4},{8,9},{9,10},{10,1... | collective-permute-start | bytes 3145736 | tf_op jit(solution)/shard_map/ppermute | solution.py:489
  64.4 14.5 %collective-permute-start.6 = (bf16[1024,128]{1,0:T(8,128)(2,1)S(1)}, bf16[1024,128]{1,0:T(8,128)(2,1)S(1)}, u32[]{:S(2)}, u32[]{:S(2)}) collective-permute-start(bf16[1024,128]{1,0:T(8,128)(2,1)S(1)} %bitcast.35), channel_id=1, source_target_pairs={{0,1},{1,2},{2,3},{3,0},{4,5},{5,6},{6,7},{7,4},{8,9},{9,10},{10,1... | collective-permute-start | bytes 786440 | tf_op jit(solution)/shard_map/ppermute | solution.py:489
  64.5 20.0 %collective-permute-start.7 = (bf16[1024,128]{1,0:T(8,128)(2,1)S(1)}, bf16[1024,128]{1,0:T(8,128)(2,1)S(1)}, u32[]{:S(2)}, u32[]{:S(2)}) collective-permute-start(bf16[1024,128]{1,0:T(8,128)(2,1)S(1)} %bitcast.32), channel_id=1, source_target_pairs={{0,1},{1,2},{2,3},{3,0},{4,5},{5,6},{6,7},{7,4},{8,9},{9,10},{10,1... | collective-permute-start | bytes 786440 | tf_op jit(solution)/shard_map/ppermute | solution.py:489
  65.4 19.1 %collective-permute-start.4 = (bf16[1024,128]{1,0:T(8,128)(2,1)S(1)}, bf16[1024,128]{1,0:T(8,128)(2,1)S(1)}, u32[]{:S(2)}, u32[]{:S(2)}) collective-permute-start(bf16[1024,128]{1,0:T(8,128)(2,1)S(1)} %bitcast.33), channel_id=1, source_target_pairs={{0,3},{1,0},{2,1},{3,2},{4,7},{5,4},{6,5},{7,6},{8,11},{9,8},{10,9... | collective-permute-start | bytes 786440 | tf_op jit(solution)/shard_map/ppermute | solution.py:489
  70.3 37.3 %collective-permute-start.15 = (bf16[128,2048]{1,0:T(8,128)(2,1)S(1)}, bf16[128,2048]{1,0:T(8,128)(2,1)S(1)}, u32[]{:S(2)}, u32[]{:S(2)}) collective-permute-start(bf16[128,2048]{1,0:T(8,128)(2,1)S(1)} %slice.27), channel_id=1, source_target_pairs={{0,3},{1,0},{2,1},{3,2},{4,7},{5,4},{6,5},{7,6},{8,11},{9,8},{10,9... | collective-permute-start | bytes 1572872 | tf_op jit(solution)/shard_map/ppermute | solution.py:489
  74.7 32.8 %collective-permute-start.14 = (bf16[128,2048]{1,0:T(8,128)(2,1)S(1)}, bf16[128,2048]{1,0:T(8,128)(2,1)S(1)}, u32[]{:S(2)}, u32[]{:S(2)}) collective-permute-start(bf16[128,2048]{1,0:T(8,128)(2,1)S(1)} %slice.26), channel_id=1, source_target_pairs={{0,1},{1,2},{2,3},{3,0},{4,5},{5,6},{6,7},{7,4},{8,9},{9,10},{10,1... | collective-permute-start | bytes 1572872 | tf_op jit(solution)/shard_map/ppermute | solution.py:489
  78.9 13.7 %collective-permute-start.3 = (bf16[1024,128]{1,0:T(8,128)(2,1)S(1)}, bf16[1024,128]{1,0:T(8,128)(2,1)S(1)}, u32[]{:S(2)}, u32[]{:S(2)}) collective-permute-start(bf16[1024,128]{1,0:T(8,128)(2,1)S(1)} %bitcast.36), channel_id=1, source_target_pairs={{0,3},{1,0},{2,1},{3,2},{4,7},{5,4},{6,5},{7,6},{8,11},{9,8},{10,9... | collective-permute-start | bytes 786440 | tf_op jit(solution)/shard_map/ppermute | solution.py:489
  84.5 16.9 %collective-permute-start.11 = (bf16[1024,128]{1,0:T(8,128)(2,1)S(1)}, bf16[1024,128]{1,0:T(8,128)(2,1)S(1)}, u32[]{:S(2)}, u32[]{:S(2)}) collective-permute-start(bf16[1024,128]{1,0:T(8,128)(2,1)S(1)} %collective-permute-done.6.top_ref), channel_id=1, source_target_pairs={{0,1},{1,2},{2,3},{3,0},{4,5},{5,6},{6,7},{7,4},{8,9},{9,10},{10,1... | collective-permute-start | bytes 786440 | tf_op jit(solution)/shard_map/ppermute | solution.py:489
  84.5 16.9 %collective-permute-start.12 = (bf16[1024,128]{1,0:T(8,128)(2,1)S(1)}, bf16[1024,128]{1,0:T(8,128)(2,1)S(1)}, u32[]{:S(2)}, u32[]{:S(2)}) collective-permute-start(bf16[1024,128]{1,0:T(8,128)(2,1)S(1)} %collective-permute-done.4.low_ref), channel_id=1, source_target_pairs={{0,3},{1,0},{2,1},{3,2},{4,7},{5,4},{6,5},{7,6},{8,11},{9,8},{10,9... | collective-permute-start | bytes 786440 | tf_op jit(solution)/shard_map/ppermute | solution.py:489
  92.6 10.6 %collective-permute-start.8 = (bf16[128,256]{1,0:T(8,128)(2,1)S(1)}, bf16[128,256]{1,0:T(8,128)(2,1)S(1)}, u32[]{:S(2)}, u32[]{:S(2)}) collective-permute-start(bf16[128,256]{1,0:T(8,128)(2,1)S(1)} %shard_map.187), channel_id=1, source_target_pairs={{0,3},{1,0},{2,1},{3,2},{4,7},{5,4},{6,5},{7,6},{8,11},{9,8},{10,9... | collective-permute-start | bytes 196616 | tf_op jit(solution)/shard_map/ppermute | solution.py:489
  96.6 9.1 %copy-start.3 = (bf16[1,256,2048]{2,1,0:T(8,128)(2,1)S(1)}, bf16[1,256,2048]{2,1,0:T(8,128)(2,1)}, u32[]{:S(2)}) copy-start(bf16[1,256,2048]{2,1,0:T(8,128)(2,1)} %param.37) | copy-start | bytes 3145732
  101.3 4.3 %collective-permute-start.5 = (bf16[128,256]{1,0:T(8,128)(2,1)S(1)}, bf16[128,256]{1,0:T(8,128)(2,1)S(1)}, u32[]{:S(2)}, u32[]{:S(2)}) collective-permute-start(bf16[128,256]{1,0:T(8,128)(2,1)S(1)} %shard_map.186), channel_id=1, source_target_pairs={{0,1},{1,2},{2,3},{3,0},{4,5},{5,6},{6,7},{7,4},{8,9},{9,10},{10,1... | collective-permute-start | bytes 196616 | tf_op jit(solution)/shard_map/ppermute | solution.py:489
  101.9 5.6 %collective-permute-start.13 = (bf16[128,256]{1,0:T(8,128)(2,1)S(1)}, bf16[128,256]{1,0:T(8,128)(2,1)S(1)}, u32[]{:S(2)}, u32[]{:S(2)}) collective-permute-start(bf16[128,256]{1,0:T(8,128)(2,1)S(1)} %shard_map.189), channel_id=1, source_target_pairs={{0,2},{1,3},{2,0},{3,1},{4,6},{5,7},{6,4},{7,5},{8,10},{9,11},{10,... | collective-permute-start | bytes 196616 | tf_op jit(solution)/shard_map/ppermute | solution.py:489
  107.5 31.2 %copy-start.6 = (f32[48,128]{1,0:T(8,128)S(1)}, f32[48,128]{1,0:T(8,128)}, u32[]{:S(2)}) copy-start(f32[48,128]{1,0:T(8,128)} %copy-done.5) | copy-start | bytes 73732
  107.5 31.2 %copy-start.8 = (f32[2048]{0:T(1024)S(1)}, f32[2048]{0:T(1024)}, u32[]{:S(2)}) copy-start(f32[2048]{0:T(1024)} %param.31) | copy-start | bytes 24580
